TPU v7x, 512 devices: a whole 4x8x8 slice. The times are simulated.
512 devices in a mesh: sp: 128 (over z, y, core), tp: 4 (over x).
Axes of the slice: x: 4, y: 8, z: 8, core: 2. Of those that a mesh axis runs over, the one named last changes fastest.
Arguments:
- tokens: bfloat16 [24576, 2048], P('sp', 'tp'), may hold values from -6 to 6
- norm_gain: float32 [2048], replicated, may hold values from 0.1 to 1.9
- query_weight: bfloat16 [2048, 512], P('sp', 'tp'), may hold values from -0.125 to 0.125
- key_weight: bfloat16 [2048, 512], P('sp', 'tp'), may hold values from -0.125 to 0.125
- value_weight: bfloat16 [2048, 512], P('sp', 'tp'), may hold values from -0.125 to 0.125
- decay_weight: bfloat16 [2048, 512], P('sp', 'tp'), may hold values from -0.09375 to 0.09375
- removal_weight: bfloat16 [2048, 512], P('sp', 'tp'), may hold values from -0.125 to 0.125
- gate_weight: bfloat16 [2048, 512], P('sp', 'tp'), may hold values from -0.125 to 0.125
- key_gain: float32 [512], P('tp'), may hold values from 0.1 to 1.9
- removal_gain: float32 [512], P('tp'), may hold values from 0.1 to 1.9
- removal_bias: float32 [512], P('tp'), may hold values from -9 to 1
- decay_bias: float32 [512], P('tp'), may hold values from -12.7 to -1.8
- decay_extra: float32 [24576, 512], P('sp', 'tp'), may hold values from 0 to 0.7
- scan_norm_gain: float32 [512], P('tp'), may hold values from 0.1 to 1.9
- conv_value_weight: bfloat16 [2048, 512], P('sp', 'tp'), may hold values from -0.125 to 0.125
- conv_gate_weight: bfloat16 [2048, 512], P('sp', 'tp'), may hold values from -0.125 to 0.125
- conv_kernel: float32 [31, 512], P(None, 'tp'), may hold values from -2 to 2
- conv_bias: float32 [512], P('tp'), may hold values from -2 to 3
- conv_norm_gain: float32 [512], P('tp'), may hold values from 0.1 to 1.9
- out_scan_weight: bfloat16 [512, 2048], P('tp', 'sp'), may hold values from -0.1875 to 0.1875
- out_conv_weight: bfloat16 [512, 2048], P('tp', 'sp'), may hold values from -0.1875 to 0.1875
Outputs:
- mixed: bfloat16 [24576, 2048], P('sp', 'tp')
All inputs are finite; a program needn't handle non-finite values.
Results may differ from a plain program's by a relative error of at most 0.0073.
Values may be sent and summed in bfloat16 or wider, within the bound.
No kernel may reach another device: no remote copies, remote signals or barrier semaphores. Data moves between devices by JAX's collectives and lax.ppermute only.
A program may use at most 64 MiB of HBM per device.

v0:
```python
import jax
import jax.numpy as jnp
from jax import lax
from jax.sharding import Mesh
from jax.sharding import PartitionSpec as P

HEAD_SIZE = 64
CONV_K = 31
BLOCK = 32
SP = ("sp_0", "sp_1", "sp_2")


exact_setting = lax.Precision.HIGHEST


def neutral_like(x, identity):
    return jax.tree.map(
        lambda part, zero: jnp.zeros_like(part) + jnp.asarray(zero, part.dtype), x, identity
    )


def collected_together(x, axis):
    leaves = jax.tree.leaves(x)
    sequence = sorted(range(len(leaves)), key=lambda k: -leaves[k].size)
    width = (1, *leaves[sequence[0]].shape)[-1]
    lines = [
        jnp.pad(leaves[k].reshape(-1), (0, -leaves[k].size % width)).reshape(-1, width)
        for k in sequence
    ]
    both, at, found = (lax.all_gather(jnp.concatenate(lines), axis), 0, {})
    for k, line in zip(sequence, lines):
        slab = both[:, at : at + len(line)].reshape(len(both), -1)
        found[k] = slab[:, : leaves[k].size].reshape(-1, *leaves[k].shape)
        at += len(line)
    numbers = iter(range(len(leaves)))
    return jax.tree.map(lambda _: found[next(numbers)], x)


def carried_in(x, axes, combine, identity):
    before = start = neutral_like(x, identity)
    total = x
    for axis in reversed(axes):
        size, here = (lax.axis_size(axis), lax.axis_index(axis))
        pieces = collected_together(total, axis)
        inside, total = (start, start)
        for k in range(size):
            passed = k < here
            total = combine(total, jax.tree.map(lambda part: part[k], pieces))
            inside = jax.tree.map(lambda new, old: jnp.where(passed, new, old), total, inside)
        before = combine(inside, before)
    return before


def shifted(value, axis, steps):
    count = lax.axis_size(axis)
    leading, last = (max(0, -steps), min(count, count - steps))
    return lax.ppermute(value, axis, [(source, source + steps) for source in range(leading, last)])


def copy_for_each(x, axis):
    size = lax.axis_size(axis)
    return lax.all_to_all(jnp.broadcast_to(x[None], (size, *x.shape)), axis, 0, 0, tiled=True)


def taken_together(x, axis):
    everything = copy_for_each(x, axis)
    return jnp.sum(everything, axis=0)


def in_one(arrays, axis):
    vector, at, finished = (jnp.concatenate([a.reshape(-1) for a in arrays]), 0, [])
    total = taken_together(vector, axis)
    for a in arrays:
        finished.append(total[at : at + a.size].reshape(a.shape))
        at += a.size
    return tuple(finished)


def laid_out(pieces, dim):
    pieces = jnp.moveaxis(pieces, 0, dim)
    shape = pieces.shape
    return pieces.reshape(*shape[:dim], shape[dim] * shape[dim + 1], *shape[dim + 2 :])


def gather_directly(x, axis, dim):
    pieces = copy_for_each(x, axis)
    return laid_out(pieces, dim)


def side_by_side(arrays, axis, dim, along):
    both = jnp.concatenate(arrays, axis=along)
    filled, at, finished = (lax.all_gather(both, axis, axis=dim, tiled=True), 0, [])
    for a in arrays:
        finished.append(lax.slice_in_dim(filled, at, at + a.shape[along], axis=along))
        at += a.shape[along]
    return tuple(finished)


def split_up(x, dim, size):
    before, after = (x.shape[:dim], x.shape[dim + 1 :])
    return jnp.moveaxis(x.reshape(*before, size, -1, *after), dim, 0)


def sent_and_summed(x, axis, dim):
    size = lax.axis_size(axis)
    pieces = lax.all_to_all(split_up(x, dim, size), axis, 0, 0, tiled=True)
    return jnp.sum(pieces, axis=0)


def fold_rows(normed, pieces):
    return tuple((jnp.dot(normed, piece, preferred_element_type=jnp.float32) for piece in pieces))


def stored_floats(sums):
    rounded = lax.optimization_barrier(tuple((item.astype(jnp.bfloat16) for item in sums)))
    return tuple((item.astype(jnp.float32) for item in rounded))


def combine_states(earlier, later):
    first = jnp.einsum("hij,hjk->hik", later[0], earlier[0], precision=exact_setting)
    second = jnp.einsum("hij,hjk->hik", later[0], earlier[1], precision=exact_setting) + later[1]
    return (first, second)


def block_product(left, right):
    return jnp.einsum("nhij,nhjk->nhik", left, right, precision=exact_setting)


def pairwise(left, right):
    return jnp.einsum("nhtk,nhik->nhti", left, right, precision=exact_setting)


def scan_mixer(sums, key_gain, removal_gain, removal_bias, decay_bias, decay_extra, scan_norm_gain):
    recept, key_rows, value_rows, decay_pre, removal_pre, gate_pre = stored_floats(sums)
    length = recept.shape[0]
    head_count = recept.shape[1] // HEAD_SIZE
    block_count = length // BLOCK
    decay_rate = jnp.exp(-jax.nn.softplus(-(decay_bias + decay_pre)) - 0.5) + decay_extra
    removal = jax.nn.sigmoid(removal_bias + removal_pre)
    scaled = (key_rows * key_gain).reshape(length, head_count, HEAD_SIZE)
    unit_keys = (
        scaled * lax.rsqrt(jnp.sum(scaled * scaled, axis=-1, keepdims=True) + 1e-06)
    ).reshape(length, -1)
    written = key_rows * (1.0 + (removal - 1.0) * removal_gain)

    def blocked(table):
        return table.reshape(block_count, BLOCK, head_count, HEAD_SIZE).transpose(0, 2, 1, 3)

    recept_b = blocked(recept)
    written_b = blocked(written)
    values_b = blocked(value_rows)
    rate_b = blocked(decay_rate)
    unit_b = blocked(unit_keys)
    removal_b = blocked(removal)
    falling = -jnp.cumsum(rate_b, axis=2)
    before = falling + rate_b
    middle = falling[:, :, BLOCK // 2 : BLOCK // 2 + 1]
    ending = falling[:, :, BLOCK - 1 :]
    alpha = -unit_b
    beta = unit_b * removal_b
    position = jnp.arange(BLOCK)
    strict = (position[:, None] > position[None, :]).astype(jnp.float32)
    inclusive = (position[:, None] >= position[None, :]).astype(jnp.float32)
    alpha_mid = alpha * jnp.exp(before - middle)
    recept_mid = recept_b * jnp.exp(falling - middle)
    beta_mid = beta * jnp.exp(middle - falling)
    keys_mid = written_b * jnp.exp(middle - falling)
    alpha_beta = pairwise(alpha_mid, beta_mid) * strict
    alpha_keys = pairwise(alpha_mid, keys_mid) * strict
    recept_beta = pairwise(recept_mid, beta_mid) * inclusive
    recept_keys = pairwise(recept_mid, keys_mid) * inclusive
    inverse = jnp.eye(BLOCK, dtype=jnp.float32) + alpha_beta
    power = alpha_beta
    for index in range(BLOCK.bit_length() - 2):
        power = block_product(power, power)
        inverse = inverse + block_product(inverse, power)
    widened = jnp.concatenate([values_b, jnp.zeros_like(values_b)], axis=-1)
    rhs_local = block_product(alpha_keys, widened)
    read_local = block_product(recept_keys, widened)
    start_alpha = alpha * jnp.exp(before)
    start_recept = recept_b * jnp.exp(falling)
    end_beta = beta * jnp.exp(ending - falling)
    end_keys = written_b * jnp.exp(ending - falling)
    end_decay = jnp.exp(ending)[:, :, 0, :]

    def advance(carried_state, inputs):
        (
            starting_alpha,
            starting_receptance,
            solver,
            r_beta,
            r_local,
            right_operand,
            ending_beta,
            ending_key_rows,
            e_decay,
            widen_width,
        ) = inputs
        gathered_rows = (
            jnp.einsum("qfl,qlz->qfz", starting_alpha, carried_state, precision=exact_setting)
            + right_operand
        )
        removed_value = jnp.einsum("hti,hiv->htv", solver, gathered_rows, precision=exact_setting)
        readout = (
            jnp.einsum("qfl,qlz->qfz", starting_receptance, carried_state, precision=exact_setting)
            + jnp.einsum("hti,hiv->htv", r_beta, removed_value, precision=exact_setting)
            + r_local
        )
        carried_state = (
            e_decay[:, :, None] * carried_state
            + jnp.einsum("pzw,pzb->pwb", ending_beta, removed_value, precision=exact_setting)
            + jnp.einsum("pzw,pzb->pwb", ending_key_rows, widen_width, precision=exact_setting)
        )
        return (carried_state, readout)

    identity = jnp.broadcast_to(
        jnp.eye(HEAD_SIZE, dtype=jnp.float32), (head_count, HEAD_SIZE, HEAD_SIZE)
    )
    initial = jnp.concatenate([jnp.zeros_like(identity), identity], axis=-1)
    final, readout_rows = lax.scan(
        advance,
        initial,
        (
            start_alpha,
            start_recept,
            inverse,
            recept_beta,
            read_local,
            rhs_local,
            end_beta,
            end_keys,
            end_decay,
            widened,
        ),
    )
    incoming_state = carried_in(
        (final[:, :, HEAD_SIZE:], final[:, :, :HEAD_SIZE]),
        SP,
        combine_states,
        (identity, jnp.zeros_like(identity)),
    )
    reads = readout_rows[..., :HEAD_SIZE] + jnp.einsum(
        "yqem,qmb->yqeb", readout_rows[..., HEAD_SIZE:], incoming_state[1], precision=exact_setting
    )
    reads = reads.transpose(0, 2, 1, 3).reshape(length, head_count, HEAD_SIZE)
    center = jnp.mean(reads, axis=-1, keepdims=True)
    spread = jnp.mean((reads - center) ** 2, axis=-1, keepdims=True)
    normalized = ((reads - center) * lax.rsqrt(spread + 0.00064)).reshape(length, -1)
    return (normalized * scan_norm_gain * jax.nn.sigmoid(gate_pre)).astype(jnp.bfloat16)


def conv_mixer(sums, conv_kernel, conv_bias, conv_norm_gain):
    value_part, gate_part = stored_floats(sums)
    conv_input = (value_part * jax.nn.sigmoid(gate_part)).astype(jnp.bfloat16)
    length = conv_input.shape[0]
    rim = shifted(conv_input[length - (CONV_K - 1) :], SP, 1)
    padded = jnp.concatenate([rim, conv_input], axis=0).astype(jnp.float32)
    filtered = conv_bias + conv_kernel[0] * padded[0:length]
    for index in range(1, CONV_K):
        filtered = filtered + conv_kernel[index] * padded[index : index + length]
    totals = in_one((jnp.sum(filtered, axis=-1), jnp.sum(filtered * filtered, axis=-1)), "tp")
    channels = filtered.shape[1] * lax.axis_size("tp")
    center = totals[0] / channels
    spread = totals[1] / channels - center * center
    scaled = (filtered - center[:, None]) * lax.rsqrt(spread[:, None] + 1e-05) * conv_norm_gain
    return jax.nn.silu(scaled).astype(jnp.bfloat16)


def shards(
    tokens,
    norm_gain,
    query_weight,
    key_weight,
    value_weight,
    decay_weight,
    removal_weight,
    gate_weight,
    key_gain,
    removal_gain,
    removal_bias,
    decay_bias,
    decay_extra,
    scan_norm_gain,
    conv_value_weight,
    conv_gate_weight,
    conv_kernel,
    conv_bias,
    conv_norm_gain,
    out_scan_weight,
    out_conv_weight,
):
    stacked = jnp.concatenate([out_scan_weight, out_conv_weight], axis=0)
    whole = gather_directly(tokens, "tp", 1)
    floats = whole.astype(jnp.float32)
    normed = (
        floats * lax.rsqrt(jnp.mean(floats * floats, axis=-1, keepdims=True) + 1e-06) * norm_gain
    ).astype(jnp.bfloat16)
    projected = fold_rows(
        normed,
        side_by_side(
            (
                query_weight,
                key_weight,
                value_weight,
                decay_weight,
                removal_weight,
                gate_weight,
                conv_value_weight,
                conv_gate_weight,
            ),
            SP,
            0,
            1,
        ),
    )
    scan_sums = projected[:6]
    conv_sums = projected[6:]
    scan_out = scan_mixer(
        scan_sums, key_gain, removal_gain, removal_bias, decay_bias, decay_extra, scan_norm_gain
    )
    conv_out = conv_mixer(conv_sums, conv_kernel, conv_bias, conv_norm_gain)
    features = jnp.concatenate([scan_out, conv_out], axis=1)
    terms = jnp.dot(
        features,
        lax.all_gather(stacked, SP, axis=1, tiled=True),
        preferred_element_type=jnp.float32,
    )
    summed = sent_and_summed(terms, "tp", 1)
    return summed.astype(jnp.bfloat16)


def solution(mesh):
    torus = Mesh(mesh.devices.reshape(8, 8, 2, mesh.shape["tp"]), ("sp_0", "sp_1", "sp_2", "tp"))
    in_specs = (
        P(SP, "tp"),
        P(),
        P(SP, "tp"),
        P(SP, "tp"),
        P(SP, "tp"),
        P(SP, "tp"),
        P(SP, "tp"),
        P(SP, "tp"),
        P("tp"),
        P("tp"),
        P("tp"),
        P("tp"),
        P(SP, "tp"),
        P("tp"),
        P(SP, "tp"),
        P(SP, "tp"),
        P(None, "tp"),
        P("tp"),
        P("tp"),
        P("tp", SP),
        P("tp", SP),
    )
    out_specs = P(SP, "tp")
    return jax.shard_map(
        shards, mesh=torus, in_specs=in_specs, out_specs=out_specs, check_vma=False
    )
```

profile of v0, /device:TPU:24, one launch (start us, length us, event | category | flops | bytes accessed | tf_op | source)
XLA Modules:
  0.0 233.7 jit_solution(4876056362150712214)
XLA Ops:
  12.7 1.9 broadcast_in_dim.27
  14.6 4.4 %all-to-all-start = ((bf16[4,192,512]{2,1,0:T(8,128)(2,1)}), bf16[4,192,512]{2,1,0:T(8,128)(2,1)S(1)}, u32[]{:S(2)}, u32[]{:S(2)}) async-start(bf16[4,192,512]{2,1,0:T(8,128)(2,1)} %broadcast_in_dim.27), calls=%async_computation | async-start | bytes 1572864 | tf_op jit(solution)/shard_map/all_to_all | solution.py:62
  19.0 1.3 pad_maximum_fusion.3
  20.6 1.6 slice_bitcast_fusion.29
  22.1 1.7 slice_bitcast_fusion.30
  23.8 7.5 %all-to-all-done = bf16[4,192,512]{2,1,0:T(8,128)(2,1)S(1)} async-done(((bf16[4,192,512]{2,1,0:T(8,128)(2,1)}), bf16[4,192,512]{2,1,0:T(8,128)(2,1)S(1)}, u32[]{:S(2)}, u32[]{:S(2)}) %all-to-all-start) | async-done | bytes 786464 | tf_op jit(solution)/shard_map/all_to_all | solution.py:62
  32.2 69.2 %all-gather.6.cloned.1.call-done = bf16[2048,1024]{1,0:T(8,128)(2,1)} async-done(((bf16[16,1024]{1,0:T(8,128)(2,1)}), bf16[2048,1024]{1,0:T(8,128)(2,1)}) %all-gather.6.cloned.1.call-update) | async-done | bytes 4194320 | tf_op jit(solution)/shard_map/all_gather | solution.py:92
  101.5 1.4 convolution_convert_fusion.7
  102.9 1.4 convolution_convert_fusion.6
  104.3 2.0 convolution_convert_fusion.5
  106.3 1.4 convolution_convert_fusion.4
  107.7 1.4 convolution_convert_fusion.3
  109.1 1.4 convolution_convert_fusion.2
  114.3 1.4 convolution_convert_fusion.1
  115.7 1.4 convolution_convert_fusion
  117.2 2.1 collective-permute-start
  122.5 8.3 %while.12 = (s32[]{:T(128)}, f32[2,64,128]{2,1,0:T(8,128)S(1)}, f32[6,2,32,128]{3,2,0,1:T(8,128)S(1)}, f32[6,2,64]{2,1,0:T(2,128)S(1)}, f32[6,2,32,64]{3,2,1,0:T...) while((s32[]{:T(128)}, f32[2,64,128]{2,1,0:T(8,128)S(1)}, ...), condition=%wide.region_4.5_spmd, body=%wide.region_3.4_spmd.sunk | while | flops 31531008 | bytes 955549 | solution.py:220
  130.9 3.3 %all-gather = f32[512,64]{1,0:T(8,128)S(1)} all-gather(f32[256,64]{1,0:T(8,128)S(1)} %pad_maximum_fusion), channel_id=2, replica_groups=mesh['sp_0'=8,'sp_1'=8,'sp_2'=2,'tp'=4] {'sp_2'}, dimensions={0}, use_global_device_ids=true | all-gather | bytes 196608 | tf_op jit(solution)/shard_map/all_gather | solution.py:30
  135.1 27.0 %all-gather.1 = f32[2048,64]{1,0:T(8,128)S(1)} all-gather(f32[256,64]{1,0:T(8,128)S(1)} %pad_maximum_fusion.1), channel_id=3, replica_groups=mesh['sp_0'=8,'sp_1'=8,'sp_2'=2,'tp'=4] {'sp_1'}, dimensions={0}, use_global_device_ids=true | all-gather | bytes 589824 | tf_op jit(solution)/shard_map/all_gather | solution.py:30
  166.3 26.7 %all-gather.2 = f32[2048,64]{1,0:T(8,128)S(1)} all-gather(f32[256,64]{1,0:T(8,128)S(1)} %pad_maximum_fusion.2), channel_id=4, replica_groups=mesh['sp_0'=8,'sp_1'=8,'sp_2'=2,'tp'=4] {'sp_0'}, dimensions={0}, use_global_device_ids=true | all-gather | bytes 589824 | tf_op jit(solution)/shard_map/all_gather | solution.py:30
  198.0 4.4 %all-to-all-start.1 = ((f32[4,1,384]{2,1,0:T(1,128)}), f32[4,1,384]{2,1,0:T(1,128)S(1)}, u32[]{:S(2)}, u32[]{:S(2)}) async-start(f32[4,1,384]{2,1,0:T(1,128)} %broadcast_in_dim.28), calls=%async_computation.1 | async-start | bytes 12288 | tf_op jit(solution)/shard_map/all_to_all | solution.py:62
  202.4 5.3 %all-to-all-done.1 = f32[4,1,384]{2,1,0:T(1,128)S(1)} async-done(((f32[4,1,384]{2,1,0:T(1,128)}), f32[4,1,384]{2,1,0:T(1,128)S(1)}, u32[]{:S(2)}, u32[]{:S(2)}) %all-to-all-start.1) | async-done | bytes 6176 | tf_op jit(solution)/shard_map/all_to_all | solution.py:62
  208.0 1.7 fusion.77
  209.9 16.1 %all_to_all.16 = f32[4,192,512]{2,1,0:T(8,128)S(1)} all-to-all(f32[4,192,512]{2,1,0:T(8,128)S(1)} %bitcast.328), channel_id=1, replica_groups=mesh['sp_0'=8,'sp_1'=8,'sp_2'=2,'tp'=4] {'tp'}, dimensions={0} | all-to-all | bytes 3145728 | tf_op jit(solution)/shard_map/all_to_all | solution.py:106
  (241 shorter events, 32.4 us)
Async XLA Ops:
  6.5 94.9 %all-gather.6.cloned.1.call-start = ((), (), s32[]{:S(2)}) async-start(), calls=%async_computation.3 | async-start | bytes 4227072 | tf_op jit(solution)/shard_map/all_gather | solution.py:92
  14.6 16.7 %all-to-all-start = ((bf16[4,192,512]{2,1,0:T(8,128)(2,1)}), bf16[4,192,512]{2,1,0:T(8,128)(2,1)S(1)}, u32[]{:S(2)}, u32[]{:S(2)}) async-start(bf16[4,192,512]{2,1,0:T(8,128)(2,1)} %broadcast_in_dim.27), calls=%async_computation | async-start | bytes 1572864 | tf_op jit(solution)/shard_map/all_to_all | solution.py:62
  19.0 189.0 %all-gather.8.cloned.1.call-start = ((), (), s32[]{:S(2)}) async-start(), calls=%async_computation.4 | async-start | bytes 1056768 | tf_op jit(solution)/shard_map/all_gather | solution.py:325
  32.2 78.4 %copy-start = (f32[192,128]{1,0:T(8,128)S(1)}, f32[192,128]{1,0:T(8,128)}, u32[]{:S(2)}) copy-start(f32[192,128]{1,0:T(8,128)} %param.35) | copy-start | bytes 294916
  32.2 78.4 %copy-start.33 = (f32[128]{0:T(128)S(1)}, f32[128]{0:T(128)}, u32[]{:S(2)}) copy-start(f32[128]{0:T(128)} %param.32) | copy-start | bytes 1540
  32.2 78.4 %copy-start.34 = (f32[128]{0:T(128)S(1)}, f32[128]{0:T(128)}, u32[]{:S(2)}) copy-start(f32[128]{0:T(128)} %param.33) | copy-start | bytes 1540
  32.2 78.4 %copy-start.35 = (f32[128]{0:T(128)S(1)}, f32[128]{0:T(128)}, u32[]{:S(2)}) copy-start(f32[128]{0:T(128)} %param.31) | copy-start | bytes 1540
  32.2 78.4 %copy-start.36 = (f32[128]{0:T(128)S(1)}, f32[128]{0:T(128)}, u32[]{:S(2)}) copy-start(f32[128]{0:T(128)} %param.34) | copy-start | bytes 1540
  117.2 79.3 %collective-permute-start = (bf16[30,128]{1,0:T(8,128)(2,1)S(1)}, bf16[30,128]{1,0:T(8,128)(2,1)S(1)}, u32[]{:S(2)}, u32[]{:S(2)}) collective-permute-start(bf16[30,128]{1,0:T(8,128)(2,1)S(1)} %slice.584), channel_id=1, source_target_pairs={{0,4},{4,8},{8,12},{12,16},{16,20},{20,24},{24,28},{28,32},{32,36}... | collective-permute-start | bytes 23048 | tf_op jit(solution)/shard_map/ppermute | solution.py:57
  166.0 30.5 %copy-start.4 = (f32[128]{0:T(128)S(1)}, f32[128]{0:T(128)}, u32[]{:S(2)}) copy-start(f32[128]{0:T(128)} %get-tuple-element.195) | copy-start | bytes 1540
  166.0 30.5 %copy-start.5 = (f32[128]{0:T(128)S(1)}, f32[128]{0:T(128)}, u32[]{:S(2)}) copy-start(f32[128]{0:T(128)} %get-tuple-element.196) | copy-start | bytes 1540
  166.0 30.5 %copy-start.6 = (f32[128]{0:T(128)S(1)}, f32[128]{0:T(128)}, u32[]{:S(2)}) copy-start(f32[128]{0:T(128)} %get-tuple-element.197) | copy-start | bytes 1540
  166.0 30.5 %copy-start.7 = (f32[128]{0:T(128)S(1)}, f32[128]{0:T(128)}, u32[]{:S(2)}) copy-start(f32[128]{0:T(128)} %get-tuple-element.198) | copy-start | bytes 1540
  166.0 30.5 %copy-start.8 = (f32[128]{0:T(128)S(1)}, f32[128]{0:T(128)}, u32[]{:S(2)}) copy-start(f32[128]{0:T(128)} %get-tuple-element.199) | copy-start | bytes 1540
  166.1 30.5 %copy-start.9 = (f32[128]{0:T(128)S(1)}, f32[128]{0:T(128)}, u32[]{:S(2)}) copy-start(f32[128]{0:T(128)} %get-tuple-element.200) | copy-start | bytes 1540
  166.1 30.5 %copy-start.10 = (f32[128]{0:T(128)S(1)}, f32[128]{0:T(128)}, u32[]{:S(2)}) copy-start(f32[128]{0:T(128)} %get-tuple-element.201) | copy-start | bytes 1540
  166.1 30.5 %copy-start.11 = (f32[128]{0:T(128)S(1)}, f32[128]{0:T(128)}, u32[]{:S(2)}) copy-start(f32[128]{0:T(128)} %get-tuple-element.202) | copy-start | bytes 1540
  166.1 30.5 %copy-start.12 = (f32[128]{0:T(128)S(1)}, f32[128]{0:T(128)}, u32[]{:S(2)}) copy-start(f32[128]{0:T(128)} %get-tuple-element.172) | copy-start | bytes 1540
  166.1 30.5 %copy-start.13 = (f32[128]{0:T(128)S(1)}, f32[128]{0:T(128)}, u32[]{:S(2)}) copy-start(f32[128]{0:T(128)} %get-tuple-element.173) | copy-start | bytes 1540
  166.1 30.5 %copy-start.14 = (f32[128]{0:T(128)S(1)}, f32[128]{0:T(128)}, u32[]{:S(2)}) copy-start(f32[128]{0:T(128)} %get-tuple-element.174) | copy-start | bytes 1540
  166.1 30.5 %copy-start.15 = (f32[128]{0:T(128)S(1)}, f32[128]{0:T(128)}, u32[]{:S(2)}) copy-start(f32[128]{0:T(128)} %get-tuple-element.175) | copy-start | bytes 1540
  166.1 30.5 %copy-start.16 = (f32[128]{0:T(128)S(1)}, f32[128]{0:T(128)}, u32[]{:S(2)}) copy-start(f32[128]{0:T(128)} %get-tuple-element.176) | copy-start | bytes 1540
  166.1 30.5 %copy-start.17 = (f32[128]{0:T(128)S(1)}, f32[128]{0:T(128)}, u32[]{:S(2)}) copy-start(f32[128]{0:T(128)} %get-tuple-element.177) | copy-start | bytes 1540
  198.0 9.7 %all-to-all-start.1 = ((f32[4,1,384]{2,1,0:T(1,128)}), f32[4,1,384]{2,1,0:T(1,128)S(1)}, u32[]{:S(2)}, u32[]{:S(2)}) async-start(f32[4,1,384]{2,1,0:T(1,128)} %broadcast_in_dim.28), calls=%async_computation.1 | async-start | bytes 12288 | tf_op jit(solution)/shard_map/all_to_all | solution.py:62
  (19 other events, 476.2 us)
Sparse Core Ops, SparseCore 0:
  12.8 88.5 all-gather.5
  104.5 75.6 all-gather.7
where the time goes:
time: 235 us; the launch traced here: 234 us
  waiting for transfers between devices  82.1 us (35%)
  blocking collectives  73.1 us (31%)
  matrix products  33.3 us (14%)
  between operations  14.8 us (6%)
  local copies, waits for them, and re-layouts  14.6 us (6%)
  starting transfers between devices  10.9 us (5%)
  other arithmetic  4.55 us (2%)
    all_gather x1, waiting for transfers between devices, side_by_side(): lax.all_gather(both, axis, axis=dim, tiled=True)  69.2 us
    all_gather x3, blocking collectives, collected_together(): both, at, found = (lax.all_gather(jnp.concatenate(lines), axis), 0, {})  57 us
    all_to_all x1, blocking collectives, sent_and_summed(): pieces = lax.all_to_all(split_up(x, dim, size), axis, 0, 0, tiled=True)  16.1 us
    all_to_all x2, waiting for transfers between devices, copy_for_each(): lax.all_to_all(jnp.broadcast_to(x[None], (size, *x.shape)), axis, 0, 0, t...  12.8 us
    dot_general x8, matrix products, fold_rows(): jnp.dot(normed, piece, preferred_element_type=jnp.float32)  11.9 us
    all_to_all x2, starting transfers between devices, copy_for_each(): lax.all_to_all(jnp.broadcast_to(x[None], (size, *x.shape)), axis, 0, 0, t...  8.81 us
    unnamed x83, local copies, waits for them, and re-layouts  5.63 us
  transfers between devices with their start and end apart: 5, of which 3 were waited for; matrix products, arithmetic and copies ran while one was open for 19% of the time, Pallas kernels for 0%

commit v1 on v0

v1 whole, which is shorter than its diff:
```python
import functools

import jax
import jax.numpy as jnp
from jax import lax
from jax.experimental import pallas as pl
from jax.experimental.pallas import tpu as pltpu
from jax.sharding import PartitionSpec as P

HEAD = 64
TAPS = 31
BLOCK = 32
LENGTH = 192
BLOCKS = LENGTH // BLOCK
MATS = 8
F32 = jnp.float32
BF16 = jnp.bfloat16

NN = (((1,), (0,)), ((), ()))
NT = (((1,), (1,)), ((), ()))
TN = (((0,), (0,)), ((), ()))


def place(z, y, c):
    return z * 16 + y * 2 + c


ALONG_Y = [[[place(z, y, c) for y in range(8)] for z in range(8)] for c in range(2)]
ALONG_Z = [[[place(z, y, c) for z in range(8)] for y in range(8)] for c in range(2)]
FIRST_AXIS = ALONG_Y[0] + ALONG_Z[1]
SECOND_AXIS = ALONG_Z[0] + ALONG_Y[1]
Y_AXIS = ALONG_Y[0] + ALONG_Y[1]
Z_AXIS = ALONG_Z[0] + ALONG_Z[1]
SWAP = [(i, i ^ 1) for i in range(128)]
ONWARD = [(i, i + 1) for i in range(127)]


def split(x):
    high = x.astype(BF16)
    return high, (x - high.astype(F32)).astype(BF16)


def dot3(a, b, dims=NN):
    a_high, a_low = split(a)
    b_high, b_low = split(b)
    one = functools.partial(lax.dot_general, dimension_numbers=dims, preferred_element_type=F32)
    return one(a_high, b_high) + (one(a_high, b_low) + one(a_low, b_high))


def exact(a, b, dims=NN):
    return lax.dot_general(
        a, b, dims, precision=lax.Precision.HIGHEST, preferred_element_type=F32
    )


def iota(shape, dim):
    return lax.broadcasted_iota(jnp.int32, shape, dim)


def pack_kernel(*refs):
    out = refs[-1]
    blocks = [ref[...] for ref in refs[:MATS]]
    blocks += [ref[...].astype(F32).T.astype(BF16) for ref in refs[MATS:-1]]
    both = jnp.concatenate(blocks, axis=0)
    for k in range(8):
        out[k] = both


def pack(mats, outs):
    rows = 16 * (len(mats) + len(outs))
    return pl.pallas_call(
        pack_kernel, out_shape=jax.ShapeDtypeStruct((8, rows, 128), BF16), name="pack"
    )(*mats, *outs)


def fill_rows(core, own, other, store):
    for a in range(8):
        for b in range(8):
            straight = (a * 16 + b * 2) * 16
            turned = (b * 16 + a * 2) * 16 + 16
            mine = jnp.where(core == 0, straight, turned)
            theirs = jnp.where(core == 0, turned, straight)
            store(pl.multiple_of(mine, 16), own, a, b)
            store(pl.multiple_of(theirs, 16), other, a, b)


def local_kernel(
    core_ref,
    own_ref,
    other_ref,
    tokens_ref,
    norm_gain_ref,
    key_gain_ref,
    removal_gain_ref,
    removal_bias_ref,
    decay_bias_ref,
    extra_ref,
    norm_out_ref,
    state_ref,
    reads_ref,
    gate_ref,
    conv_ref,
    weights,
    normed,
):
    core = core_ref[0]

    def store(row, source, a, b):
        for m in range(MATS):
            lanes = slice((m % 2) * 128, (m % 2) * 128 + 128)
            weights[m // 2, pl.ds(row, 16), lanes] = source[a, b, m * 16 : m * 16 + 16, :]

    fill_rows(core, own_ref, other_ref, store)
    parts = [tokens_ref[j].astype(F32) for j in range(4)]
    total = sum(jnp.sum(part * part, axis=-1, keepdims=True) for part in parts)
    inverse_rms = lax.rsqrt(total * (1.0 / 2048.0) + 1e-06)
    for j in range(4):
        normed[:, j * 512 : j * 512 + 512] = (
            parts[j] * inverse_rms * norm_gain_ref[j : j + 1, :]
        ).astype(BF16)
    products = []
    for p in range(4):
        product = jnp.dot(normed[...], weights[p], preferred_element_type=F32)
        product = product.astype(BF16).astype(F32)
        products += [product[:, :128], product[:, 128:]]
    recept, keys, values, decay_pre, removal_pre, gate_pre, conv_value, conv_gate = products
    gate_ref[...] = norm_out_ref[...] * jax.nn.sigmoid(gate_pre)
    conv_ref[...] = (conv_value * jax.nn.sigmoid(conv_gate)).astype(BF16)

    rate = 0.6065306597126334 * jax.nn.sigmoid(decay_bias_ref[...] + decay_pre) + extra_ref[...]
    removal = jax.nn.sigmoid(removal_bias_ref[...] + removal_pre)
    lane = iota((LENGTH, 128), 1)
    first = lane < HEAD
    scaled = keys * key_gain_ref[...]
    square = scaled * scaled
    low = jnp.sum(jnp.where(first, square, 0.0), axis=-1, keepdims=True)
    high = jnp.sum(jnp.where(first, 0.0, square), axis=-1, keepdims=True)
    unit = scaled * lax.rsqrt(jnp.where(first, low, high) + 1e-06)
    written = keys * (1.0 + (removal - 1.0) * removal_gain_ref[...])

    row, column = iota((LENGTH, LENGTH), 0), iota((LENGTH, LENGTH), 1)
    same = (row // BLOCK) == (column // BLOCK)
    strict = same & (row > column)
    inclusive = same & (row >= column)
    falling = -exact(inclusive.astype(F32), rate)
    before = falling + rate
    by_block = falling.reshape(BLOCKS, BLOCK, 128)
    middle = jnp.broadcast_to(
        by_block[:, BLOCK // 2 : BLOCK // 2 + 1], (BLOCKS, BLOCK, 128)
    ).reshape(LENGTH, 128)
    ending = jnp.broadcast_to(by_block[:, BLOCK - 1 :], (BLOCKS, BLOCK, 128)).reshape(LENGTH, 128)
    beta = unit * removal
    rising = jnp.exp(middle - falling)
    alpha_mid = -unit * jnp.exp(before - middle)
    recept_mid = recept * jnp.exp(falling - middle)
    right = jnp.concatenate([beta * rising, written * rising], axis=0)
    start_alpha = -unit * jnp.exp(before)
    start_recept = recept * jnp.exp(falling)
    closing = jnp.exp(ending - falling)
    end_beta = beta * closing
    end_keys = written * closing
    kept = jnp.exp(by_block[:, BLOCK - 1, :])
    turned_values = pltpu.roll(values, HEAD, 1)

    square_row, square_lane = iota((128, 128), 0), iota((128, 128), 1)
    diagonal = square_row == square_lane
    for h in range(2):
        mine = first if h == 0 else jnp.logical_not(first)
        mine_row = (square_row < HEAD) if h == 0 else (square_row >= HEAD)
        left = jnp.concatenate(
            [jnp.where(mine, alpha_mid, 0.0), jnp.where(mine, recept_mid, 0.0)], axis=0
        )
        pairs = dot3(left, right, NT)
        power = jnp.where(strict, pairs[:LENGTH, :LENGTH], 0.0)
        alpha_keys = jnp.where(strict, pairs[:LENGTH, LENGTH:], 0.0)
        recept_beta = jnp.where(inclusive, pairs[LENGTH:, :LENGTH], 0.0)
        recept_keys = jnp.where(inclusive, pairs[LENGTH:, LENGTH:], 0.0)
        value_rows = jnp.where(mine, 0.0, turned_values)
        solved = jnp.where(mine, start_alpha, dot3(alpha_keys, value_rows))
        for step in range(5):
            solved = solved + dot3(power, solved)
            if step < 4:
                power = dot3(power, power)
        query = jnp.where(mine, start_recept, 0.0) + dot3(
            jnp.concatenate([recept_beta, recept_keys], axis=1),
            jnp.concatenate([solved, value_rows], axis=0),
        )
        steps = []
        for b in range(BLOCKS):
            rows = slice(b * BLOCK, b * BLOCK + BLOCK)
            moved = dot3(
                jnp.concatenate([end_beta[rows], end_keys[rows]], axis=0),
                jnp.concatenate([solved[rows], value_rows[rows]], axis=0),
                TN,
            )
            held = jnp.where(diagonal, jnp.broadcast_to(kept[b : b + 1], (128, 128)), 0.0)
            whole = jnp.where(diagonal, 1.0, 0.0)
            steps.append(jnp.where(mine_row, moved + held, whole))
        one = dot3(steps[1], steps[0])
        two = dot3(steps[3], steps[2])
        three = dot3(steps[5], steps[4])
        four = dot3(two, one)
        prefixes = [None, steps[0], one, dot3(steps[2], one), four, dot3(steps[4], four)]
        final = dot3(three, four)[h * HEAD : h * HEAD + HEAD]
        if h == 1:
            final = pltpu.roll(final, HEAD, 1)
        state_ref[h] = final
        reads_ref[h, 0:BLOCK, :] = query[0:BLOCK]
        for b in range(1, BLOCKS):
            rows = slice(b * BLOCK, b * BLOCK + BLOCK)
            reads_ref[h, rows, :] = dot3(query[rows], prefixes[b])


def local_part(core, own, other, tokens, norm_gain, vectors, extra, norm_out):
    block = pl.BlockSpec((8, 8, MATS * 16, 128), lambda i: (0, 0, 0, 0))
    whole = lambda shape: pl.BlockSpec(shape, lambda i: (0,) * len(shape))
    operands = (tokens, norm_gain, *vectors, extra, norm_out)
    shapes = (
        jax.ShapeDtypeStruct((2, HEAD, 128), F32),
        jax.ShapeDtypeStruct((2, LENGTH, 128), F32),
        jax.ShapeDtypeStruct((LENGTH, 128), F32),
        jax.ShapeDtypeStruct((LENGTH, 128), BF16),
    )
    return pl.pallas_call(
        local_kernel,
        grid=(1,),
        in_specs=[pl.BlockSpec(memory_space=pltpu.SMEM), block, block]
        + [whole(x.shape) for x in operands],
        out_specs=tuple(whole(x.shape) for x in shapes),
        out_shape=shapes,
        scratch_shapes=[pltpu.VMEM((4, 2048, 256), BF16), pltpu.VMEM((LENGTH, 2048), BF16)],
        name="local",
    )(core, own, other, *operands)


def after(later, earlier):
    product = exact(later[:, :HEAD], earlier)
    return product + jnp.where(iota((HEAD, 128), 1) < HEAD, 0.0, later)


def chained(steps):
    while len(steps) > 1:
        steps = [after(steps[k + 1], steps[k]) for k in range(0, len(steps), 2)]
    return steps[0]


def nothing():
    return jnp.where(iota((HEAD, 128), 0) == iota((HEAD, 128), 1), 1.0, 0.0)


def chip_kernel(core_ref, mine_ref, theirs_ref, out_ref):
    core = core_ref[0]
    mine, theirs = mine_ref[...], theirs_ref[...]
    earlier = jnp.where(core == 0, mine, theirs)
    later = jnp.where(core == 0, theirs, mine)
    out_ref[...] = jnp.broadcast_to(after(later, earlier)[None], (8, HEAD, 128))


def row_kernel(place_ref, steps_ref, before_ref, total_ref):
    here = place_ref[0]
    steps = [steps_ref[k] for k in range(8)]
    total_ref[...] = jnp.broadcast_to(chained(steps)[None], (8, HEAD, 128))
    before_ref[...] = chained([jnp.where(k < here, steps[k], nothing()) for k in range(8)])


def incoming_kernel(place_ref, steps_ref, before_ref, mine_ref, theirs_ref, own_ref, sent_ref):
    here, core = place_ref[0], place_ref[1]
    steps = [steps_ref[k] for k in range(8)]
    start = chained([jnp.where(k < here, steps[k], nothing()) for k in range(8)])
    at_chip = after(before_ref[...], start)
    earlier = jnp.where(core == 0, mine_ref[...], theirs_ref[...])
    at_second = after(earlier, at_chip)
    own_ref[...] = jnp.where(core == 0, at_chip, at_second)
    sent_ref[...] = jnp.where(core == 0, at_second, at_chip)


def on_core(kernel, shapes, scalars, *operands, name):
    return pl.pallas_call(
        kernel,
        in_specs=[pl.BlockSpec(memory_space=pltpu.SMEM)]
        + [pl.BlockSpec(x.shape, lambda n=x.ndim: (0,) * n) for x in operands],
        out_shape=shapes,
        name=name,
    )(scalars, *operands)


def conv_kernel(input_ref, rim_ref, taps_ref, bias_ref, filtered_ref, sums_ref):
    padded = jnp.concatenate([rim_ref[...], input_ref[...]], axis=0).astype(F32)
    filtered = jnp.broadcast_to(bias_ref[...], (LENGTH, 128))
    for k in range(TAPS):
        filtered = filtered + taps_ref[k : k + 1, :] * padded[k + 2 : k + 2 + LENGTH]
    filtered_ref[...] = filtered
    ones = jnp.ones((8, 128), F32)
    sums_ref[0:8, :] = exact(ones, filtered, NT)
    sums_ref[8:16, :] = exact(ones, filtered * filtered, NT)


def columns_kernel(core_ref, own_ref, other_ref, out_ref):
    def store(row, source, a, b):
        for m in range(2):
            out_ref[pl.ds(row, 16), m * 128 : m * 128 + 128] = source[a, b, m * 16 : m * 16 + 16, :]

    fill_rows(core_ref[0], own_ref, other_ref, store)


def output_columns(core, own, other):
    block = pl.BlockSpec((8, 8, 32, 128), lambda i: (0, 0, MATS // 2, 0))
    return pl.pallas_call(
        columns_kernel,
        grid=(1,),
        in_specs=[pl.BlockSpec(memory_space=pltpu.SMEM), block, block],
        out_specs=pl.BlockSpec((2048, 256), lambda i: (0, 0)),
        out_shape=jax.ShapeDtypeStruct((2048, 256), BF16),
        name="columns",
    )(core, own, other)


def final_kernel(
    core_ref,
    reads_ref,
    mine_ref,
    theirs_ref,
    gate_ref,
    filtered_ref,
    sums_ref,
    conv_gain_ref,
    columns_ref,
    out_ref,
):
    core = core_ref[0]
    mine, theirs = mine_ref[...], theirs_ref[...]
    head0 = jnp.where(core == 0, mine, theirs)
    head1 = jnp.where(core == 0, theirs, mine)
    lane = iota((HEAD, 128), 1)
    equal = iota((HEAD, 128), 0)
    zero = jnp.zeros((HEAD, 128), F32)
    right0 = jnp.concatenate(
        [
            jnp.where(lane < HEAD, pltpu.roll(head0, HEAD, 1), zero),
            jnp.where(lane == equal, 1.0, 0.0),
        ],
        axis=0,
    )
    right1 = jnp.concatenate(
        [jnp.where(lane == equal + HEAD, 1.0, 0.0), jnp.where(lane < HEAD, zero, head1)], axis=0
    )
    reads = exact(reads_ref[0], right0) + exact(reads_ref[1], right1)
    first = iota((LENGTH, 128), 1) < HEAD

    def head_mean(x):
        low = jnp.sum(jnp.where(first, x, 0.0), axis=-1, keepdims=True)
        high = jnp.sum(jnp.where(first, 0.0, x), axis=-1, keepdims=True)
        return jnp.where(first, low, high) * (1.0 / HEAD)

    centered = reads - head_mean(reads)
    spread = head_mean(centered * centered)
    scan_out = (centered * lax.rsqrt(spread + 0.00064) * gate_ref[...]).astype(BF16)

    eighth = jnp.full((8, 128), 0.125 / 512.0, F32)
    center = exact(sums_ref[0:8, :], eighth, TN)
    second = exact(sums_ref[8:16, :], eighth, TN)
    scaled = (
        (filtered_ref[...] - center)
        * lax.rsqrt(second - center * center + 1e-05)
        * conv_gain_ref[...]
    )
    conv_out = (scaled * jax.nn.sigmoid(scaled)).astype(BF16)
    features = jnp.concatenate([scan_out, conv_out], axis=1)
    for j in range(4):
        out_ref[j] = lax.dot_general(
            features, columns_ref[j * 512 : j * 512 + 512, :], NT, preferred_element_type=F32
        ).astype(BF16)


def to_each(x, groups):
    return lax.all_to_all(x, "sp", 0, 0, tiled=True, axis_index_groups=groups)


def shards(
    tokens,
    norm_gain,
    query_weight,
    key_weight,
    value_weight,
    decay_weight,
    removal_weight,
    gate_weight,
    key_gain,
    removal_gain,
    removal_bias,
    decay_bias,
    decay_extra,
    scan_norm_gain,
    conv_value_weight,
    conv_gate_weight,
    conv_taps,
    conv_bias,
    conv_norm_gain,
    out_scan_weight,
    out_conv_weight,
):
    index = lax.axis_index("sp")
    core = (index % 2).astype(jnp.int32)
    core1 = core[None]
    z, y = index // 16, (index // 2) % 8
    row = lambda v: v.reshape(1, -1)

    packed = pack(
        (
            query_weight,
            key_weight,
            value_weight,
            decay_weight,
            removal_weight,
            gate_weight,
            conv_value_weight,
            conv_gate_weight,
        ),
        (out_scan_weight, out_conv_weight),
    )
    stage1 = to_each(packed, FIRST_AXIS)
    stage2 = to_each(jnp.broadcast_to(stage1[None], (8, *stage1.shape)), SECOND_AXIS)
    whole = lax.all_gather(tokens, "tp")
    swapped = lax.ppermute(stage2, "sp", SWAP)

    state, reads, gate, conv_input = local_part(
        core1,
        stage2,
        swapped,
        whole,
        norm_gain.reshape(4, 512),
        (row(key_gain), row(removal_gain), row(removal_bias), row(decay_bias)),
        decay_extra,
        row(scan_norm_gain),
    )

    mine = jnp.where(core == 0, state[0], state[1])
    theirs = lax.ppermute(jnp.where(core == 0, state[1], state[0]), "sp", SWAP)
    rim = lax.ppermute(conv_input[LENGTH - 32 :], "sp", ONWARD)
    table = jax.ShapeDtypeStruct((8, HEAD, 128), F32)
    step = jax.ShapeDtypeStruct((HEAD, 128), F32)
    chip = on_core(chip_kernel, table, core1, mine, theirs, name="chip")
    before, total = on_core(
        row_kernel, (step, table), y.astype(jnp.int32)[None], to_each(chip, Y_AXIS), name="row"
    )
    own_state, sent_state = on_core(
        incoming_kernel,
        (step, step),
        jnp.stack([z, core]).astype(jnp.int32),
        to_each(total, Z_AXIS),
        before,
        mine,
        theirs,
        name="incoming",
    )
    other_state = lax.ppermute(sent_state, "sp", SWAP)

    filtered, sums = pl.pallas_call(
        conv_kernel,
        out_shape=(
            jax.ShapeDtypeStruct((LENGTH, 128), F32),
            jax.ShapeDtypeStruct((16, LENGTH), F32),
        ),
        name="conv",
    )(conv_input, rim, conv_taps, row(conv_bias))
    sums = lax.psum(sums, "tp")
    columns = output_columns(core1, stage2, swapped)

    terms = on_core(
        final_kernel,
        jax.ShapeDtypeStruct((4, LENGTH, 512), BF16),
        core1,
        reads,
        own_state,
        other_state,
        gate,
        filtered,
        sums,
        row(conv_norm_gain),
        columns,
        name="final",
    )
    parts = lax.all_to_all(terms, "tp", 0, 0, tiled=True)
    return jnp.sum(parts.astype(F32), axis=0).astype(BF16)


def solution(mesh):
    weights = P("sp", "tp")
    in_specs = (
        (P("sp", "tp"), P())
        + (weights,) * 6
        + (P("tp"),) * 4
        + (P("sp", "tp"), P("tp"), weights, weights, P(None, "tp"), P("tp"), P("tp"))
        + (P("tp", "sp"), P("tp", "sp"))
    )
    return jax.shard_map(
        shards, mesh=mesh, in_specs=in_specs, out_specs=P("sp", "tp"), check_vma=False
    )
```

time: 235 us -> 191 us (0.81)
  the two profiles are of different devices: /device:TPU:24 before, /device:TPU:64 now
where the time goes in v1:
time: 191 us; the launch traced here: 190 us
  blocking collectives  109 us (57%)
  Pallas kernels  28.3 us (15%)
  waiting for transfers between devices  26.1 us (14%)
  starting transfers between devices  16.3 us (9%)
  local copies, waits for them, and re-layouts  7.76 us (4%)
  other arithmetic  2.81 us (1%)
    all_to_all x2, blocking collectives, to_each(): return lax.all_to_all(x, 'sp', 0, 0, tiled=True, axis_index_groups=groups)  62.5 us
    all_to_all x2, waiting for transfers between devices, to_each(): return lax.all_to_all(x, 'sp', 0, 0, tiled=True, axis_index_groups=groups)  22.7 us
    psum x1, blocking collectives, shards(): sums = lax.psum(sums, 'tp')  18.5 us
    all_gather x1, blocking collectives, shards(): whole = lax.all_gather(tokens, 'tp')  15 us
    all_to_all x1, blocking collectives, shards(): parts = lax.all_to_all(terms, 'tp', 0, 0, tiled=True)  12.9 us
    pallas_call x1, Pallas kernels, local_part(): pl.pallas_call(local_kernel, grid=(1,), in_specs=[pl.BlockSpec(memory_spa...  11.6 us
    pallas_call x4, Pallas kernels, on_core(): pl.pallas_call(kernel, in_specs=[pl.BlockSpec(memory_space=pltpu.SMEM)] +...  10.2 us
    all_to_all x2, starting transfers between devices, to_each(): return lax.all_to_all(x, 'sp', 0, 0, tiled=True, axis_index_groups=groups)  8.18 us
  transfers between devices with their start and end apart: 6, of which 4 were waited for; matrix products, arithmetic and copies ran while one was open for 1% of the time, Pallas kernels for 2%

profile of v1, /device:TPU:64, one launch (start us, length us, event | category | flops | bytes accessed | tf_op | source)
XLA Modules:
  0.0 190.2 jit_solution(2906872599291071147)
XLA Ops:
  0.0 1.4 copy.22.refs_8_
  1.4 1.4 copy.23.refs_9_
  2.8 1.7 pack.1
  4.5 18.3 %all_to_all.25 = bf16[8,160,128]{2,1,0:T(8,128)(2,1)S(1)} all-to-all(bf16[8,160,128]{2,1,0:T(8,128)(2,1)} %pack.1), channel_id=1, replica_groups={{0,8,16,24,32,40,48,56},{64,72,80,88,96,104,112,120},{128,136,144,152,1..., dimensions={0} | all-to-all | bytes 655360 | tf_op jit(solution)/shard_map/all_to_all | solution.py:376
  23.2 44.2 %all_to_all.26.own_ref = bf16[8,8,160,128]{3,2,1,0:T(8,128)(2,1)S(1)} all-to-all(bf16[8,8,160,128]{3,2,1,0:T(8,128)(2,1)S(1)} %broadcast_in_dim.13), channel_id=1, replica_groups={{0,64,128,192,256,320,384,448},{8,72,136,200,264,328,392,456},{16,80,14..., dimensions={0} | all-to-all | bytes 5242880 | tf_op jit(solution)/shard_map/all_to_all | solution.py:376
  67.4 1.9 %collective-permute-start = (bf16[8,8,160,128]{3,2,1,0:T(8,128)(2,1)S(1)}, bf16[8,8,160,128]{3,2,1,0:T(8,128)(2,1)}, u32[]{:S(2)}, u32[]{:S(2)}) collective-permute-start(bf16[8,8,160,128]{3,2,1,0:T(8,128)(2,1)S(1)} %all_to_all.26.own_ref), channel_id=1, source_target_pairs={{0,4},{4,0},{8,12},{12,8},{16,20},{20,16},{24,28},{28,24},{32,36},... | collective-permute-start | bytes 7864328 | tf_op jit(solution)/shard_map/ppermute | solution.py:424
  70.0 15.0 %all-gather = bf16[768,512]{1,0:T(8,128)(2,1)} all-gather(bf16[192,512]{1,0:T(8,128)(2,1)S(1)} %copy-done.3), channel_id=2, replica_groups=mesh['sp'=128,'tp'=4] {'tp'}, dimensions={0}, use_global_device_ids=true | all-gather | bytes 983040 | tf_op jit(solution)/shard_map/all_gather | solution.py:423
  85.0 11.6 %local.1 = (f32[2,64,128]{2,1,0:T(8,128)}, f32[2,192,128]{2,1,0:T(8,128)}, f32[192,128]{1,0:T(8,128)}, bf16[192,128]{1,0:T(8,128)(2,1)}) custom-call(s32[1]{0:T(128)} %bitcast.core_ref, bf16[8,8,160,128]{3,2,1,0:T(8,128)(2,1)} %copy-done, bf16[8,8,160,128]{3,2,1,0:T(8,128)(2,1)} %collective-permute-done.other_ref, bf16[4,192,512]{2,1,0:T(8,128)(2,1)} %bitcast.15, ...), custom_call_target="tpu_custom_call" | custom-call | tf_op jit(solution)/shard_map/local/pallas_call | solution.py:224
  98.0 1.9 %collective-permute-start.1 = (f32[64,128]{1,0:T(8,128)S(1)}, f32[64,128]{1,0:T(8,128)S(1)}, u32[]{:S(2)}, u32[]{:S(2)}) collective-permute-start(f32[64,128]{1,0:T(8,128)S(1)} %get-tuple-element.25), channel_id=1, source_target_pairs={{0,4},{4,0},{8,12},{12,8},{16,20},{20,16},{24,28},{28,24},{32,36},... | collective-permute-start | bytes 98312 | tf_op jit(solution)/shard_map/ppermute | solution.py:438
  101.7 1.7 chip.1
  103.3 3.4 %all-to-all-start.2 = ((f32[8,64,128]{2,1,0:T(8,128)}), f32[8,64,128]{2,1,0:T(8,128)S(1)}, u32[]{:S(2)}, u32[]{:S(2)}) async-start(f32[8,64,128]{2,1,0:T(8,128)} %chip.1), calls=%async_computation.2 | async-start | bytes 524288 | tf_op jit(solution)/shard_map/all_to_all | solution.py:376
  106.8 12.4 %all-to-all-done.2.steps_ref = f32[8,64,128]{2,1,0:T(8,128)S(1)} async-done(((f32[8,64,128]{2,1,0:T(8,128)}), f32[8,64,128]{2,1,0:T(8,128)S(1)}, u32[]{:S(2)}, u32[]{:S(2)}) %all-to-all-start.2) | async-done | bytes 262176 | tf_op jit(solution)/shard_map/all_to_all | solution.py:376
  119.8 2.6 %row.1 = (f32[64,128]{1,0:T(8,128)}, f32[8,64,128]{2,1,0:T(8,128)}) custom-call(s32[1]{0:T(128)} %bitcast.8.place_ref, f32[8,64,128]{2,1,0:T(8,128)} %copy-done.1), custom_call_target="tpu_custom_call" | custom-call | tf_op jit(solution)/shard_map/row/pallas_call | solution.py:278
  122.4 4.8 %all-to-all-start.3 = ((f32[8,64,128]{2,1,0:T(8,128)}), f32[8,64,128]{2,1,0:T(8,128)S(1)}, u32[]{:S(2)}, u32[]{:S(2)}) async-start(f32[8,64,128]{2,1,0:T(8,128)} %get-tuple-element.17), calls=%async_computation.3 | async-start | bytes 524288 | tf_op jit(solution)/shard_map/all_to_all | solution.py:376
  127.8 10.3 %all-to-all-done.3.steps_ref = f32[8,64,128]{2,1,0:T(8,128)S(1)} async-done(((f32[8,64,128]{2,1,0:T(8,128)}), f32[8,64,128]{2,1,0:T(8,128)S(1)}, u32[]{:S(2)}, u32[]{:S(2)}) %all-to-all-start.3) | async-done | bytes 262176 | tf_op jit(solution)/shard_map/all_to_all | solution.py:376
  138.8 2.6 %incoming.1 = (f32[64,128]{1,0:T(8,128)}, f32[64,128]{1,0:T(8,128)}) custom-call(s32[2]{0:T(128)} %pad_add_fusion.place_ref, f32[8,64,128]{2,1,0:T(8,128)} %copy-done.2, f32[64,128]{1,0:T(8,128)} %get-tuple-element.18.before_ref, f32[64,128]{1,0:T(8,128)} %get-tuple-element.26.mine_ref, f32[64,128]{1,0:T(8,128)} %copy-done.4), custom_call_target="tpu_custom_call" | custom-call | tf_op jit(solution)/shard_map/incoming/pallas_call | solution.py:278
  141.4 1.9 %collective-permute-start.2 = (f32[64,128]{1,0:T(8,128)}, f32[64,128]{1,0:T(8,128)S(1)}, u32[]{:S(2)}, u32[]{:S(2)}) collective-permute-start(f32[64,128]{1,0:T(8,128)} %get-tuple-element.20), channel_id=1, source_target_pairs={{0,4},{4,0},{8,12},{12,8},{16,20},{20,16},{24,28},{28,24},{32,36},... | collective-permute-start | bytes 98312 | tf_op jit(solution)/shard_map/ppermute | solution.py:456
  144.0 2.4 %collective-permute-start.3 = (bf16[32,128]{1,0:T(8,128)(2,1)S(1)}, bf16[32,128]{1,0:T(8,128)(2,1)S(1)}, u32[]{:S(2)}, u32[]{:S(2)}) collective-permute-start(bf16[32,128]{1,0:T(8,128)(2,1)S(1)} %slice.13), channel_id=1, source_target_pairs={{0,4},{4,8},{8,12},{12,16},{16,20},{20,24},{24,28},{28,32},{32,36}... | collective-permute-start | bytes 24584 | tf_op jit(solution)/shard_map/ppermute | solution.py:439
  146.4 2.5 %columns.1.columns_ref = bf16[2048,256]{1,0:T(8,128)(2,1)} custom-call(s32[1]{0:T(128)} %bitcast.core_ref, bf16[8,8,160,128]{3,2,1,0:T(8,128)(2,1)} %copy-done, bf16[8,8,160,128]{3,2,1,0:T(8,128)(2,1)} %collective-permute-done.other_ref), custom_call_target="tpu_custom_call" | custom-call | tf_op jit(solution)/shard_map/columns/pallas_call | solution.py:308
  148.8 2.2 %collective-permute-done.3.rim_ref = bf16[32,128]{1,0:T(8,128)(2,1)S(1)} collective-permute-done((bf16[32,128]{1,0:T(8,128)(2,1)S(1)}, bf16[32,128]{1,0:T(8,128)(2,1)S(1)}, u32[]{:S(2)}, u32[]{:S(2)}) %collective-permute-start.3) | collective-permute-done | bytes 8224 | tf_op jit(solution)/shard_map/ppermute | solution.py:439
  151.7 2.3 %conv.1 = (f32[192,128]{1,0:T(8,128)}, f32[16,192]{1,0:T(8,128)}) custom-call(bf16[192,128]{1,0:T(8,128)(2,1)} %get-tuple-element.22.input_ref, bf16[32,128]{1,0:T(8,128)(2,1)} %copy-done.6, f32[31,128]{1,0:T(8,128)} %taps_ref.1, f32[1,128]{1,0:T(1,128)} %bitcast.21), custom_call_target="tpu_custom_call" | custom-call | tf_op jit(solution)/shard_map/conv/pallas_call | solution.py:458
  153.9 18.5 %psum.7.sums_ref = f32[16,192]{1,0:T(8,128)} all-reduce(f32[16,192]{1,0:T(8,128)} %get-tuple-element.24), channel_id=1, replica_groups=mesh['sp'=128,'tp'=4] {'tp'}, use_global_device_ids=true, to_apply=%region_0.1 | all-reduce | flops 3072 | bytes 24576 | tf_op jit(solution)/shard_map/psum | solution.py:466
  173.0 3.4 %final.1 = bf16[4,192,512]{2,1,0:T(8,128)(2,1)} custom-call(s32[1]{0:T(128)} %bitcast.core_ref, f32[2,192,128]{2,1,0:T(8,128)} %get-tuple-element.15.reads_ref, f32[64,128]{1,0:T(8,128)} %get-tuple-element.19.mine_ref, f32[64,128]{1,0:T(8,128)} %copy-done.5, f32[192,128]{1,0:T(8,128)} %get-tuple-element.21.gate_ref, ...), custom_call_target="tpu_custom_call" | custom-call | tf_op jit(solution)/shard_map/final/pallas_call | solution.py:278
  176.4 12.9 %all_to_all.27 = bf16[4,192,512]{2,1,0:T(8,128)(2,1)S(1)} all-to-all(bf16[4,192,512]{2,1,0:T(8,128)(2,1)} %final.1), channel_id=1, replica_groups=mesh['sp'=128,'tp'=4] {'tp'}, dimensions={0} | all-to-all | bytes 1572864 | tf_op jit(solution)/shard_map/all_to_all | solution.py:483
  (25 shorter events, 9.0 us)
Async XLA Ops:
  23.2 46.2 %copy-start.7 = (f32[2048]{0:T(1024)S(1)}, f32[2048]{0:T(1024)}, u32[]{:S(2)}) copy-start(f32[2048]{0:T(1024)} %param.22) | copy-start | bytes 24580
  23.2 46.8 %copy-start.3 = (bf16[192,512]{1,0:T(8,128)(2,1)S(1)}, bf16[192,512]{1,0:T(8,128)(2,1)}, u32[]{:S(2)}) copy-start(bf16[192,512]{1,0:T(8,128)(2,1)} %param.21) | copy-start | bytes 589828
  67.4 17.5 %copy-start = (bf16[8,8,160,128]{3,2,1,0:T(8,128)(2,1)}, bf16[8,8,160,128]{3,2,1,0:T(8,128)(2,1)S(1)}, u32[]{:S(2)}) copy-start(bf16[8,8,160,128]{3,2,1,0:T(8,128)(2,1)S(1)} %all_to_all.26.own_ref) | copy-start | bytes 7864324
  67.4 17.5 %collective-permute-start = (bf16[8,8,160,128]{3,2,1,0:T(8,128)(2,1)S(1)}, bf16[8,8,160,128]{3,2,1,0:T(8,128)(2,1)}, u32[]{:S(2)}, u32[]{:S(2)}) collective-permute-start(bf16[8,8,160,128]{3,2,1,0:T(8,128)(2,1)S(1)} %all_to_all.26.own_ref), channel_id=1, source_target_pairs={{0,4},{4,0},{8,12},{12,8},{16,20},{20,16},{24,28},{28,24},{32,36},... | collective-permute-start | bytes 7864328 | tf_op jit(solution)/shard_map/ppermute | solution.py:424
  98.0 3.1 %collective-permute-start.1 = (f32[64,128]{1,0:T(8,128)S(1)}, f32[64,128]{1,0:T(8,128)S(1)}, u32[]{:S(2)}, u32[]{:S(2)}) collective-permute-start(f32[64,128]{1,0:T(8,128)S(1)} %get-tuple-element.25), channel_id=1, source_target_pairs={{0,4},{4,0},{8,12},{12,8},{16,20},{20,16},{24,28},{28,24},{32,36},... | collective-permute-start | bytes 98312 | tf_op jit(solution)/shard_map/ppermute | solution.py:438
  101.0 0.6 copy-start.4
  103.3 15.8 %all-to-all-start.2 = ((f32[8,64,128]{2,1,0:T(8,128)}), f32[8,64,128]{2,1,0:T(8,128)S(1)}, u32[]{:S(2)}, u32[]{:S(2)}) async-start(f32[8,64,128]{2,1,0:T(8,128)} %chip.1), calls=%async_computation.2 | async-start | bytes 524288 | tf_op jit(solution)/shard_map/all_to_all | solution.py:376
  119.1 0.7 copy-start.1
  122.4 15.7 %all-to-all-start.3 = ((f32[8,64,128]{2,1,0:T(8,128)}), f32[8,64,128]{2,1,0:T(8,128)S(1)}, u32[]{:S(2)}, u32[]{:S(2)}) async-start(f32[8,64,128]{2,1,0:T(8,128)} %get-tuple-element.17), calls=%async_computation.3 | async-start | bytes 524288 | tf_op jit(solution)/shard_map/all_to_all | solution.py:376
  138.1 0.7 copy-start.2
  141.4 31.0 %collective-permute-start.2 = (f32[64,128]{1,0:T(8,128)}, f32[64,128]{1,0:T(8,128)S(1)}, u32[]{:S(2)}, u32[]{:S(2)}) collective-permute-start(f32[64,128]{1,0:T(8,128)} %get-tuple-element.20), channel_id=1, source_target_pairs={{0,4},{4,0},{8,12},{12,8},{16,20},{20,16},{24,28},{28,24},{32,36},... | collective-permute-start | bytes 98312 | tf_op jit(solution)/shard_map/ppermute | solution.py:456
  144.0 7.1 %collective-permute-start.3 = (bf16[32,128]{1,0:T(8,128)(2,1)S(1)}, bf16[32,128]{1,0:T(8,128)(2,1)S(1)}, u32[]{:S(2)}, u32[]{:S(2)}) collective-permute-start(bf16[32,128]{1,0:T(8,128)(2,1)S(1)} %slice.13), channel_id=1, source_target_pairs={{0,4},{4,8},{8,12},{12,16},{16,20},{20,24},{24,28},{28,32},{32,36}... | collective-permute-start | bytes 24584 | tf_op jit(solution)/shard_map/ppermute | solution.py:439
  151.1 0.6 copy-start.6
  172.4 0.6 copy-start.5

commit v2 on v1

--- a/solution.py
+++ b/solution.py
@@ -25,12 +25,28 @@
     return z * 16 + y * 2 + c
 
 
-ALONG_Y = [[[place(z, y, c) for y in range(8)] for z in range(8)] for c in range(2)]
-ALONG_Z = [[[place(z, y, c) for z in range(8)] for y in range(8)] for c in range(2)]
-FIRST_AXIS = ALONG_Y[0] + ALONG_Z[1]
-SECOND_AXIS = ALONG_Z[0] + ALONG_Y[1]
-Y_AXIS = ALONG_Y[0] + ALONG_Y[1]
-Z_AXIS = ALONG_Z[0] + ALONG_Z[1]
+def near(k, parity, c):
+    return (2 * k + parity + (2 if c == 1 and parity == 0 else 0)) % 8
+
+
+FAR = [
+    [place(z + 2 * i, y + 2 * j, c) for i in range(4) for j in range(4)]
+    for c in range(2)
+    for z in range(2)
+    for y in range(2)
+]
+NEAR = [
+    [
+        place(near(k, p, c), near(l, q, c), c)
+        for p in range(2)
+        for q in range(2)
+    ]
+    for c in range(2)
+    for k in range(4)
+    for l in range(4)
+]
+Y_AXIS = [[place(z, y, c) for y in range(8)] for z in range(8) for c in range(2)]
+Z_AXIS = [[place(z, y, c) for z in range(8)] for y in range(8) for c in range(2)]
 SWAP = [(i, i ^ 1) for i in range(128)]
 ONWARD = [(i, i + 1) for i in range(127)]
 
@@ -59,29 +75,27 @@
 
 def pack_kernel(*refs):
     out = refs[-1]
-    blocks = [ref[...] for ref in refs[:MATS]]
-    blocks += [ref[...].astype(F32).T.astype(BF16) for ref in refs[MATS:-1]]
+    blocks = [ref[...] for ref in refs[:-1]]
     both = jnp.concatenate(blocks, axis=0)
-    for k in range(8):
+    for k in range(16):
         out[k] = both
 
 
-def pack(mats, outs):
-    rows = 16 * (len(mats) + len(outs))
+def pack(*mats):
     return pl.pallas_call(
-        pack_kernel, out_shape=jax.ShapeDtypeStruct((8, rows, 128), BF16), name="pack"
-    )(*mats, *outs)
+        pack_kernel,
+        out_shape=jax.ShapeDtypeStruct((16, 16 * len(mats), 128), BF16),
+        name="pack",
+    )(*mats)
 
 
 def fill_rows(core, own, other, store):
-    for a in range(8):
-        for b in range(8):
-            straight = (a * 16 + b * 2) * 16
-            turned = (b * 16 + a * 2) * 16 + 16
-            mine = jnp.where(core == 0, straight, turned)
-            theirs = jnp.where(core == 0, turned, straight)
-            store(pl.multiple_of(mine, 16), own, a, b)
-            store(pl.multiple_of(theirs, 16), other, a, b)
+    for a in range(4):
+        for b in range(16):
+            z, y = a // 2 + 2 * (b // 4), a % 2 + 2 * (b % 4)
+            row = (z * 16 + y * 2) * 16
+            store(pl.multiple_of(row + core * 16, 16), own, a, b)
+            store(pl.multiple_of(row + 16 - core * 16, 16), other, a, b)
 
 
 def local_kernel(
@@ -96,7 +110,8 @@
     decay_bias_ref,
     extra_ref,
     norm_out_ref,
-    state_ref,
+    mine_ref,
+    theirs_ref,
     reads_ref,
     gate_ref,
     conv_ref,
@@ -164,6 +179,7 @@
 
     square_row, square_lane = iota((128, 128), 0), iota((128, 128), 1)
     diagonal = square_row == square_lane
+    finals = []
     for h in range(2):
         mine = first if h == 0 else jnp.logical_not(first)
         mine_row = (square_row < HEAD) if h == 0 else (square_row >= HEAD)
@@ -204,19 +220,22 @@
         final = dot3(three, four)[h * HEAD : h * HEAD + HEAD]
         if h == 1:
             final = pltpu.roll(final, HEAD, 1)
-        state_ref[h] = final
+        finals.append(final)
         reads_ref[h, 0:BLOCK, :] = query[0:BLOCK]
         for b in range(1, BLOCKS):
             rows = slice(b * BLOCK, b * BLOCK + BLOCK)
             reads_ref[h, rows, :] = dot3(query[rows], prefixes[b])
+    mine_ref[...] = jnp.where(core == 0, finals[0], finals[1])
+    theirs_ref[...] = jnp.where(core == 0, finals[1], finals[0])
 
 
 def local_part(core, own, other, tokens, norm_gain, vectors, extra, norm_out):
-    block = pl.BlockSpec((8, 8, MATS * 16, 128), lambda i: (0, 0, 0, 0))
+    block = pl.BlockSpec((4, 16, MATS * 16, 128), lambda i: (0, 0, 0, 0))
     whole = lambda shape: pl.BlockSpec(shape, lambda i: (0,) * len(shape))
     operands = (tokens, norm_gain, *vectors, extra, norm_out)
     shapes = (
-        jax.ShapeDtypeStruct((2, HEAD, 128), F32),
+        jax.ShapeDtypeStruct((HEAD, 128), F32),
+        jax.ShapeDtypeStruct((HEAD, 128), F32),
         jax.ShapeDtypeStruct((2, LENGTH, 128), F32),
         jax.ShapeDtypeStruct((LENGTH, 128), F32),
         jax.ShapeDtypeStruct((LENGTH, 128), BF16),
@@ -234,7 +253,7 @@
 
 
 def after(later, earlier):
-    product = exact(later[:, :HEAD], earlier)
+    product = dot3(later[:, :HEAD], earlier)
     return product + jnp.where(iota((HEAD, 128), 1) < HEAD, 0.0, later)
 
 
@@ -246,6 +265,14 @@
 
 def nothing():
     return jnp.where(iota((HEAD, 128), 0) == iota((HEAD, 128), 1), 1.0, 0.0)
+
+
+def sent(step):
+    return jnp.broadcast_to((step - nothing()).astype(BF16)[None], (8, HEAD, 128))
+
+
+def received(steps_ref):
+    return [steps_ref[k].astype(F32) + nothing() for k in range(8)]
 
 
 def chip_kernel(core_ref, mine_ref, theirs_ref, out_ref):
@@ -253,19 +280,19 @@
     mine, theirs = mine_ref[...], theirs_ref[...]
     earlier = jnp.where(core == 0, mine, theirs)
     later = jnp.where(core == 0, theirs, mine)
-    out_ref[...] = jnp.broadcast_to(after(later, earlier)[None], (8, HEAD, 128))
+    out_ref[...] = sent(after(later, earlier))
 
 
 def row_kernel(place_ref, steps_ref, before_ref, total_ref):
     here = place_ref[0]
-    steps = [steps_ref[k] for k in range(8)]
-    total_ref[...] = jnp.broadcast_to(chained(steps)[None], (8, HEAD, 128))
+    steps = received(steps_ref)
+    total_ref[...] = sent(chained(steps))
     before_ref[...] = chained([jnp.where(k < here, steps[k], nothing()) for k in range(8)])
 
 
 def incoming_kernel(place_ref, steps_ref, before_ref, mine_ref, theirs_ref, own_ref, sent_ref):
     here, core = place_ref[0], place_ref[1]
-    steps = [steps_ref[k] for k in range(8)]
+    steps = received(steps_ref)
     start = chained([jnp.where(k < here, steps[k], nothing()) for k in range(8)])
     at_chip = after(before_ref[...], start)
     earlier = jnp.where(core == 0, mine_ref[...], theirs_ref[...])
@@ -274,13 +301,12 @@
     sent_ref[...] = jnp.where(core == 0, at_second, at_chip)
 
 
-def on_core(kernel, shapes, scalars, *operands, name):
+def on_core(kernel, shapes, scalars, *operands):
     return pl.pallas_call(
         kernel,
         in_specs=[pl.BlockSpec(memory_space=pltpu.SMEM)]
         + [pl.BlockSpec(x.shape, lambda n=x.ndim: (0,) * n) for x in operands],
         out_shape=shapes,
-        name=name,
     )(scalars, *operands)
 
 
@@ -304,7 +330,7 @@
 
 
 def output_columns(core, own, other):
-    block = pl.BlockSpec((8, 8, 32, 128), lambda i: (0, 0, MATS // 2, 0))
+    block = pl.BlockSpec((4, 16, 32, 128), lambda i: (0, 0, MATS // 2, 0))
     return pl.pallas_call(
         columns_kernel,
         grid=(1,),
@@ -376,7 +402,7 @@
     return lax.all_to_all(x, "sp", 0, 0, tiled=True, axis_index_groups=groups)
 
 
-def shards(
+def layer(
     tokens,
     norm_gain,
     query_weight,
@@ -406,24 +432,24 @@
     row = lambda v: v.reshape(1, -1)
 
     packed = pack(
-        (
-            query_weight,
-            key_weight,
-            value_weight,
-            decay_weight,
-            removal_weight,
-            gate_weight,
-            conv_value_weight,
-            conv_gate_weight,
-        ),
-        (out_scan_weight, out_conv_weight),
-    )
-    stage1 = to_each(packed, FIRST_AXIS)
-    stage2 = to_each(jnp.broadcast_to(stage1[None], (8, *stage1.shape)), SECOND_AXIS)
+        query_weight,
+        key_weight,
+        value_weight,
+        decay_weight,
+        removal_weight,
+        gate_weight,
+        conv_value_weight,
+        conv_gate_weight,
+        out_scan_weight.T,
+        out_conv_weight.T,
+    )
+    stage1 = to_each(packed, FAR)
+    wide = jnp.broadcast_to(stage1[None], (4, *stage1.shape))
+    stage2 = to_each(wide, NEAR)
     whole = lax.all_gather(tokens, "tp")
     swapped = lax.ppermute(stage2, "sp", SWAP)
 
-    state, reads, gate, conv_input = local_part(
+    mine, theirs, reads, gate, conv_input = local_part(
         core1,
         stage2,
         swapped,
@@ -434,24 +460,22 @@
         row(scan_norm_gain),
     )
 
-    mine = jnp.where(core == 0, state[0], state[1])
-    theirs = lax.ppermute(jnp.where(core == 0, state[1], state[0]), "sp", SWAP)
+    theirs = lax.ppermute(theirs, "sp", SWAP)
     rim = lax.ppermute(conv_input[LENGTH - 32 :], "sp", ONWARD)
-    table = jax.ShapeDtypeStruct((8, HEAD, 128), F32)
+    table = jax.ShapeDtypeStruct((8, HEAD, 128), BF16)
     step = jax.ShapeDtypeStruct((HEAD, 128), F32)
-    chip = on_core(chip_kernel, table, core1, mine, theirs, name="chip")
-    before, total = on_core(
-        row_kernel, (step, table), y.astype(jnp.int32)[None], to_each(chip, Y_AXIS), name="row"
-    )
+    chip = on_core(chip_kernel, table, core1, mine, theirs)
+    chips = to_each(chip, Y_AXIS)
+    before, total = on_core(row_kernel, (step, table), y.astype(jnp.int32)[None], chips)
+    totals = to_each(total, Z_AXIS)
     own_state, sent_state = on_core(
         incoming_kernel,
         (step, step),
         jnp.stack([z, core]).astype(jnp.int32),
-        to_each(total, Z_AXIS),
+        totals,
         before,
         mine,
         theirs,
-        name="incoming",
     )
     other_state = lax.ppermute(sent_state, "sp", SWAP)
 
@@ -478,7 +502,6 @@
         sums,
         row(conv_norm_gain),
         columns,
-        name="final",
     )
     parts = lax.all_to_all(terms, "tp", 0, 0, tiled=True)
     return jnp.sum(parts.astype(F32), axis=0).astype(BF16)
@@ -494,5 +517,5 @@
         + (P("tp", "sp"), P("tp", "sp"))
     )
     return jax.shard_map(
-        shards, mesh=mesh, in_specs=in_specs, out_specs=P("sp", "tp"), check_vma=False
-    )
+        layer, mesh=mesh, in_specs=in_specs, out_specs=P("sp", "tp"), check_vma=False
+    )

time: 191 us -> 178 us (0.932)
  waiting for transfers between devices: 26.1 us -> 20 us
  blocking collectives: 109 us -> 105 us
  local copies, waits for them, and re-layouts: 7.76 us -> 4.89 us
    all_to_all x2, waiting for transfers between devices: 22.7 us -> 16.4 us  [to_each(): return lax.all_to_all(x, 'sp', 0, 0, tiled=True, axis_index_groups=groups)]
    all_to_all x2, blocking collectives: 62.5 us -> 59 us  [to_each(): return lax.all_to_all(x, 'sp', 0, 0, tiled=True, axis_index_groups=groups)]
    unnamed x18 -> x16, local copies, waits for them, and re-layouts: 6.04 us -> 3.17 us
  transfers between devices with their start and end apart: 6 -> 6, of which waited for: 4 -> 4; matrix products, arithmetic and copies ran while one was open for 1% -> 1% of each run, Pallas kernels for 2% -> 3%
where the time goes in v2:
time: 178 us; the launch traced here: 177 us
  blocking collectives  105 us (59%)
  Pallas kernels  27.8 us (16%)
  waiting for transfers between devices  20 us (11%)
  starting transfers between devices  17.7 us (10%)
  local copies, waits for them, and re-layouts  4.89 us (3%)
    all_to_all x2, blocking collectives, to_each(): return lax.all_to_all(x, 'sp', 0, 0, tiled=True, axis_index_groups=groups)  59 us
    psum x1, blocking collectives, layer(): sums = lax.psum(sums, 'tp')  18.6 us
    all_to_all x2, waiting for transfers between devices, to_each(): return lax.all_to_all(x, 'sp', 0, 0, tiled=True, axis_index_groups=groups)  16.4 us
    all_gather x1, blocking collectives, layer(): whole = lax.all_gather(tokens, 'tp')  15 us
    all_to_all x1, blocking collectives, layer(): parts = lax.all_to_all(terms, 'tp', 0, 0, tiled=True)  12.9 us
    pallas_call x1, Pallas kernels, local_part(): pl.pallas_call(local_kernel, grid=(1,), in_specs=[pl.BlockSpec(memory_spa...  11.6 us
    pallas_call x4, Pallas kernels, on_core(): pl.pallas_call(kernel, in_specs=[pl.BlockSpec(memory_space=pltpu.SMEM)] +...  9.72 us
    all_to_all x2, starting transfers between devices, to_each(): return lax.all_to_all(x, 'sp', 0, 0, tiled=True, axis_index_groups=groups)  9.53 us
  transfers between devices with their start and end apart: 6, of which 4 were waited for; matrix products, arithmetic and copies ran while one was open for 1% of the time, Pallas kernels for 3%

profile of v2, /device:TPU:64, one launch (start us, length us, event | category | flops | bytes accessed | tf_op | source)
XLA Modules:
  0.0 177.4 jit_solution(3740643444510429895)
XLA Ops:
  0.0 1.8 pack.1
  1.8 38.3 %all_to_all.25 = bf16[16,160,128]{2,1,0:T(8,128)(2,1)S(1)} all-to-all(bf16[16,160,128]{2,1,0:T(8,128)(2,1)} %pack.1), channel_id=1, replica_groups={{0,16,32,48,128,144,160,176,256,272,288,304,384,400,416,432},{8,24,40,5..., dimensions={0} | all-to-all | bytes 1310720 | tf_op jit(solution)/shard_map/all_to_all | solution.py:402
  40.5 20.7 %all_to_all.26.own_ref = bf16[4,16,160,128]{3,2,1,0:T(8,128)(2,1)S(1)} all-to-all(bf16[4,16,160,128]{3,2,1,0:T(8,128)(2,1)S(1)} %broadcast_in_dim.13), channel_id=1, replica_groups={{0,8,64,72},{16,24,80,88},{32,40,96,104},{48,56,112,120},{128,136,192,2..., dimensions={0} | all-to-all | bytes 5242880 | tf_op jit(solution)/shard_map/all_to_all | solution.py:402
  61.2 1.9 %collective-permute-start = (bf16[4,16,160,128]{3,2,1,0:T(8,128)(2,1)S(1)}, bf16[4,16,160,128]{3,2,1,0:T(8,128)(2,1)}, u32[]{:S(2)}, u32[]{:S(2)}) collective-permute-start(bf16[4,16,160,128]{3,2,1,0:T(8,128)(2,1)S(1)} %all_to_all.26.own_ref), channel_id=1, source_target_pairs={{0,4},{4,0},{8,12},{12,8},{16,20},{20,16},{24,28},{28,24},{32,36},... | collective-permute-start | bytes 7864328 | tf_op jit(solution)/shard_map/ppermute | solution.py:450
  63.8 15.0 %all-gather = bf16[768,512]{1,0:T(8,128)(2,1)} all-gather(bf16[192,512]{1,0:T(8,128)(2,1)S(1)} %copy-done.3), channel_id=2, replica_groups=mesh['sp'=128,'tp'=4] {'tp'}, dimensions={0}, use_global_device_ids=true | all-gather | bytes 983040 | tf_op jit(solution)/shard_map/all_gather | solution.py:449
  78.8 11.6 %local.1 = (f32[64,128]{1,0:T(8,128)}, f32[64,128]{1,0:T(8,128)}, f32[2,192,128]{2,1,0:T(8,128)}, f32[192,128]{1,0:T(8,128)}, bf16[192,128]{1,0:T(8,128)(2,1)}) custom-call(s32[1]{0:T(128)} %bitcast.core_ref, bf16[4,16,160,128]{3,2,1,0:T(8,128)(2,1)} %copy-done, bf16[4,16,160,128]{3,2,1,0:T(8,128)(2,1)} %collective-permute-done.other_ref, ...), custom_call_target="tpu_custom_call" | custom-call | tf_op jit(solution)/shard_map/local/pallas_call | solution.py:243
  90.4 1.9 %collective-permute-start.1 = (f32[64,128]{1,0:T(8,128)}, f32[64,128]{1,0:T(8,128)S(1)}, u32[]{:S(2)}, u32[]{:S(2)}) collective-permute-start(f32[64,128]{1,0:T(8,128)} %get-tuple-element.18), channel_id=1, source_target_pairs={{0,4},{4,0},{8,12},{12,8},{16,20},{20,16},{24,28},{28,24},{32,36},... | collective-permute-start | bytes 98312 | tf_op jit(solution)/shard_map/ppermute | solution.py:463
  92.3 1.4 collective-permute-done.1.theirs_ref
  94.3 1.6 shard_map.199
  95.9 4.3 %all-to-all-start.2 = ((bf16[8,64,128]{2,1,0:T(8,128)(2,1)}), bf16[8,64,128]{2,1,0:T(8,128)(2,1)S(1)}, u32[]{:S(2)}, u32[]{:S(2)}) async-start(bf16[8,64,128]{2,1,0:T(8,128)(2,1)} %shard_map.199), calls=%async_computation.2 | async-start | bytes 262144 | tf_op jit(solution)/shard_map/all_to_all | solution.py:402
  100.1 9.4 %all-to-all-done.2.steps_ref = bf16[8,64,128]{2,1,0:T(8,128)(2,1)S(1)} async-done(((bf16[8,64,128]{2,1,0:T(8,128)(2,1)}), bf16[8,64,128]{2,1,0:T(8,128)(2,1)S(1)}, u32[]{:S(2)}, u32[]{:S(2)}) %all-to-all-start.2) | async-done | bytes 131104 | tf_op jit(solution)/shard_map/all_to_all | solution.py:402
  110.2 2.3 %shard_map.200 = (f32[64,128]{1,0:T(8,128)}, bf16[8,64,128]{2,1,0:T(8,128)(2,1)}) custom-call(s32[1]{0:T(128)} %bitcast.10.place_ref, bf16[8,64,128]{2,1,0:T(8,128)(2,1)} %copy-done.2), custom_call_target="tpu_custom_call" | custom-call | tf_op jit(solution)/shard_map/pallas_call | solution.py:305
  112.5 5.2 %all-to-all-start.3 = ((bf16[8,64,128]{2,1,0:T(8,128)(2,1)}), bf16[8,64,128]{2,1,0:T(8,128)(2,1)S(1)}, u32[]{:S(2)}, u32[]{:S(2)}) async-start(bf16[8,64,128]{2,1,0:T(8,128)(2,1)} %get-tuple-element.19), calls=%async_computation.3 | async-start | bytes 262144 | tf_op jit(solution)/shard_map/all_to_all | solution.py:402
  118.5 7.0 %all-to-all-done.3.steps_ref = bf16[8,64,128]{2,1,0:T(8,128)(2,1)S(1)} async-done(((bf16[8,64,128]{2,1,0:T(8,128)(2,1)}), bf16[8,64,128]{2,1,0:T(8,128)(2,1)S(1)}, u32[]{:S(2)}, u32[]{:S(2)}) %all-to-all-start.3) | async-done | bytes 131104 | tf_op jit(solution)/shard_map/all_to_all | solution.py:402
  126.1 2.3 %shard_map.201 = (f32[64,128]{1,0:T(8,128)}, f32[64,128]{1,0:T(8,128)}) custom-call(s32[2]{0:T(128)} %pad_add_fusion.place_ref, bf16[8,64,128]{2,1,0:T(8,128)(2,1)} %copy-done.1, f32[64,128]{1,0:T(8,128)} %get-tuple-element.20.before_ref, f32[64,128]{1,0:T(8,128)} %get-tuple-element.17.mine_ref, f32[64,128]{1,0:T(8,128)} %copy-done.4), custom_call_target="tpu_custom_call" | custom-call | tf_op jit(solution)/shard_map/pallas_call | solution.py:305
  128.4 1.9 %collective-permute-start.2 = (f32[64,128]{1,0:T(8,128)}, f32[64,128]{1,0:T(8,128)S(1)}, u32[]{:S(2)}, u32[]{:S(2)}) collective-permute-start(f32[64,128]{1,0:T(8,128)} %get-tuple-element.22), channel_id=1, source_target_pairs={{0,4},{4,0},{8,12},{12,8},{16,20},{20,16},{24,28},{28,24},{32,36},... | collective-permute-start | bytes 98312 | tf_op jit(solution)/shard_map/ppermute | solution.py:480
  131.0 2.4 %collective-permute-start.3 = (bf16[32,128]{1,0:T(8,128)(2,1)S(1)}, bf16[32,128]{1,0:T(8,128)(2,1)S(1)}, u32[]{:S(2)}, u32[]{:S(2)}) collective-permute-start(bf16[32,128]{1,0:T(8,128)(2,1)S(1)} %slice.3), channel_id=1, source_target_pairs={{0,4},{4,8},{8,12},{12,16},{16,20},{20,24},{24,28},{28,32},{32,36}... | collective-permute-start | bytes 24584 | tf_op jit(solution)/shard_map/ppermute | solution.py:464
  133.4 2.4 %columns.1.columns_ref = bf16[2048,256]{1,0:T(8,128)(2,1)} custom-call(s32[1]{0:T(128)} %bitcast.core_ref, bf16[4,16,160,128]{3,2,1,0:T(8,128)(2,1)} %copy-done, bf16[4,16,160,128]{3,2,1,0:T(8,128)(2,1)} %collective-permute-done.other_ref), custom_call_target="tpu_custom_call" | custom-call | tf_op jit(solution)/shard_map/columns/pallas_call | solution.py:334
  135.9 2.2 %collective-permute-done.3.rim_ref = bf16[32,128]{1,0:T(8,128)(2,1)S(1)} collective-permute-done((bf16[32,128]{1,0:T(8,128)(2,1)S(1)}, bf16[32,128]{1,0:T(8,128)(2,1)S(1)}, u32[]{:S(2)}, u32[]{:S(2)}) %collective-permute-start.3) | collective-permute-done | bytes 8224 | tf_op jit(solution)/shard_map/ppermute | solution.py:464
  138.7 2.3 %conv.1 = (f32[192,128]{1,0:T(8,128)}, f32[16,192]{1,0:T(8,128)}) custom-call(bf16[192,128]{1,0:T(8,128)(2,1)} %get-tuple-element.24.input_ref, bf16[32,128]{1,0:T(8,128)(2,1)} %copy-done.6, f32[31,128]{1,0:T(8,128)} %taps_ref.1, f32[1,128]{1,0:T(1,128)} %bitcast.21), custom_call_target="tpu_custom_call" | custom-call | tf_op jit(solution)/shard_map/conv/pallas_call | solution.py:482
  141.0 18.6 %psum.7.sums_ref = f32[16,192]{1,0:T(8,128)} all-reduce(f32[16,192]{1,0:T(8,128)} %get-tuple-element.26), channel_id=1, replica_groups=mesh['sp'=128,'tp'=4] {'tp'}, use_global_device_ids=true, to_apply=%region_0.1 | all-reduce | flops 3072 | bytes 24576 | tf_op jit(solution)/shard_map/psum | solution.py:490
  160.1 3.5 %shard_map.202 = bf16[4,192,512]{2,1,0:T(8,128)(2,1)} custom-call(s32[1]{0:T(128)} %bitcast.core_ref, f32[2,192,128]{2,1,0:T(8,128)} %get-tuple-element.16.reads_ref, f32[64,128]{1,0:T(8,128)} %get-tuple-element.21.mine_ref, f32[64,128]{1,0:T(8,128)} %copy-done.5, f32[192,128]{1,0:T(8,128)} %get-tuple-element.23.gate_ref, ...), custom_call_target="tpu_custom_call" | custom-call | tf_op jit(solution)/shard_map/pallas_call | solution.py:305
  163.6 12.9 %all_to_all.27 = bf16[4,192,512]{2,1,0:T(8,128)(2,1)S(1)} all-to-all(bf16[4,192,512]{2,1,0:T(8,128)(2,1)} %shard_map.202), channel_id=1, replica_groups=mesh['sp'=128,'tp'=4] {'tp'}, dimensions={0} | all-to-all | bytes 1572864 | tf_op jit(solution)/shard_map/all_to_all | solution.py:506
  176.5 0.8 reduce_sum.12
  (22 shorter events, 5.6 us)
Async XLA Ops:
  40.5 22.7 %copy-start.7 = (f32[2048]{0:T(1024)S(1)}, f32[2048]{0:T(1024)}, u32[]{:S(2)}) copy-start(f32[2048]{0:T(1024)} %param.22) | copy-start | bytes 24580
  40.5 23.3 %copy-start.3 = (bf16[192,512]{1,0:T(8,128)(2,1)S(1)}, bf16[192,512]{1,0:T(8,128)(2,1)}, u32[]{:S(2)}) copy-start(bf16[192,512]{1,0:T(8,128)(2,1)} %param.21) | copy-start | bytes 589828
  61.2 17.5 %copy-start = (bf16[4,16,160,128]{3,2,1,0:T(8,128)(2,1)}, bf16[4,16,160,128]{3,2,1,0:T(8,128)(2,1)S(1)}, u32[]{:S(2)}) copy-start(bf16[4,16,160,128]{3,2,1,0:T(8,128)(2,1)S(1)} %all_to_all.26.own_ref) | copy-start | bytes 7864324
  61.2 17.5 %collective-permute-start = (bf16[4,16,160,128]{3,2,1,0:T(8,128)(2,1)S(1)}, bf16[4,16,160,128]{3,2,1,0:T(8,128)(2,1)}, u32[]{:S(2)}, u32[]{:S(2)}) collective-permute-start(bf16[4,16,160,128]{3,2,1,0:T(8,128)(2,1)S(1)} %all_to_all.26.own_ref), channel_id=1, source_target_pairs={{0,4},{4,0},{8,12},{12,8},{16,20},{20,16},{24,28},{28,24},{32,36},... | collective-permute-start | bytes 7864328 | tf_op jit(solution)/shard_map/ppermute | solution.py:450
  90.4 3.3 %collective-permute-start.1 = (f32[64,128]{1,0:T(8,128)}, f32[64,128]{1,0:T(8,128)S(1)}, u32[]{:S(2)}, u32[]{:S(2)}) collective-permute-start(f32[64,128]{1,0:T(8,128)} %get-tuple-element.18), channel_id=1, source_target_pairs={{0,4},{4,0},{8,12},{12,8},{16,20},{20,16},{24,28},{28,24},{32,36},... | collective-permute-start | bytes 98312 | tf_op jit(solution)/shard_map/ppermute | solution.py:463
  93.7 0.6 copy-start.4
  95.9 13.7 %all-to-all-start.2 = ((bf16[8,64,128]{2,1,0:T(8,128)(2,1)}), bf16[8,64,128]{2,1,0:T(8,128)(2,1)S(1)}, u32[]{:S(2)}, u32[]{:S(2)}) async-start(bf16[8,64,128]{2,1,0:T(8,128)(2,1)} %shard_map.199), calls=%async_computation.2 | async-start | bytes 262144 | tf_op jit(solution)/shard_map/all_to_all | solution.py:402
  109.5 0.7 copy-start.2
  112.5 12.9 %all-to-all-start.3 = ((bf16[8,64,128]{2,1,0:T(8,128)(2,1)}), bf16[8,64,128]{2,1,0:T(8,128)(2,1)S(1)}, u32[]{:S(2)}, u32[]{:S(2)}) async-start(bf16[8,64,128]{2,1,0:T(8,128)(2,1)} %get-tuple-element.19), calls=%async_computation.3 | async-start | bytes 262144 | tf_op jit(solution)/shard_map/all_to_all | solution.py:402
  125.4 0.7 copy-start.1
  128.4 31.1 %collective-permute-start.2 = (f32[64,128]{1,0:T(8,128)}, f32[64,128]{1,0:T(8,128)S(1)}, u32[]{:S(2)}, u32[]{:S(2)}) collective-permute-start(f32[64,128]{1,0:T(8,128)} %get-tuple-element.22), channel_id=1, source_target_pairs={{0,4},{4,0},{8,12},{12,8},{16,20},{20,16},{24,28},{28,24},{32,36},... | collective-permute-start | bytes 98312 | tf_op jit(solution)/shard_map/ppermute | solution.py:480
  131.0 7.1 %collective-permute-start.3 = (bf16[32,128]{1,0:T(8,128)(2,1)S(1)}, bf16[32,128]{1,0:T(8,128)(2,1)S(1)}, u32[]{:S(2)}, u32[]{:S(2)}) collective-permute-start(bf16[32,128]{1,0:T(8,128)(2,1)S(1)} %slice.3), channel_id=1, source_target_pairs={{0,4},{4,8},{8,12},{12,16},{16,20},{20,24},{24,28},{28,32},{32,36}... | collective-permute-start | bytes 24584 | tf_op jit(solution)/shard_map/ppermute | solution.py:464
  138.1 0.6 copy-start.6
  159.5 0.6 copy-start.5

commit v3 on v2

--- a/solution.py
+++ b/solution.py
@@ -25,22 +25,22 @@
     return z * 16 + y * 2 + c
 
 
-def near(k, parity, c):
-    return (2 * k + parity + (2 if c == 1 and parity == 0 else 0)) % 8
-
-
+SETS = (((0, 2, 5, 7), (1, 3, 4, 6)), ((1, 3, 6, 0), (2, 4, 5, 7)))
 FAR = [
-    [place(z + 2 * i, y + 2 * j, c) for i in range(4) for j in range(4)]
+    [place(z, y, c) for z in SETS[c][p] for y in SETS[c][q]]
     for c in range(2)
-    for z in range(2)
-    for y in range(2)
+    for p in range(2)
+    for q in range(2)
 ]
+
+
+def near(k, p, c):
+    pair = ((2 * k + c) % 8, (2 * k + c + 1) % 8)
+    return [chip for chip in pair if chip in SETS[c][p]][0]
+
+
 NEAR = [
-    [
-        place(near(k, p, c), near(l, q, c), c)
-        for p in range(2)
-        for q in range(2)
-    ]
+    [place(near(k, p, c), near(l, q, c), c) for p in range(2) for q in range(2)]
     for c in range(2)
     for k in range(4)
     for l in range(4)
@@ -73,6 +73,21 @@
     return lax.broadcasted_iota(jnp.int32, shape, dim)
 
 
+def vmem(shape, dtype):
+    return pltpu.VMEM(shape, dtype)
+
+
+def on_core(kernel, shapes, index, *operands, given=(), scratch=(), limit=8):
+    return pl.pallas_call(
+        kernel,
+        in_specs=[pl.BlockSpec(memory_space=pltpu.SMEM)]
+        + [pl.BlockSpec(memory_space=pltpu.VMEM)] * (len(operands) + len(given)),
+        out_shape=shapes,
+        scratch_shapes=scratch,
+        compiler_params=pltpu.CompilerParams(vmem_limit_bytes=limit * 1024 * 1024),
+    )(index, *(pltpu.with_memory_space_constraint(x, pltpu.VMEM) for x in operands), *given)
+
+
 def pack_kernel(*refs):
     out = refs[-1]
     blocks = [ref[...] for ref in refs[:-1]]
@@ -92,10 +107,11 @@
 def fill_rows(core, own, other, store):
     for a in range(4):
         for b in range(16):
-            z, y = a // 2 + 2 * (b // 4), a % 2 + 2 * (b % 4)
-            row = (z * 16 + y * 2) * 16
-            store(pl.multiple_of(row + core * 16, 16), own, a, b)
-            store(pl.multiple_of(row + 16 - core * 16, 16), other, a, b)
+            row0, row1 = (
+                place(SETS[c][a // 2][b // 4], SETS[c][a % 2][b % 4], c) * 16 for c in range(2)
+            )
+            store(pl.multiple_of(jnp.where(core == 0, row0, row1), 16), own, a, b)
+            store(pl.multiple_of(jnp.where(core == 0, row1, row0), 16), other, a, b)
 
 
 def local_kernel(
@@ -115,10 +131,11 @@
     reads_ref,
     gate_ref,
     conv_ref,
+    rim_ref,
     weights,
     normed,
 ):
-    core = core_ref[0]
+    core = core_ref[0] % 2
 
     def store(row, source, a, b):
         for m in range(MATS):
@@ -140,7 +157,9 @@
         products += [product[:, :128], product[:, 128:]]
     recept, keys, values, decay_pre, removal_pre, gate_pre, conv_value, conv_gate = products
     gate_ref[...] = norm_out_ref[...] * jax.nn.sigmoid(gate_pre)
-    conv_ref[...] = (conv_value * jax.nn.sigmoid(conv_gate)).astype(BF16)
+    conv_input = (conv_value * jax.nn.sigmoid(conv_gate)).astype(BF16)
+    conv_ref[...] = conv_input
+    rim_ref[...] = conv_input[LENGTH - 32 :]
 
     rate = 0.6065306597126334 * jax.nn.sigmoid(decay_bias_ref[...] + decay_pre) + extra_ref[...]
     removal = jax.nn.sigmoid(removal_bias_ref[...] + removal_pre)
@@ -229,27 +248,25 @@
     theirs_ref[...] = jnp.where(core == 0, finals[1], finals[0])
 
 
-def local_part(core, own, other, tokens, norm_gain, vectors, extra, norm_out):
-    block = pl.BlockSpec((4, 16, MATS * 16, 128), lambda i: (0, 0, 0, 0))
-    whole = lambda shape: pl.BlockSpec(shape, lambda i: (0,) * len(shape))
-    operands = (tokens, norm_gain, *vectors, extra, norm_out)
-    shapes = (
-        jax.ShapeDtypeStruct((HEAD, 128), F32),
-        jax.ShapeDtypeStruct((HEAD, 128), F32),
-        jax.ShapeDtypeStruct((2, LENGTH, 128), F32),
-        jax.ShapeDtypeStruct((LENGTH, 128), F32),
-        jax.ShapeDtypeStruct((LENGTH, 128), BF16),
-    )
-    return pl.pallas_call(
+def local_part(index, own, other, tokens, *given):
+    return on_core(
         local_kernel,
-        grid=(1,),
-        in_specs=[pl.BlockSpec(memory_space=pltpu.SMEM), block, block]
-        + [whole(x.shape) for x in operands],
-        out_specs=tuple(whole(x.shape) for x in shapes),
-        out_shape=shapes,
-        scratch_shapes=[pltpu.VMEM((4, 2048, 256), BF16), pltpu.VMEM((LENGTH, 2048), BF16)],
-        name="local",
-    )(core, own, other, *operands)
+        (
+            vmem((HEAD, 128), F32),
+            vmem((HEAD, 128), F32),
+            vmem((2, LENGTH, 128), F32),
+            vmem((LENGTH, 128), F32),
+            vmem((LENGTH, 128), BF16),
+            vmem((32, 128), BF16),
+        ),
+        index,
+        own,
+        other,
+        tokens,
+        given=given,
+        scratch=[pltpu.VMEM((4, 2048, 256), BF16), pltpu.VMEM((LENGTH, 2048), BF16)],
+        limit=28,
+    )
 
 
 def after(later, earlier):
@@ -276,7 +293,7 @@
 
 
 def chip_kernel(core_ref, mine_ref, theirs_ref, out_ref):
-    core = core_ref[0]
+    core = core_ref[0] % 2
     mine, theirs = mine_ref[...], theirs_ref[...]
     earlier = jnp.where(core == 0, mine, theirs)
     later = jnp.where(core == 0, theirs, mine)
@@ -284,14 +301,14 @@
 
 
 def row_kernel(place_ref, steps_ref, before_ref, total_ref):
-    here = place_ref[0]
+    here = (place_ref[0] // 2) % 8
     steps = received(steps_ref)
     total_ref[...] = sent(chained(steps))
     before_ref[...] = chained([jnp.where(k < here, steps[k], nothing()) for k in range(8)])
 
 
 def incoming_kernel(place_ref, steps_ref, before_ref, mine_ref, theirs_ref, own_ref, sent_ref):
-    here, core = place_ref[0], place_ref[1]
+    here, core = place_ref[0] // 16, place_ref[0] % 2
     steps = received(steps_ref)
     start = chained([jnp.where(k < here, steps[k], nothing()) for k in range(8)])
     at_chip = after(before_ref[...], start)
@@ -301,44 +318,28 @@
     sent_ref[...] = jnp.where(core == 0, at_second, at_chip)
 
 
-def on_core(kernel, shapes, scalars, *operands):
-    return pl.pallas_call(
-        kernel,
-        in_specs=[pl.BlockSpec(memory_space=pltpu.SMEM)]
-        + [pl.BlockSpec(x.shape, lambda n=x.ndim: (0,) * n) for x in operands],
-        out_shape=shapes,
-    )(scalars, *operands)
-
-
-def conv_kernel(input_ref, rim_ref, taps_ref, bias_ref, filtered_ref, sums_ref):
+def conv_kernel(place_ref, input_ref, rim_ref, taps_ref, bias_ref, filtered_ref, sums_ref):
     padded = jnp.concatenate([rim_ref[...], input_ref[...]], axis=0).astype(F32)
     filtered = jnp.broadcast_to(bias_ref[...], (LENGTH, 128))
     for k in range(TAPS):
         filtered = filtered + taps_ref[k : k + 1, :] * padded[k + 2 : k + 2 + LENGTH]
     filtered_ref[...] = filtered
     ones = jnp.ones((8, 128), F32)
-    sums_ref[0:8, :] = exact(ones, filtered, NT)
-    sums_ref[8:16, :] = exact(ones, filtered * filtered, NT)
+    square = filtered * filtered
+    rest = jnp.concatenate([filtered[128:], square[128:]], axis=0)
+    at = iota((8, 128), 0)
+    sums = jnp.where(at == 0, exact(ones, filtered[:128], NT), 0.0)
+    sums = jnp.where(at == 1, exact(ones, square[:128], NT), sums)
+    sums_ref[...] = jnp.where(at == 2, exact(ones, rest, NT), sums)
 
 
 def columns_kernel(core_ref, own_ref, other_ref, out_ref):
     def store(row, source, a, b):
         for m in range(2):
-            out_ref[pl.ds(row, 16), m * 128 : m * 128 + 128] = source[a, b, m * 16 : m * 16 + 16, :]
-
-    fill_rows(core_ref[0], own_ref, other_ref, store)
-
-
-def output_columns(core, own, other):
-    block = pl.BlockSpec((4, 16, 32, 128), lambda i: (0, 0, MATS // 2, 0))
-    return pl.pallas_call(
-        columns_kernel,
-        grid=(1,),
-        in_specs=[pl.BlockSpec(memory_space=pltpu.SMEM), block, block],
-        out_specs=pl.BlockSpec((2048, 256), lambda i: (0, 0)),
-        out_shape=jax.ShapeDtypeStruct((2048, 256), BF16),
-        name="columns",
-    )(core, own, other)
+            at = (MATS + m) * 16
+            out_ref[pl.ds(row, 16), m * 128 : m * 128 + 128] = source[a, b, at : at + 16, :]
+
+    fill_rows(core_ref[0] % 2, own_ref, other_ref, store)
 
 
 def final_kernel(
@@ -349,11 +350,11 @@
     gate_ref,
     filtered_ref,
     sums_ref,
+    columns_ref,
     conv_gain_ref,
-    columns_ref,
     out_ref,
 ):
-    core = core_ref[0]
+    core = core_ref[0] % 2
     mine, theirs = mine_ref[...], theirs_ref[...]
     head0 = jnp.where(core == 0, mine, theirs)
     head1 = jnp.where(core == 0, theirs, mine)
@@ -382,9 +383,12 @@
     spread = head_mean(centered * centered)
     scan_out = (centered * lax.rsqrt(spread + 0.00064) * gate_ref[...]).astype(BF16)
 
-    eighth = jnp.full((8, 128), 0.125 / 512.0, F32)
-    center = exact(sums_ref[0:8, :], eighth, TN)
-    second = exact(sums_ref[8:16, :], eighth, TN)
+    def spread_out(k):
+        return exact(sums_ref[...], jnp.where(iota((8, 128), 0) == k, 1.0 / 512.0, 0.0), TN)
+
+    rest = spread_out(2)
+    center = jnp.concatenate([spread_out(0), rest[:64]], axis=0)
+    second = jnp.concatenate([spread_out(1), rest[64:]], axis=0)
     scaled = (
         (filtered_ref[...] - center)
         * lax.rsqrt(second - center * center + 1e-05)
@@ -425,10 +429,7 @@
     out_scan_weight,
     out_conv_weight,
 ):
-    index = lax.axis_index("sp")
-    core = (index % 2).astype(jnp.int32)
-    core1 = core[None]
-    z, y = index // 16, (index // 2) % 8
+    index = lax.axis_index("sp").astype(jnp.int32)[None]
     row = lambda v: v.reshape(1, -1)
 
     packed = pack(
@@ -449,59 +450,56 @@
     whole = lax.all_gather(tokens, "tp")
     swapped = lax.ppermute(stage2, "sp", SWAP)
 
-    mine, theirs, reads, gate, conv_input = local_part(
-        core1,
+    mine, theirs, reads, gate, conv_input, rim = local_part(
+        index,
         stage2,
         swapped,
         whole,
         norm_gain.reshape(4, 512),
-        (row(key_gain), row(removal_gain), row(removal_bias), row(decay_bias)),
+        row(key_gain),
+        row(removal_gain),
+        row(removal_bias),
+        row(decay_bias),
         decay_extra,
         row(scan_norm_gain),
     )
 
     theirs = lax.ppermute(theirs, "sp", SWAP)
-    rim = lax.ppermute(conv_input[LENGTH - 32 :], "sp", ONWARD)
-    table = jax.ShapeDtypeStruct((8, HEAD, 128), BF16)
-    step = jax.ShapeDtypeStruct((HEAD, 128), F32)
-    chip = on_core(chip_kernel, table, core1, mine, theirs)
+    rim = lax.ppermute(rim, "sp", ONWARD)
+    table = vmem((8, HEAD, 128), BF16)
+    step = vmem((HEAD, 128), F32)
+    chip = on_core(chip_kernel, table, index, mine, theirs)
     chips = to_each(chip, Y_AXIS)
-    before, total = on_core(row_kernel, (step, table), y.astype(jnp.int32)[None], chips)
+    before, total = on_core(row_kernel, (step, table), index, chips)
     totals = to_each(total, Z_AXIS)
     own_state, sent_state = on_core(
-        incoming_kernel,
-        (step, step),
-        jnp.stack([z, core]).astype(jnp.int32),
-        totals,
-        before,
-        mine,
-        theirs,
+        incoming_kernel, (step, step), index, totals, before, mine, theirs
     )
     other_state = lax.ppermute(sent_state, "sp", SWAP)
 
-    filtered, sums = pl.pallas_call(
+    filtered, sums = on_core(
         conv_kernel,
-        out_shape=(
-            jax.ShapeDtypeStruct((LENGTH, 128), F32),
-            jax.ShapeDtypeStruct((16, LENGTH), F32),
-        ),
-        name="conv",
-    )(conv_input, rim, conv_taps, row(conv_bias))
+        (vmem((LENGTH, 128), F32), vmem((8, 128), F32)),
+        index,
+        conv_input,
+        rim,
+        given=(conv_taps, row(conv_bias)),
+    )
     sums = lax.psum(sums, "tp")
-    columns = output_columns(core1, stage2, swapped)
+    columns = on_core(columns_kernel, vmem((2048, 256), BF16), index, stage2, swapped)
 
     terms = on_core(
         final_kernel,
-        jax.ShapeDtypeStruct((4, LENGTH, 512), BF16),
-        core1,
+        vmem((4, LENGTH, 512), BF16),
+        index,
         reads,
         own_state,
         other_state,
         gate,
         filtered,
         sums,
-        row(conv_norm_gain),
         columns,
+        given=(row(conv_norm_gain),),
     )
     parts = lax.all_to_all(terms, "tp", 0, 0, tiled=True)
     return jnp.sum(parts.astype(F32), axis=0).astype(BF16)

time: 178 us -> 151 us (0.85)
  the two profiles are of different devices: /device:TPU:64 before, /device:TPU:2 now
where the time goes in v3:
time: 151 us
  blocking collectives  120 us (79%)
  Pallas kernels  17.5 us (12%)
  starting transfers between devices  8.29 us (5%)
  local copies, waits for them, and re-layouts  2.67 us (2%)
    all_to_all x4, blocking collectives, to_each(): return lax.all_to_all(x, 'sp', 0, 0, tiled=True, axis_index_groups=groups)  82.7 us
    pallas_call x7, Pallas kernels, on_core(): pl.pallas_call(kernel, in_specs=[pl.BlockSpec(memory_space=pltpu.SMEM)] +...  15.7 us
    all_to_all x1, blocking collectives, layer(): parts = lax.all_to_all(terms, 'tp', 0, 0, tiled=True)  14.9 us
    all_gather x1, blocking collectives, layer(): whole = lax.all_gather(tokens, 'tp')  14.6 us
    psum x1, blocking collectives, layer(): sums = lax.psum(sums, 'tp')  7.89 us
  transfers between devices with their start and end apart: 4, of which 1 were waited for; matrix products, arithmetic and copies ran while one was open for 0% of the time, Pallas kernels for 2%

profile of v3, /device:TPU:2, one launch (start us, length us, event | category | flops | bytes accessed | tf_op | source)
XLA Modules:
  0.0 150.7 jit_solution(7181651978936772272)
XLA Ops:
  0.0 1.8 %pack.1 = bf16[16,160,128]{2,1,0:T(8,128)(2,1)} custom-call(bf16[16,128]{1,0:T(8,128)(2,1)} %refs_0_.1, bf16[16,128]{1,0:T(8,128)(2,1)} %refs_1_.1, bf16[16,128]{1,0:T(8,128)(2,1)} %refs_2_.1, bf16[16,128]{1,0:T(8,128)(2,1)} %refs_3_.1, bf16[16,128]{1,0:T(8,128)(2,1)} %refs_4_.1, bf16[16,128]{1,0:T(8,128)(2,1)} %refs_5_.1, bf16[16,128]{1,0:T(8,128)(2,1)} %refs_6_.1, ...), custom_call_target="tpu_custom_call" | custom-call | tf_op jit(solution)/shard_map/pack/pallas_call | solution.py:100
  1.8 36.8 %all_to_all.25 = bf16[16,160,128]{2,1,0:T(8,128)(2,1)S(1)} all-to-all(bf16[16,160,128]{2,1,0:T(8,128)(2,1)} %pack.1), channel_id=1, replica_groups={{0,16,40,56,128,144,168,184,320,336,360,376,448,464,488,504},{8,24,32,4..., dimensions={0} | all-to-all | bytes 1310720 | tf_op jit(solution)/shard_map/all_to_all | solution.py:406
  38.6 0.4 broadcast_in_dim.10
  39.1 21.0 %all_to_all.26.own_ref = bf16[4,16,160,128]{3,2,1,0:T(8,128)(2,1)S(1)} all-to-all(bf16[4,16,160,128]{3,2,1,0:T(8,128)(2,1)S(1)} %broadcast_in_dim.10), channel_id=1, replica_groups={{0,8,64,72},{16,24,80,88},{40,32,104,96},{56,48,120,112},{128,136,192,2..., dimensions={0} | all-to-all | bytes 5242880 | tf_op jit(solution)/shard_map/all_to_all | solution.py:406
  60.0 1.9 %collective-permute-start = (bf16[4,16,160,128]{3,2,1,0:T(8,128)(2,1)S(1)}, bf16[4,16,160,128]{3,2,1,0:T(8,128)(2,1)}, u32[]{:S(2)}, u32[]{:S(2)}) collective-permute-start(bf16[4,16,160,128]{3,2,1,0:T(8,128)(2,1)S(1)} %all_to_all.26.own_ref), channel_id=1, source_target_pairs={{0,4},{4,0},{8,12},{12,8},{16,20},{20,16},{24,28},{28,24},{32,36},... | collective-permute-start | bytes 7864328 | tf_op jit(solution)/shard_map/ppermute | solution.py:451
  62.0 14.6 %all-gather = bf16[768,512]{1,0:T(8,128)(2,1)S(1)} all-gather(bf16[192,512]{1,0:T(8,128)(2,1)S(1)} %copy-done.11), channel_id=2, replica_groups=mesh['sp'=128,'tp'=4] {'tp'}, dimensions={0}, use_global_device_ids=true | all-gather | bytes 983040 | tf_op jit(solution)/shard_map/all_gather | solution.py:450
  76.6 10.2 %shard_map.199 = (f32[64,128]{1,0:T(8,128)S(1)}, f32[64,128]{1,0:T(8,128)S(1)}, f32[2,192,128]{2,1,0:T(8,128)S(1)}, f32[192,128]{1,0:T(8,128)S(1)}, bf16[192,128...) custom-call(s32[1]{0:T(128)} %bitcast.core_ref.place_ref, bf16[4,16,160,128]{3,2,1,0:T(8,128)(2,1)S(1)} %all_to_all.26.own_ref, ...), custom_call_target="tpu_custom_call" | custom-call | tf_op jit(solution)/shard_map/pallas_call | solution.py:81
  86.8 1.9 %collective-permute-start.1 = (f32[64,128]{1,0:T(8,128)S(1)}, f32[64,128]{1,0:T(8,128)S(1)}, u32[]{:S(2)}, u32[]{:S(2)}) collective-permute-start(f32[64,128]{1,0:T(8,128)S(1)} %get-tuple-element.19), channel_id=1, source_target_pairs={{0,4},{4,0},{8,12},{12,8},{16,20},{20,16},{24,28},{28,24},{32,36},... | collective-permute-start | bytes 98312 | tf_op jit(solution)/shard_map/ppermute | solution.py:467
  88.8 1.2 collective-permute-done.1.theirs_ref
  89.9 0.1 shard_map.200
  90.1 12.6 %all_to_all.27.steps_ref = bf16[8,64,128]{2,1,0:T(8,128)(2,1)S(1)} all-to-all(bf16[8,64,128]{2,1,0:T(8,128)(2,1)S(1)} %shard_map.200), channel_id=1, replica_groups={{0,8,16,24,32,40,48,56},{4,12,20,28,36,44,52,60},{64,72,80,88,96,104,11..., dimensions={0} | all-to-all | bytes 262144 | tf_op jit(solution)/shard_map/all_to_all | solution.py:406
  102.7 0.8 shard_map.201
  103.5 12.4 %all_to_all.28.steps_ref = bf16[8,64,128]{2,1,0:T(8,128)(2,1)S(1)} all-to-all(bf16[8,64,128]{2,1,0:T(8,128)(2,1)S(1)} %get-tuple-element.20), channel_id=1, replica_groups={{0,64,128,192,256,320,384,448},{4,68,132,196,260,324,388,452},{8,72,136..., dimensions={0} | all-to-all | bytes 262144 | tf_op jit(solution)/shard_map/all_to_all | solution.py:406
  115.8 0.8 shard_map.202
  116.6 1.9 %collective-permute-start.2 = (f32[64,128]{1,0:T(8,128)S(1)}, f32[64,128]{1,0:T(8,128)S(1)}, u32[]{:S(2)}, u32[]{:S(2)}) collective-permute-start(f32[64,128]{1,0:T(8,128)S(1)} %get-tuple-element.23), channel_id=1, source_target_pairs={{0,4},{4,0},{8,12},{12,8},{16,20},{20,16},{24,28},{28,24},{32,36},... | collective-permute-start | bytes 98312 | tf_op jit(solution)/shard_map/ppermute | solution.py:478
  118.6 2.5 %collective-permute-start.3 = (bf16[32,128]{1,0:T(8,128)(2,1)S(1)}, bf16[32,128]{1,0:T(8,128)(2,1)S(1)}, u32[]{:S(2)}, u32[]{:S(2)}) collective-permute-start(bf16[32,128]{1,0:T(8,128)(2,1)S(1)} %get-tuple-element.26), channel_id=1, source_target_pairs={{0,4},{4,8},{8,12},{12,16},{16,20},{20,24},{24,28},{28,32},{32,36}... | collective-permute-start | bytes 24584 | tf_op jit(solution)/shard_map/ppermute | solution.py:468
  121.1 2.0 %shard_map.204.columns_ref = bf16[2048,256]{1,0:T(8,128)(2,1)S(1)} custom-call(s32[1]{0:T(128)} %bitcast.core_ref.place_ref, bf16[4,16,160,128]{3,2,1,0:T(8,128)(2,1)S(1)} %all_to_all.26.own_ref, bf16[4,16,160,128]{3,2,1,0:T(8,128)(2,1)} %collective-permute-done.other_ref), custom_call_target="tpu_custom_call" | custom-call | tf_op jit(solution)/shard_map/pallas_call | solution.py:81
  123.1 1.0 copy-done
  124.1 0.7 shard_map.203
  124.8 7.9 %psum.7.sums_ref = f32[8,128]{1,0:T(8,128)S(1)} all-reduce(f32[8,128]{1,0:T(8,128)S(1)} %get-tuple-element.28), channel_id=1, replica_groups=mesh['sp'=128,'tp'=4] {'tp'}, use_global_device_ids=true, to_apply=%region_0.0 | all-reduce | flops 1024 | bytes 8192 | tf_op jit(solution)/shard_map/psum | solution.py:488
  132.7 1.2 copy-done.1
  133.9 1.0 shard_map.205
  135.0 14.9 %all_to_all.29 = bf16[4,192,512]{2,1,0:T(8,128)(2,1)S(1)} all-to-all(bf16[4,192,512]{2,1,0:T(8,128)(2,1)S(1)} %shard_map.205), channel_id=1, replica_groups=mesh['sp'=128,'tp'=4] {'tp'}, dimensions={0} | all-to-all | bytes 1572864 | tf_op jit(solution)/shard_map/all_to_all | solution.py:504
  149.9 0.8 reduce_sum.12
  (28 shorter events, 0.1 us)
Async XLA Ops:
  39.0 23.0 %copy-start.12 = (f32[2048]{0:T(1024)S(1)}, f32[2048]{0:T(1024)}, u32[]{:S(2)}) copy-start(f32[2048]{0:T(1024)} %param.22) | copy-start | bytes 24580
  39.0 23.0 %copy-start.11 = (bf16[192,512]{1,0:T(8,128)(2,1)S(1)}, bf16[192,512]{1,0:T(8,128)(2,1)}, u32[]{:S(2)}) copy-start(bf16[192,512]{1,0:T(8,128)(2,1)} %param.21) | copy-start | bytes 589828
  39.0 37.6 %copy-start.2 = (f32[192,128]{1,0:T(8,128)S(1)}, f32[192,128]{1,0:T(8,128)}, u32[]{:S(2)}) copy-start(f32[192,128]{1,0:T(8,128)} %extra_ref.1) | copy-start | bytes 294916
  39.0 37.6 %copy-start.4 = (f32[128]{0:T(128)S(1)}, f32[128]{0:T(128)}, u32[]{:S(2)}) copy-start(f32[128]{0:T(128)} %param.29) | copy-start | bytes 1540
  39.0 37.6 %copy-start.5 = (f32[128]{0:T(128)S(1)}, f32[128]{0:T(128)}, u32[]{:S(2)}) copy-start(f32[128]{0:T(128)} %param.30) | copy-start | bytes 1540
  39.0 37.6 %copy-start.6 = (f32[128]{0:T(128)S(1)}, f32[128]{0:T(128)}, u32[]{:S(2)}) copy-start(f32[128]{0:T(128)} %param.31) | copy-start | bytes 1540
  39.0 37.6 %copy-start.7 = (f32[128]{0:T(128)S(1)}, f32[128]{0:T(128)}, u32[]{:S(2)}) copy-start(f32[128]{0:T(128)} %param.32) | copy-start | bytes 1540
  39.0 37.6 %copy-start.8 = (f32[128]{0:T(128)S(1)}, f32[128]{0:T(128)}, u32[]{:S(2)}) copy-start(f32[128]{0:T(128)} %param.34) | copy-start | bytes 1540
  60.0 16.5 %collective-permute-start = (bf16[4,16,160,128]{3,2,1,0:T(8,128)(2,1)S(1)}, bf16[4,16,160,128]{3,2,1,0:T(8,128)(2,1)}, u32[]{:S(2)}, u32[]{:S(2)}) collective-permute-start(bf16[4,16,160,128]{3,2,1,0:T(8,128)(2,1)S(1)} %all_to_all.26.own_ref), channel_id=1, source_target_pairs={{0,4},{4,0},{8,12},{12,8},{16,20},{20,16},{24,28},{28,24},{32,36},... | collective-permute-start | bytes 7864328 | tf_op jit(solution)/shard_map/ppermute | solution.py:451
  86.8 3.1 %collective-permute-start.1 = (f32[64,128]{1,0:T(8,128)S(1)}, f32[64,128]{1,0:T(8,128)S(1)}, u32[]{:S(2)}, u32[]{:S(2)}) collective-permute-start(f32[64,128]{1,0:T(8,128)S(1)} %get-tuple-element.19), channel_id=1, source_target_pairs={{0,4},{4,0},{8,12},{12,8},{16,20},{20,16},{24,28},{28,24},{32,36},... | collective-permute-start | bytes 98312 | tf_op jit(solution)/shard_map/ppermute | solution.py:467
  116.6 16.1 %collective-permute-start.2 = (f32[64,128]{1,0:T(8,128)S(1)}, f32[64,128]{1,0:T(8,128)S(1)}, u32[]{:S(2)}, u32[]{:S(2)}) collective-permute-start(f32[64,128]{1,0:T(8,128)S(1)} %get-tuple-element.23), channel_id=1, source_target_pairs={{0,4},{4,0},{8,12},{12,8},{16,20},{20,16},{24,28},{28,24},{32,36},... | collective-permute-start | bytes 98312 | tf_op jit(solution)/shard_map/ppermute | solution.py:478
  118.5 5.5 %copy-start.3 = (f32[31,128]{1,0:T(8,128)S(1)}, f32[31,128]{1,0:T(8,128)}, u32[]{:S(2)}) copy-start(f32[31,128]{1,0:T(8,128)} %taps_ref.1) | copy-start | bytes 47620
  118.5 5.5 %copy-start.9 = (f32[128]{0:T(128)S(1)}, f32[128]{0:T(128)}, u32[]{:S(2)}) copy-start(f32[128]{0:T(128)} %param.38) | copy-start | bytes 1540
  118.5 14.2 %copy-start.10 = (f32[128]{0:T(128)S(1)}, f32[128]{0:T(128)}, u32[]{:S(2)}) copy-start(f32[128]{0:T(128)} %param.39) | copy-start | bytes 1540
  118.6 5.5 %collective-permute-start.3 = (bf16[32,128]{1,0:T(8,128)(2,1)S(1)}, bf16[32,128]{1,0:T(8,128)(2,1)S(1)}, u32[]{:S(2)}, u32[]{:S(2)}) collective-permute-start(bf16[32,128]{1,0:T(8,128)(2,1)S(1)} %get-tuple-element.26), channel_id=1, source_target_pairs={{0,4},{4,8},{8,12},{12,16},{16,20},{20,24},{24,28},{28,32},{32,36}... | collective-permute-start | bytes 24584 | tf_op jit(solution)/shard_map/ppermute | solution.py:468
  123.1 1.0 copy-start
  132.7 1.2 copy-start.1

commit v4 on v3

--- a/solution.py
+++ b/solution.py
@@ -69,6 +69,13 @@
     )
 
 
+def sums_of(ones, x):
+    high = x.astype(BF16)
+    middle, low = split(x - high.astype(F32))
+    one = lambda part: jnp.dot(ones, part, preferred_element_type=F32)
+    return one(high) + (one(middle) + one(low))
+
+
 def iota(shape, dim):
     return lax.broadcasted_iota(jnp.int32, shape, dim)
 
@@ -104,28 +111,66 @@
     )(*mats)
 
 
-def fill_rows(core, own, other, store):
+def fill_rows(core, source, height, store):
     for a in range(4):
         for b in range(16):
             row0, row1 = (
-                place(SETS[c][a // 2][b // 4], SETS[c][a % 2][b % 4], c) * 16 for c in range(2)
+                height(SETS[c][a // 2][b // 4], SETS[c][a % 2][b % 4], c) for c in range(2)
             )
-            store(pl.multiple_of(jnp.where(core == 0, row0, row1), 16), own, a, b)
-            store(pl.multiple_of(jnp.where(core == 0, row1, row0), 16), other, a, b)
+            store(pl.multiple_of(jnp.where(core == 0, row0, row1), 16), source, a, b)
+
+
+def norm_kernel(place_ref, tokens_ref, gain_ref, *refs):
+    vectors, (taps_ref, extra_ref), (normed_ref, table_ref, extra_out_ref) = (
+        refs[:-5],
+        refs[-5:-3],
+        refs[-3:],
+    )
+    parts = [tokens_ref[j].astype(F32) for j in range(4)]
+    total = sum(jnp.sum(part * part, axis=-1, keepdims=True) for part in parts)
+    inverse_rms = lax.rsqrt(total * (1.0 / 2048.0) + 1e-06)
+    goal = iota((256, 256), 1)
+    source = ((goal % 128) // 16) * 32 + (goal // 128) * 16 + goal % 16
+    moves = jnp.where(iota((256, 256), 0) == source, 1.0, 0.0).astype(BF16)
+    for j in range(4):
+        normed = (parts[j] * inverse_rms * gain_ref[j : j + 1, :]).astype(BF16)
+        for k in range(2):
+            moved = jnp.dot(
+                normed[:, k * 256 : k * 256 + 256], moves, preferred_element_type=F32
+            ).astype(BF16)
+            z = j * 2 + k
+            normed_ref[0, :, z * 128 : z * 128 + 128] = moved[:, :128]
+            normed_ref[1, :, z * 128 : z * 128 + 128] = moved[:, 128:]
+    for k, ref in enumerate(vectors):
+        table_ref[k : k + 1, :] = ref[...]
+    table_ref[8 : 8 + TAPS, :] = taps_ref[...]
+    extra_out_ref[...] = extra_ref[...]
+
+
+def projected(core, source_ref, normed_ref, weights):
+    def store(row, source, a, b):
+        for m in range(MATS):
+            lanes = slice((m % 2) * 128, (m % 2) * 128 + 128)
+            weights[m // 2, pl.ds(row, 16), lanes] = source[a, b, m * 16 : m * 16 + 16, :]
+
+    fill_rows(core, source_ref, lambda z, y, c: (z * 8 + y) * 16, store)
+    normed = normed_ref[core]
+    return [jnp.dot(normed, weights[p], preferred_element_type=F32) for p in range(MATS // 2)]
+
+
+def half_kernel(place_ref, own_ref, normed_ref, out_ref, weights):
+    products = projected(place_ref[0] % 2, own_ref, normed_ref, weights)
+    for p in range(MATS // 2):
+        out_ref[p] = products[p]
 
 
 def local_kernel(
     core_ref,
-    own_ref,
     other_ref,
-    tokens_ref,
-    norm_gain_ref,
-    key_gain_ref,
-    removal_gain_ref,
-    removal_bias_ref,
-    decay_bias_ref,
+    normed_ref,
+    half_ref,
+    table_ref,
     extra_ref,
-    norm_out_ref,
     mine_ref,
     theirs_ref,
     reads_ref,
@@ -133,50 +178,40 @@
     conv_ref,
     rim_ref,
     weights,
-    normed,
 ):
     core = core_ref[0] % 2
-
-    def store(row, source, a, b):
-        for m in range(MATS):
-            lanes = slice((m % 2) * 128, (m % 2) * 128 + 128)
-            weights[m // 2, pl.ds(row, 16), lanes] = source[a, b, m * 16 : m * 16 + 16, :]
-
-    fill_rows(core, own_ref, other_ref, store)
-    parts = [tokens_ref[j].astype(F32) for j in range(4)]
-    total = sum(jnp.sum(part * part, axis=-1, keepdims=True) for part in parts)
-    inverse_rms = lax.rsqrt(total * (1.0 / 2048.0) + 1e-06)
-    for j in range(4):
-        normed[:, j * 512 : j * 512 + 512] = (
-            parts[j] * inverse_rms * norm_gain_ref[j : j + 1, :]
-        ).astype(BF16)
     products = []
-    for p in range(4):
-        product = jnp.dot(normed[...], weights[p], preferred_element_type=F32)
-        product = product.astype(BF16).astype(F32)
+    for p, product in enumerate(projected(1 - core, other_ref, normed_ref, weights)):
+        product = (product + half_ref[p]).astype(BF16).astype(F32)
         products += [product[:, :128], product[:, 128:]]
     recept, keys, values, decay_pre, removal_pre, gate_pre, conv_value, conv_gate = products
-    gate_ref[...] = norm_out_ref[...] * jax.nn.sigmoid(gate_pre)
+    key_gain, removal_gain, removal_bias, decay_bias, norm_out = (
+        table_ref[k : k + 1, :] for k in range(5)
+    )
+    gate_ref[...] = norm_out * jax.nn.sigmoid(gate_pre)
     conv_input = (conv_value * jax.nn.sigmoid(conv_gate)).astype(BF16)
     conv_ref[...] = conv_input
     rim_ref[...] = conv_input[LENGTH - 32 :]
 
-    rate = 0.6065306597126334 * jax.nn.sigmoid(decay_bias_ref[...] + decay_pre) + extra_ref[...]
-    removal = jax.nn.sigmoid(removal_bias_ref[...] + removal_pre)
+    rate = 0.6065306597126334 * jax.nn.sigmoid(decay_bias + decay_pre) + extra_ref[...]
+    removal = jax.nn.sigmoid(removal_bias + removal_pre)
     lane = iota((LENGTH, 128), 1)
     first = lane < HEAD
-    scaled = keys * key_gain_ref[...]
+    scaled = keys * key_gain
     square = scaled * scaled
     low = jnp.sum(jnp.where(first, square, 0.0), axis=-1, keepdims=True)
     high = jnp.sum(jnp.where(first, 0.0, square), axis=-1, keepdims=True)
     unit = scaled * lax.rsqrt(jnp.where(first, low, high) + 1e-06)
-    written = keys * (1.0 + (removal - 1.0) * removal_gain_ref[...])
+    written = keys * (1.0 + (removal - 1.0) * removal_gain)
 
     row, column = iota((LENGTH, LENGTH), 0), iota((LENGTH, LENGTH), 1)
     same = (row // BLOCK) == (column // BLOCK)
     strict = same & (row > column)
     inclusive = same & (row >= column)
-    falling = -exact(inclusive.astype(F32), rate)
+    wide_row, wide_column = iota((LENGTH, 2 * LENGTH), 0), iota((LENGTH, 2 * LENGTH), 1)
+    wide_column = jnp.where(wide_column >= LENGTH, wide_column - LENGTH, wide_column)
+    inclusive_twice = ((wide_row // BLOCK) == (wide_column // BLOCK)) & (wide_row >= wide_column)
+    falling = -sums_of(jnp.where(inclusive, 1.0, 0.0).astype(BF16), rate)
     before = falling + rate
     by_block = falling.reshape(BLOCKS, BLOCK, 128)
     middle = jnp.broadcast_to(
@@ -198,75 +233,60 @@
 
     square_row, square_lane = iota((128, 128), 0), iota((128, 128), 1)
     diagonal = square_row == square_lane
-    finals = []
+    own = [first, jnp.logical_not(first)]
+    own_row = [square_row < HEAD, square_row >= HEAD]
+    power, solved, query, value_rows = [], [], [], []
+    recept_pairs = []
     for h in range(2):
-        mine = first if h == 0 else jnp.logical_not(first)
-        mine_row = (square_row < HEAD) if h == 0 else (square_row >= HEAD)
         left = jnp.concatenate(
-            [jnp.where(mine, alpha_mid, 0.0), jnp.where(mine, recept_mid, 0.0)], axis=0
+            [jnp.where(own[h], alpha_mid, 0.0), jnp.where(own[h], recept_mid, 0.0)], axis=0
         )
         pairs = dot3(left, right, NT)
-        power = jnp.where(strict, pairs[:LENGTH, :LENGTH], 0.0)
+        power.append(jnp.where(strict, pairs[:LENGTH, :LENGTH], 0.0))
         alpha_keys = jnp.where(strict, pairs[:LENGTH, LENGTH:], 0.0)
-        recept_beta = jnp.where(inclusive, pairs[LENGTH:, :LENGTH], 0.0)
-        recept_keys = jnp.where(inclusive, pairs[LENGTH:, LENGTH:], 0.0)
-        value_rows = jnp.where(mine, 0.0, turned_values)
-        solved = jnp.where(mine, start_alpha, dot3(alpha_keys, value_rows))
-        for step in range(5):
-            solved = solved + dot3(power, solved)
-            if step < 4:
-                power = dot3(power, power)
-        query = jnp.where(mine, start_recept, 0.0) + dot3(
-            jnp.concatenate([recept_beta, recept_keys], axis=1),
-            jnp.concatenate([solved, value_rows], axis=0),
-        )
-        steps = []
-        for b in range(BLOCKS):
-            rows = slice(b * BLOCK, b * BLOCK + BLOCK)
-            moved = dot3(
-                jnp.concatenate([end_beta[rows], end_keys[rows]], axis=0),
-                jnp.concatenate([solved[rows], value_rows[rows]], axis=0),
-                TN,
-            )
-            held = jnp.where(diagonal, jnp.broadcast_to(kept[b : b + 1], (128, 128)), 0.0)
-            whole = jnp.where(diagonal, 1.0, 0.0)
-            steps.append(jnp.where(mine_row, moved + held, whole))
-        one = dot3(steps[1], steps[0])
-        two = dot3(steps[3], steps[2])
-        three = dot3(steps[5], steps[4])
-        four = dot3(two, one)
-        prefixes = [None, steps[0], one, dot3(steps[2], one), four, dot3(steps[4], four)]
-        final = dot3(three, four)[h * HEAD : h * HEAD + HEAD]
-        if h == 1:
-            final = pltpu.roll(final, HEAD, 1)
-        finals.append(final)
-        reads_ref[h, 0:BLOCK, :] = query[0:BLOCK]
+        recept_pairs.append(jnp.where(inclusive_twice, pairs[LENGTH:], 0.0))
+        value_rows.append(jnp.where(own[h], 0.0, turned_values))
+        solved.append(jnp.where(own[h], start_alpha, dot3(alpha_keys, value_rows[h])))
+    for step in range(5):
+        solved = [solved[h] + dot3(power[h], solved[h]) for h in range(2)]
+        if step < 4:
+            power = [dot3(power[h], power[h]) for h in range(2)]
+    for h in range(2):
+        known = jnp.concatenate([solved[h], value_rows[h]], axis=0)
+        query.append(jnp.where(own[h], start_recept, 0.0) + dot3(recept_pairs[h], known))
+    steps = [[], []]
+    whole = jnp.where(diagonal, 1.0, 0.0)
+    for b in range(BLOCKS):
+        rows = slice(b * BLOCK, b * BLOCK + BLOCK)
+        ends = jnp.concatenate([end_beta[rows], end_keys[rows]], axis=0)
+        held = jnp.where(diagonal, jnp.broadcast_to(kept[b : b + 1], (128, 128)), 0.0)
+        for h in range(2):
+            known = jnp.concatenate([solved[h][rows], value_rows[h][rows]], axis=0)
+            steps[h].append(jnp.where(own_row[h], dot3(ends, known, TN) + held, whole))
+    one = [dot3(steps[h][1], steps[h][0]) for h in range(2)]
+    two = [dot3(steps[h][3], steps[h][2]) for h in range(2)]
+    three = [dot3(steps[h][5], steps[h][4]) for h in range(2)]
+    four = [dot3(two[h], one[h]) for h in range(2)]
+    finals = [dot3(three[h], four[h])[h * HEAD : h * HEAD + HEAD] for h in range(2)]
+    finals[1] = pltpu.roll(finals[1], HEAD, 1)
+    mine_ref[...] = jnp.where(core == 0, finals[0], finals[1])
+    theirs_ref[...] = jnp.where(core == 0, finals[1], finals[0])
+    for h in range(2):
+        prefixes = [
+            None,
+            steps[h][0],
+            one[h],
+            dot3(steps[h][2], one[h]),
+            four[h],
+            dot3(steps[h][4], four[h]),
+        ]
+        reads_ref[h, 0:BLOCK, :] = query[h][0:BLOCK]
         for b in range(1, BLOCKS):
             rows = slice(b * BLOCK, b * BLOCK + BLOCK)
-            reads_ref[h, rows, :] = dot3(query[rows], prefixes[b])
-    mine_ref[...] = jnp.where(core == 0, finals[0], finals[1])
-    theirs_ref[...] = jnp.where(core == 0, finals[1], finals[0])
-
-
-def local_part(index, own, other, tokens, *given):
-    return on_core(
-        local_kernel,
-        (
-            vmem((HEAD, 128), F32),
-            vmem((HEAD, 128), F32),
-            vmem((2, LENGTH, 128), F32),
-            vmem((LENGTH, 128), F32),
-            vmem((LENGTH, 128), BF16),
-            vmem((32, 128), BF16),
-        ),
-        index,
-        own,
-        other,
-        tokens,
-        given=given,
-        scratch=[pltpu.VMEM((4, 2048, 256), BF16), pltpu.VMEM((LENGTH, 2048), BF16)],
-        limit=28,
-    )
+            reads_ref[h, rows, :] = dot3(query[h][rows], prefixes[b])
+
+
+WEIGHTS = (MATS // 2, 1024, 256)
 
 
 def after(later, earlier):
@@ -318,11 +338,11 @@
     sent_ref[...] = jnp.where(core == 0, at_second, at_chip)
 
 
-def conv_kernel(place_ref, input_ref, rim_ref, taps_ref, bias_ref, filtered_ref, sums_ref):
+def conv_kernel(place_ref, input_ref, rim_ref, table_ref, filtered_ref, sums_ref):
     padded = jnp.concatenate([rim_ref[...], input_ref[...]], axis=0).astype(F32)
-    filtered = jnp.broadcast_to(bias_ref[...], (LENGTH, 128))
+    filtered = jnp.broadcast_to(table_ref[5:6, :], (LENGTH, 128))
     for k in range(TAPS):
-        filtered = filtered + taps_ref[k : k + 1, :] * padded[k + 2 : k + 2 + LENGTH]
+        filtered = filtered + table_ref[8 + k : 9 + k, :] * padded[k + 2 : k + 2 + LENGTH]
     filtered_ref[...] = filtered
     ones = jnp.ones((8, 128), F32)
     square = filtered * filtered
@@ -334,12 +354,16 @@
 
 
 def columns_kernel(core_ref, own_ref, other_ref, out_ref):
+    core = core_ref[0] % 2
+
     def store(row, source, a, b):
         for m in range(2):
             at = (MATS + m) * 16
             out_ref[pl.ds(row, 16), m * 128 : m * 128 + 128] = source[a, b, at : at + 16, :]
 
-    fill_rows(core_ref[0] % 2, own_ref, other_ref, store)
+    height = lambda z, y, c: place(z, y, c) * 16
+    fill_rows(core, own_ref, height, store)
+    fill_rows(1 - core, other_ref, height, store)
 
 
 def final_kernel(
@@ -351,7 +375,7 @@
     filtered_ref,
     sums_ref,
     columns_ref,
-    conv_gain_ref,
+    table_ref,
     out_ref,
 ):
     core = core_ref[0] % 2
@@ -392,7 +416,7 @@
     scaled = (
         (filtered_ref[...] - center)
         * lax.rsqrt(second - center * center + 1e-05)
-        * conv_gain_ref[...]
+        * table_ref[6:7, :]
     )
     conv_out = (scaled * jax.nn.sigmoid(scaled)).astype(BF16)
     features = jnp.concatenate([scan_out, conv_out], axis=1)
@@ -448,29 +472,61 @@
     wide = jnp.broadcast_to(stage1[None], (4, *stage1.shape))
     stage2 = to_each(wide, NEAR)
     whole = lax.all_gather(tokens, "tp")
+    normed, table, extra = on_core(
+        norm_kernel,
+        (vmem((2, LENGTH, 1024), BF16), vmem((40, 128), F32), vmem((LENGTH, 128), F32)),
+        index,
+        whole,
+        given=(
+            norm_gain.reshape(4, 512),
+            row(key_gain),
+            row(removal_gain),
+            row(removal_bias),
+            row(decay_bias),
+            row(scan_norm_gain),
+            row(conv_bias),
+            row(conv_norm_gain),
+            conv_taps,
+            decay_extra,
+        ),
+    )
     swapped = lax.ppermute(stage2, "sp", SWAP)
-
-    mine, theirs, reads, gate, conv_input, rim = local_part(
+    half = on_core(
+        half_kernel,
+        vmem((MATS // 2, LENGTH, 256), F32),
         index,
         stage2,
+        normed,
+        scratch=[pltpu.VMEM(WEIGHTS, BF16)],
+        limit=16,
+    )
+    mine, theirs, reads, gate, conv_input, rim = on_core(
+        local_kernel,
+        (
+            vmem((HEAD, 128), F32),
+            vmem((HEAD, 128), F32),
+            vmem((2, LENGTH, 128), F32),
+            vmem((LENGTH, 128), F32),
+            vmem((LENGTH, 128), BF16),
+            vmem((32, 128), BF16),
+        ),
+        index,
         swapped,
-        whole,
-        norm_gain.reshape(4, 512),
-        row(key_gain),
-        row(removal_gain),
-        row(removal_bias),
-        row(decay_bias),
-        decay_extra,
-        row(scan_norm_gain),
+        normed,
+        half,
+        table,
+        extra,
+        scratch=[pltpu.VMEM(WEIGHTS, BF16)],
+        limit=28,
     )
 
     theirs = lax.ppermute(theirs, "sp", SWAP)
     rim = lax.ppermute(rim, "sp", ONWARD)
-    table = vmem((8, HEAD, 128), BF16)
+    message = vmem((8, HEAD, 128), BF16)
     step = vmem((HEAD, 128), F32)
-    chip = on_core(chip_kernel, table, index, mine, theirs)
+    chip = on_core(chip_kernel, message, index, mine, theirs)
     chips = to_each(chip, Y_AXIS)
-    before, total = on_core(row_kernel, (step, table), index, chips)
+    before, total = on_core(row_kernel, (step, message), index, chips)
     totals = to_each(total, Z_AXIS)
     own_state, sent_state = on_core(
         incoming_kernel, (step, step), index, totals, before, mine, theirs
@@ -478,12 +534,7 @@
     other_state = lax.ppermute(sent_state, "sp", SWAP)
 
     filtered, sums = on_core(
-        conv_kernel,
-        (vmem((LENGTH, 128), F32), vmem((8, 128), F32)),
-        index,
-        conv_input,
-        rim,
-        given=(conv_taps, row(conv_bias)),
+        conv_kernel, (vmem((LENGTH, 128), F32), vmem((8, 128), F32)), index, conv_input, rim, table
     )
     sums = lax.psum(sums, "tp")
     columns = on_core(columns_kernel, vmem((2048, 256), BF16), index, stage2, swapped)
@@ -499,7 +550,7 @@
         filtered,
         sums,
         columns,
-        given=(row(conv_norm_gain),),
+        table,
     )
     parts = lax.all_to_all(terms, "tp", 0, 0, tiled=True)
     return jnp.sum(parts.astype(F32), axis=0).astype(BF16)

time: 151 us -> 151 us (level)
    pallas_call x7 -> x9, Pallas kernels: 15.7 us -> 15.1 us  [on_core(): pl.pallas_call(kernel, in_specs=[pl.BlockSpec(memory_space=pltpu.SMEM)] +...]
  transfers between devices with their start and end apart: 4 -> 4, of which waited for: 1 -> 1; matrix products, arithmetic and copies ran while one was open for 0% -> 0% of each run, Pallas kernels for 2% -> 3%
where the time goes in v4:
time: 151 us; the launch traced here: 150 us
  blocking collectives  120 us (79%)
  Pallas kernels  16.8 us (11%)
  starting transfers between devices  8.16 us (5%)
  local copies, waits for them, and re-layouts  2.67 us (2%)
    all_to_all x4, blocking collectives, to_each(): return lax.all_to_all(x, 'sp', 0, 0, tiled=True, axis_index_groups=groups)  82.7 us
    pallas_call x9, Pallas kernels, on_core(): pl.pallas_call(kernel, in_specs=[pl.BlockSpec(memory_space=pltpu.SMEM)] +...  15.1 us
    all_to_all x1, blocking collectives, layer(): parts = lax.all_to_all(terms, 'tp', 0, 0, tiled=True)  14.9 us
    all_gather x1, blocking collectives, layer(): whole = lax.all_gather(tokens, 'tp')  14.6 us
    psum x1, blocking collectives, layer(): sums = lax.psum(sums, 'tp')  7.89 us
  transfers between devices with their start and end apart: 4, of which 1 were waited for; matrix products, arithmetic and copies ran while one was open for 0% of the time, Pallas kernels for 3%

profile of v4, /device:TPU:2, one launch (start us, length us, event | category | flops | bytes accessed | tf_op | source)
XLA Modules:
  0.0 150.0 jit_solution(12984787470028753298)
XLA Ops:
  0.0 1.8 %pack.1 = bf16[16,160,128]{2,1,0:T(8,128)(2,1)} custom-call(bf16[16,128]{1,0:T(8,128)(2,1)} %refs_0_.1, bf16[16,128]{1,0:T(8,128)(2,1)} %refs_1_.1, bf16[16,128]{1,0:T(8,128)(2,1)} %refs_2_.1, bf16[16,128]{1,0:T(8,128)(2,1)} %refs_3_.1, bf16[16,128]{1,0:T(8,128)(2,1)} %refs_4_.1, bf16[16,128]{1,0:T(8,128)(2,1)} %refs_5_.1, bf16[16,128]{1,0:T(8,128)(2,1)} %refs_6_.1, ...), custom_call_target="tpu_custom_call" | custom-call | tf_op jit(solution)/shard_map/pack/pallas_call | solution.py:107
  1.8 36.8 %all_to_all.25 = bf16[16,160,128]{2,1,0:T(8,128)(2,1)S(1)} all-to-all(bf16[16,160,128]{2,1,0:T(8,128)(2,1)} %pack.1), channel_id=1, replica_groups={{0,16,40,56,128,144,168,184,320,336,360,376,448,464,488,504},{8,24,32,4..., dimensions={0} | all-to-all | bytes 1310720 | tf_op jit(solution)/shard_map/all_to_all | solution.py:430
  39.1 21.0 %all_to_all.26.own_ref = bf16[4,16,160,128]{3,2,1,0:T(8,128)(2,1)S(1)} all-to-all(bf16[4,16,160,128]{3,2,1,0:T(8,128)(2,1)S(1)} %broadcast_in_dim.10), channel_id=1, replica_groups={{0,8,64,72},{16,24,80,88},{40,32,104,96},{56,48,120,112},{128,136,192,2..., dimensions={0} | all-to-all | bytes 5242880 | tf_op jit(solution)/shard_map/all_to_all | solution.py:430
  60.1 1.9 %collective-permute-start = (bf16[4,16,160,128]{3,2,1,0:T(8,128)(2,1)S(1)}, bf16[4,16,160,128]{3,2,1,0:T(8,128)(2,1)}, u32[]{:S(2)}, u32[]{:S(2)}) collective-permute-start(bf16[4,16,160,128]{3,2,1,0:T(8,128)(2,1)S(1)} %all_to_all.26.own_ref), channel_id=1, source_target_pairs={{0,4},{4,0},{8,12},{12,8},{16,20},{20,16},{24,28},{28,24},{32,36},... | collective-permute-start | bytes 7864328 | tf_op jit(solution)/shard_map/ppermute | solution.py:493
  62.0 14.6 %all-gather = bf16[768,512]{1,0:T(8,128)(2,1)S(1)} all-gather(bf16[192,512]{1,0:T(8,128)(2,1)S(1)} %copy-done.11), channel_id=2, replica_groups=mesh['sp'=128,'tp'=4] {'tp'}, dimensions={0}, use_global_device_ids=true | all-gather | bytes 983040 | tf_op jit(solution)/shard_map/all_gather | solution.py:474
  76.7 0.6 shard_map.199
  77.2 1.0 shard_map.200.half_ref
  78.3 8.0 %shard_map.201 = (f32[64,128]{1,0:T(8,128)S(1)}, f32[64,128]{1,0:T(8,128)S(1)}, f32[2,192,128]{2,1,0:T(8,128)S(1)}, f32[192,128]{1,0:T(8,128)S(1)}, bf16[192,128...) custom-call(s32[1]{0:T(128)} %bitcast.place_ref.core_ref, bf16[4,16,160,128]{3,2,1,0:T(8,128)(2,1)} %collective-permute-done.other_ref, ...), custom_call_target="tpu_custom_call" | custom-call | tf_op jit(solution)/shard_map/pallas_call | solution.py:88
  86.2 1.9 %collective-permute-start.1 = (f32[64,128]{1,0:T(8,128)S(1)}, f32[64,128]{1,0:T(8,128)S(1)}, u32[]{:S(2)}, u32[]{:S(2)}) collective-permute-start(f32[64,128]{1,0:T(8,128)S(1)} %get-tuple-element.25), channel_id=1, source_target_pairs={{0,4},{4,0},{8,12},{12,8},{16,20},{20,16},{24,28},{28,24},{32,36},... | collective-permute-start | bytes 98312 | tf_op jit(solution)/shard_map/ppermute | solution.py:523
  88.2 1.2 collective-permute-done.1.theirs_ref
  89.5 12.6 %all_to_all.27.steps_ref = bf16[8,64,128]{2,1,0:T(8,128)(2,1)S(1)} all-to-all(bf16[8,64,128]{2,1,0:T(8,128)(2,1)S(1)} %shard_map.202), channel_id=1, replica_groups={{0,8,16,24,32,40,48,56},{4,12,20,28,36,44,52,60},{64,72,80,88,96,104,11..., dimensions={0} | all-to-all | bytes 262144 | tf_op jit(solution)/shard_map/all_to_all | solution.py:430
  102.1 0.8 shard_map.203
  102.9 12.4 %all_to_all.28.steps_ref = bf16[8,64,128]{2,1,0:T(8,128)(2,1)S(1)} all-to-all(bf16[8,64,128]{2,1,0:T(8,128)(2,1)S(1)} %get-tuple-element.26), channel_id=1, replica_groups={{0,64,128,192,256,320,384,448},{4,68,132,196,260,324,388,452},{8,72,136..., dimensions={0} | all-to-all | bytes 262144 | tf_op jit(solution)/shard_map/all_to_all | solution.py:430
  115.2 0.8 shard_map.204
  116.0 1.9 %collective-permute-start.2 = (f32[64,128]{1,0:T(8,128)S(1)}, f32[64,128]{1,0:T(8,128)S(1)}, u32[]{:S(2)}, u32[]{:S(2)}) collective-permute-start(f32[64,128]{1,0:T(8,128)S(1)} %get-tuple-element.29), channel_id=1, source_target_pairs={{0,4},{4,0},{8,12},{12,8},{16,20},{20,16},{24,28},{28,24},{32,36},... | collective-permute-start | bytes 98312 | tf_op jit(solution)/shard_map/ppermute | solution.py:534
  117.9 2.4 %collective-permute-start.3 = (bf16[32,128]{1,0:T(8,128)(2,1)S(1)}, bf16[32,128]{1,0:T(8,128)(2,1)S(1)}, u32[]{:S(2)}, u32[]{:S(2)}) collective-permute-start(bf16[32,128]{1,0:T(8,128)(2,1)S(1)} %get-tuple-element.32), channel_id=1, source_target_pairs={{0,4},{4,8},{8,12},{12,16},{16,20},{20,24},{24,28},{28,32},{32,36}... | collective-permute-start | bytes 24584 | tf_op jit(solution)/shard_map/ppermute | solution.py:524
  120.3 2.0 %shard_map.206.columns_ref = bf16[2048,256]{1,0:T(8,128)(2,1)S(1)} custom-call(s32[1]{0:T(128)} %bitcast.place_ref.core_ref, bf16[4,16,160,128]{3,2,1,0:T(8,128)(2,1)S(1)} %all_to_all.26.own_ref, bf16[4,16,160,128]{3,2,1,0:T(8,128)(2,1)} %collective-permute-done.other_ref), custom_call_target="tpu_custom_call" | custom-call | tf_op jit(solution)/shard_map/pallas_call | solution.py:88
  122.3 1.0 copy-done
  123.3 0.7 shard_map.205
  124.1 7.9 %psum.7.sums_ref = f32[8,128]{1,0:T(8,128)S(1)} all-reduce(f32[8,128]{1,0:T(8,128)S(1)} %get-tuple-element.34), channel_id=1, replica_groups=mesh['sp'=128,'tp'=4] {'tp'}, use_global_device_ids=true, to_apply=%region_0.0 | all-reduce | flops 1024 | bytes 8192 | tf_op jit(solution)/shard_map/psum | solution.py:539
  132.0 1.2 copy-done.1
  133.2 1.1 shard_map.207
  134.2 14.9 %all_to_all.29 = bf16[4,192,512]{2,1,0:T(8,128)(2,1)S(1)} all-to-all(bf16[4,192,512]{2,1,0:T(8,128)(2,1)S(1)} %shard_map.207), channel_id=1, replica_groups=mesh['sp'=128,'tp'=4] {'tp'}, dimensions={0} | all-to-all | bytes 1572864 | tf_op jit(solution)/shard_map/all_to_all | solution.py:555
  149.1 0.8 reduce_sum.12
  (30 shorter events, 0.6 us)
Async XLA Ops:
  39.0 23.0 %copy-start.12 = (f32[2048]{0:T(1024)S(1)}, f32[2048]{0:T(1024)}, u32[]{:S(2)}) copy-start(f32[2048]{0:T(1024)} %param.22) | copy-start | bytes 24580
  39.0 23.1 %copy-start.11 = (bf16[192,512]{1,0:T(8,128)(2,1)S(1)}, bf16[192,512]{1,0:T(8,128)(2,1)}, u32[]{:S(2)}) copy-start(bf16[192,512]{1,0:T(8,128)(2,1)} %param.21) | copy-start | bytes 589828
  39.0 37.6 %copy-start.2 = (f32[192,128]{1,0:T(8,128)S(1)}, f32[192,128]{1,0:T(8,128)}, u32[]{:S(2)}) copy-start(f32[192,128]{1,0:T(8,128)} %refs_8_.1) | copy-start | bytes 294916
  39.0 37.6 %copy-start.3 = (f32[31,128]{1,0:T(8,128)S(1)}, f32[31,128]{1,0:T(8,128)}, u32[]{:S(2)}) copy-start(f32[31,128]{1,0:T(8,128)} %refs_7_.3) | copy-start | bytes 47620
  39.0 37.6 %copy-start.4 = (f32[128]{0:T(128)S(1)}, f32[128]{0:T(128)}, u32[]{:S(2)}) copy-start(f32[128]{0:T(128)} %param.29) | copy-start | bytes 1540
  39.0 37.6 %copy-start.5 = (f32[128]{0:T(128)S(1)}, f32[128]{0:T(128)}, u32[]{:S(2)}) copy-start(f32[128]{0:T(128)} %param.30) | copy-start | bytes 1540
  39.0 37.6 %copy-start.6 = (f32[128]{0:T(128)S(1)}, f32[128]{0:T(128)}, u32[]{:S(2)}) copy-start(f32[128]{0:T(128)} %param.31) | copy-start | bytes 1540
  39.0 37.6 %copy-start.7 = (f32[128]{0:T(128)S(1)}, f32[128]{0:T(128)}, u32[]{:S(2)}) copy-start(f32[128]{0:T(128)} %param.32) | copy-start | bytes 1540
  39.1 37.6 %copy-start.8 = (f32[128]{0:T(128)S(1)}, f32[128]{0:T(128)}, u32[]{:S(2)}) copy-start(f32[128]{0:T(128)} %param.34) | copy-start | bytes 1540
  39.1 37.6 %copy-start.9 = (f32[128]{0:T(128)S(1)}, f32[128]{0:T(128)}, u32[]{:S(2)}) copy-start(f32[128]{0:T(128)} %param.38) | copy-start | bytes 1540
  39.1 37.6 %copy-start.10 = (f32[128]{0:T(128)S(1)}, f32[128]{0:T(128)}, u32[]{:S(2)}) copy-start(f32[128]{0:T(128)} %param.39) | copy-start | bytes 1540
  60.1 18.2 %collective-permute-start = (bf16[4,16,160,128]{3,2,1,0:T(8,128)(2,1)S(1)}, bf16[4,16,160,128]{3,2,1,0:T(8,128)(2,1)}, u32[]{:S(2)}, u32[]{:S(2)}) collective-permute-start(bf16[4,16,160,128]{3,2,1,0:T(8,128)(2,1)S(1)} %all_to_all.26.own_ref), channel_id=1, source_target_pairs={{0,4},{4,0},{8,12},{12,8},{16,20},{20,16},{24,28},{28,24},{32,36},... | collective-permute-start | bytes 7864328 | tf_op jit(solution)/shard_map/ppermute | solution.py:493
  86.2 3.1 %collective-permute-start.1 = (f32[64,128]{1,0:T(8,128)S(1)}, f32[64,128]{1,0:T(8,128)S(1)}, u32[]{:S(2)}, u32[]{:S(2)}) collective-permute-start(f32[64,128]{1,0:T(8,128)S(1)} %get-tuple-element.25), channel_id=1, source_target_pairs={{0,4},{4,0},{8,12},{12,8},{16,20},{20,16},{24,28},{28,24},{32,36},... | collective-permute-start | bytes 98312 | tf_op jit(solution)/shard_map/ppermute | solution.py:523
  116.0 15.9 %collective-permute-start.2 = (f32[64,128]{1,0:T(8,128)S(1)}, f32[64,128]{1,0:T(8,128)S(1)}, u32[]{:S(2)}, u32[]{:S(2)}) collective-permute-start(f32[64,128]{1,0:T(8,128)S(1)} %get-tuple-element.29), channel_id=1, source_target_pairs={{0,4},{4,0},{8,12},{12,8},{16,20},{20,16},{24,28},{28,24},{32,36},... | collective-permute-start | bytes 98312 | tf_op jit(solution)/shard_map/ppermute | solution.py:534
  117.9 5.4 %collective-permute-start.3 = (bf16[32,128]{1,0:T(8,128)(2,1)S(1)}, bf16[32,128]{1,0:T(8,128)(2,1)S(1)}, u32[]{:S(2)}, u32[]{:S(2)}) collective-permute-start(bf16[32,128]{1,0:T(8,128)(2,1)S(1)} %get-tuple-element.32), channel_id=1, source_target_pairs={{0,4},{4,8},{8,12},{12,16},{16,20},{20,24},{24,28},{28,32},{32,36}... | collective-permute-start | bytes 24584 | tf_op jit(solution)/shard_map/ppermute | solution.py:524
  122.3 1.0 copy-start
  131.9 1.2 copy-start.1

commit v5 on v4

--- a/solution.py
+++ b/solution.py
@@ -26,25 +26,25 @@
 
 
 SETS = (((0, 2, 5, 7), (1, 3, 4, 6)), ((1, 3, 6, 0), (2, 4, 5, 7)))
-FAR = [
-    [place(z, y, c) for z in SETS[c][p] for y in SETS[c][q]]
-    for c in range(2)
-    for p in range(2)
-    for q in range(2)
-]
-
-
-def near(k, p, c):
-    pair = ((2 * k + c) % 8, (2 * k + c + 1) % 8)
-    return [chip for chip in pair if chip in SETS[c][p]][0]
-
-
-NEAR = [
-    [place(near(k, p, c), near(l, q, c), c) for p in range(2) for q in range(2)]
-    for c in range(2)
-    for k in range(4)
-    for l in range(4)
-]
+FAR_Y = [[[place(z, y, c) for y in ys] for z in range(8) for ys in SETS[c]] for c in range(2)]
+FAR_Z = [[[place(z, y, c) for z in zs] for y in range(8) for zs in SETS[c]] for c in range(2)]
+FAR_FIRST = FAR_Y[0] + FAR_Z[1]
+FAR_SECOND = FAR_Z[0] + FAR_Y[1]
+
+
+def partner(v, c):
+    return v ^ 1 if c == 0 else (((v - 1) % 8 ^ 1) + 1) % 8
+
+
+def neighbours(along_z, along_y):
+    return [
+        (place(z, y, c), place(partner(z, c) if along_z else z, partner(y, c) if along_y else y, c))
+        for z in range(8)
+        for y in range(8)
+        for c in range(2)
+    ]
+
+
 Y_AXIS = [[place(z, y, c) for y in range(8)] for z in range(8) for c in range(2)]
 Z_AXIS = [[place(z, y, c) for z in range(8)] for y in range(8) for c in range(2)]
 SWAP = [(i, i ^ 1) for i in range(128)]
@@ -99,74 +99,112 @@
     out = refs[-1]
     blocks = [ref[...] for ref in refs[:-1]]
     both = jnp.concatenate(blocks, axis=0)
-    for k in range(16):
+    for k in range(4):
         out[k] = both
 
 
 def pack(*mats):
     return pl.pallas_call(
         pack_kernel,
-        out_shape=jax.ShapeDtypeStruct((16, 16 * len(mats), 128), BF16),
+        out_shape=jax.ShapeDtypeStruct((4, 16 * len(mats), 128), BF16),
         name="pack",
     )(*mats)
 
 
-def fill_rows(core, source, height, store):
-    for a in range(4):
+FLIPS = ((0, 0), (0, 1), (1, 0), (1, 1))
+
+
+def chosen(conditions, values):
+    if not conditions:
+        return values[0]
+    half = len(values) // 2
+    low, high = (chosen(conditions[1:], part) for part in (values[:half], values[half:]))
+    return low if isinstance(low, int) and low == high else jnp.where(conditions[0], high, low)
+
+
+def fill_rows(index, core, pieces, height, store):
+    second = core == 1
+
+    def axis(position):
+        in_set1 = functools.reduce(
+            jnp.logical_or,
+            [
+                jnp.logical_and(second == (c == 1), position == v)
+                for c in range(2)
+                for v in SETS[c][1]
+            ],
+        )
+        return [
+            [
+                chosen(
+                    (second, in_set1),
+                    [SETS[c][p ^ flip][k] for c in range(2) for p in range(2)],
+                )
+                for k in range(4)
+            ]
+            for flip in range(2)
+        ]
+
+    zs, ys = axis(index // 16), axis((index // 2) % 8)
+    for piece, (flip_z, flip_y) in zip(pieces, FLIPS):
         for b in range(16):
-            row0, row1 = (
-                height(SETS[c][a // 2][b // 4], SETS[c][a % 2][b % 4], c) for c in range(2)
-            )
-            store(pl.multiple_of(jnp.where(core == 0, row0, row1), 16), source, a, b)
-
-
-def norm_kernel(place_ref, tokens_ref, gain_ref, *refs):
+            i, j = b // 4, b % 4
+            z = jnp.where(second, zs[flip_z][j], zs[flip_z][i])
+            y = jnp.where(second, ys[flip_y][i], ys[flip_y][j])
+            store(pl.multiple_of(height(z, y, core), 16), piece, b)
+
+
+def norm_kernel(place_ref, t0_ref, t1_ref, t2_ref, t3_ref, gain_ref, *refs):
     vectors, (taps_ref, extra_ref), (normed_ref, table_ref, extra_out_ref) = (
         refs[:-5],
         refs[-5:-3],
         refs[-3:],
     )
-    parts = [tokens_ref[j].astype(F32) for j in range(4)]
+    parts = [ref[...].astype(F32) for ref in (t0_ref, t1_ref, t2_ref, t3_ref)]
     total = sum(jnp.sum(part * part, axis=-1, keepdims=True) for part in parts)
     inverse_rms = lax.rsqrt(total * (1.0 / 2048.0) + 1e-06)
     goal = iota((256, 256), 1)
     source = ((goal % 128) // 16) * 32 + (goal // 128) * 16 + goal % 16
     moves = jnp.where(iota((256, 256), 0) == source, 1.0, 0.0).astype(BF16)
-    for j in range(4):
-        normed = (parts[j] * inverse_rms * gain_ref[j : j + 1, :]).astype(BF16)
-        for k in range(2):
+    for k, part in enumerate(parts):
+        j = (place_ref[1] + 4 - k) % 4
+        normed = (part * inverse_rms * gain_ref[pl.ds(j, 1), :]).astype(BF16)
+        for h in range(2):
             moved = jnp.dot(
-                normed[:, k * 256 : k * 256 + 256], moves, preferred_element_type=F32
+                normed[:, h * 256 : h * 256 + 256], moves, preferred_element_type=F32
             ).astype(BF16)
-            z = j * 2 + k
-            normed_ref[0, :, z * 128 : z * 128 + 128] = moved[:, :128]
-            normed_ref[1, :, z * 128 : z * 128 + 128] = moved[:, 128:]
+            normed_ref[0, j * 2 + h] = moved[:, :128]
+            normed_ref[1, j * 2 + h] = moved[:, 128:]
     for k, ref in enumerate(vectors):
         table_ref[k : k + 1, :] = ref[...]
     table_ref[8 : 8 + TAPS, :] = taps_ref[...]
     extra_out_ref[...] = extra_ref[...]
 
 
-def projected(core, source_ref, normed_ref, weights):
-    def store(row, source, a, b):
+def projected(index, core, pieces, normed_ref, weights):
+    def store(row, piece, b):
         for m in range(MATS):
             lanes = slice((m % 2) * 128, (m % 2) * 128 + 128)
-            weights[m // 2, pl.ds(row, 16), lanes] = source[a, b, m * 16 : m * 16 + 16, :]
-
-    fill_rows(core, source_ref, lambda z, y, c: (z * 8 + y) * 16, store)
-    normed = normed_ref[core]
+            weights[m // 2, pl.ds(row, 16), lanes] = piece[b, m * 16 : m * 16 + 16, :]
+
+    fill_rows(index, core, pieces, lambda z, y, c: (z * 8 + y) * 16, store)
+    normed = jnp.concatenate([normed_ref[core, z] for z in range(8)], axis=1)
     return [jnp.dot(normed, weights[p], preferred_element_type=F32) for p in range(MATS // 2)]
 
 
-def half_kernel(place_ref, own_ref, normed_ref, out_ref, weights):
-    products = projected(place_ref[0] % 2, own_ref, normed_ref, weights)
+def half_kernel(place_ref, p0, p1, p2, p3, normed_ref, out_ref, weights):
+    index = place_ref[0]
+    products = projected(index, index % 2, (p0, p1, p2, p3), normed_ref, weights)
     for p in range(MATS // 2):
         out_ref[p] = products[p]
 
 
 def local_kernel(
     core_ref,
-    other_ref,
+    p0,
+    p1,
+    p2,
+    p3,
     normed_ref,
     half_ref,
     table_ref,
@@ -181,7 +219,8 @@
 ):
     core = core_ref[0] % 2
     products = []
-    for p, product in enumerate(projected(1 - core, other_ref, normed_ref, weights)):
+    others = projected(core_ref[0], 1 - core, (p0, p1, p2, p3), normed_ref, weights)
+    for p, product in enumerate(others):
         product = (product + half_ref[p]).astype(BF16).astype(F32)
         products += [product[:, :128], product[:, 128:]]
     recept, keys, values, decay_pre, removal_pre, gate_pre, conv_value, conv_gate = products
@@ -353,17 +392,18 @@
     sums_ref[...] = jnp.where(at == 2, exact(ones, rest, NT), sums)
 
 
-def columns_kernel(core_ref, own_ref, other_ref, out_ref):
-    core = core_ref[0] % 2
-
-    def store(row, source, a, b):
+def columns_kernel(core_ref, *refs):
+    index, out_ref = core_ref[0], refs[-1]
+    core = index % 2
+
+    def store(row, piece, b):
         for m in range(2):
             at = (MATS + m) * 16
-            out_ref[pl.ds(row, 16), m * 128 : m * 128 + 128] = source[a, b, at : at + 16, :]
+            out_ref[pl.ds(row, 16), m * 128 : m * 128 + 128] = piece[b, at : at + 16, :]
 
     height = lambda z, y, c: place(z, y, c) * 16
-    fill_rows(core, own_ref, height, store)
-    fill_rows(1 - core, other_ref, height, store)
+    fill_rows(index, core, refs[:4], height, store)
+    fill_rows(index, 1 - core, refs[4:8], height, store)
 
 
 def final_kernel(
@@ -453,7 +493,7 @@
     out_scan_weight,
     out_conv_weight,
 ):
-    index = lax.axis_index("sp").astype(jnp.int32)[None]
+    index = jnp.stack([lax.axis_index("sp"), lax.axis_index("tp")]).astype(jnp.int32)
     row = lambda v: v.reshape(1, -1)
 
     packed = pack(
@@ -468,15 +508,22 @@
         out_scan_weight.T,
         out_conv_weight.T,
     )
-    stage1 = to_each(packed, FAR)
-    wide = jnp.broadcast_to(stage1[None], (4, *stage1.shape))
-    stage2 = to_each(wide, NEAR)
-    whole = lax.all_gather(tokens, "tp")
+    line = to_each(packed, FAR_FIRST)
+    around = [tokens]
+    for k in range(1, 4):
+        around.append(lax.ppermute(tokens, "tp", [(x, (x + k) % 4) for x in range(4)]))
+    plane = to_each(jnp.broadcast_to(line[None], (4, *line.shape)), FAR_SECOND)
+    pieces = [plane.reshape(16, *plane.shape[2:])]
+    for along_z, along_y in FLIPS[1:]:
+        pieces.append(lax.ppermute(pieces[0], "sp", neighbours(along_z, along_y)))
+    swapped = []
+    for piece in pieces:
+        swapped.append(lax.ppermute(piece, "sp", SWAP))
     normed, table, extra = on_core(
         norm_kernel,
-        (vmem((2, LENGTH, 1024), BF16), vmem((40, 128), F32), vmem((LENGTH, 128), F32)),
+        (vmem((2, 8, LENGTH, 128), BF16), vmem((40, 128), F32), vmem((LENGTH, 128), F32)),
         index,
-        whole,
+        *around,
         given=(
             norm_gain.reshape(4, 512),
             row(key_gain),
@@ -490,12 +537,11 @@
             decay_extra,
         ),
     )
-    swapped = lax.ppermute(stage2, "sp", SWAP)
     half = on_core(
         half_kernel,
         vmem((MATS // 2, LENGTH, 256), F32),
         index,
-        stage2,
+        *pieces,
         normed,
         scratch=[pltpu.VMEM(WEIGHTS, BF16)],
         limit=16,
@@ -511,7 +557,7 @@
             vmem((32, 128), BF16),
         ),
         index,
-        swapped,
+        *swapped,
         normed,
         half,
         table,
@@ -537,7 +583,7 @@
         conv_kernel, (vmem((LENGTH, 128), F32), vmem((8, 128), F32)), index, conv_input, rim, table
     )
     sums = lax.psum(sums, "tp")
-    columns = on_core(columns_kernel, vmem((2048, 256), BF16), index, stage2, swapped)
+    columns = on_core(columns_kernel, vmem((2048, 256), BF16), index, *pieces, *swapped)
 
     terms = on_core(
         final_kernel,

time: 151 us -> 174 us (1.15)
  the two profiles are of different devices: /device:TPU:2 before, /device:TPU:64 now
where the time goes in v5:
time: 174 us; the launch traced here: 173 us
  blocking collectives  82.7 us (48%)
  starting transfers between devices  34.4 us (20%)
  waiting for transfers between devices  29.7 us (17%)
  Pallas kernels  21.3 us (12%)
  local copies, waits for them, and re-layouts  3.41 us (2%)
    all_to_all x4, blocking collectives, to_each(): return lax.all_to_all(x, 'sp', 0, 0, tiled=True, axis_index_groups=groups)  60.3 us
    pallas_call x9, Pallas kernels, on_core(): pl.pallas_call(kernel, in_specs=[pl.BlockSpec(memory_space=pltpu.SMEM)] +...  19.8 us
    ppermute x3, waiting for transfers between devices, layer(): lax.ppermute(tokens, 'tp', [(x, (x + k) % 4) for x in range(4)])  16.1 us
    all_to_all x1, blocking collectives, layer(): parts = lax.all_to_all(terms, 'tp', 0, 0, tiled=True)  11.9 us
    ppermute x3, starting transfers between devices, layer(): lax.ppermute(tokens, 'tp', [(x, (x + k) % 4) for x in range(4)])  10.6 us
    psum x1, blocking collectives, layer(): sums = lax.psum(sums, 'tp')  10.5 us
    ppermute x3, waiting for transfers between devices, layer(): pieces.append(lax.ppermute(pieces[0], 'sp', neighbours(along_z, along_y)))  10 us
    ppermute x3, starting transfers between devices, layer(): pieces.append(lax.ppermute(pieces[0], 'sp', neighbours(along_z, along_y)))  9.33 us
  transfers between devices with their start and end apart: 13, of which 7 were waited for; matrix products, arithmetic and copies ran while one was open for 0% of the time, Pallas kernels for 4%

profile of v5, /device:TPU:64, one launch (start us, length us, event | category | flops | bytes accessed | tf_op | source)
XLA Modules:
  0.0 172.6 jit_solution(2508483320964890259)
XLA Ops:
  1.5 14.1 %all_to_all.25 = bf16[4,160,128]{2,1,0:T(8,128)(2,1)S(1)} all-to-all(bf16[4,160,128]{2,1,0:T(8,128)(2,1)} %pack.1), channel_id=1, replica_groups={{0,16,40,56},{8,24,32,48},{64,80,104,120},{72,88,96,112},{128,144,168,1..., dimensions={0} | all-to-all | bytes 327680 | tf_op jit(solution)/shard_map/all_to_all | solution.py:470
  15.7 22.8 %all_to_all.26 = bf16[4,4,160,128]{3,2,1,0:T(8,128)(2,1)S(1)} all-to-all(bf16[4,4,160,128]{3,2,1,0:T(8,128)(2,1)S(1)} %broadcast_in_dim.2), channel_id=1, replica_groups={{0,128,320,448},{64,192,256,384},{8,136,328,456},{72,200,264,392},{16,1..., dimensions={0} | all-to-all | bytes 1310720 | tf_op jit(solution)/shard_map/all_to_all | solution.py:470
  38.5 3.7 %collective-permute-start.1 = (bf16[16,160,128]{2,1,0:T(8,128)(2,1)S(1)}, bf16[16,160,128]{2,1,0:T(8,128)(2,1)S(1)}, u32[]{:S(2)}, u32[]{:S(2)}) collective-permute-start(bf16[16,160,128]{2,1,0:T(8,128)(2,1)S(1)} %bitcast.12), channel_id=1, source_target_pairs={{0,8},{4,60},{8,0},{12,20},{16,24},{20,12},{24,16},{28,36},{32,40}... | collective-permute-start | bytes 1966088 | tf_op jit(solution)/shard_map/ppermute | solution.py:518
  42.2 2.1 %collective-permute-start.3 = (bf16[16,160,128]{2,1,0:T(8,128)(2,1)S(1)}, bf16[16,160,128]{2,1,0:T(8,128)(2,1)S(1)}, u32[]{:S(2)}, u32[]{:S(2)}) collective-permute-start(bf16[16,160,128]{2,1,0:T(8,128)(2,1)S(1)} %bitcast.13), channel_id=1, source_target_pairs={{0,64},{4,452},{8,72},{12,460},{16,80},{20,468},{24,88},{28,476},{... | collective-permute-start | bytes 1966088 | tf_op jit(solution)/shard_map/ppermute | solution.py:518
  44.3 3.5 %collective-permute-start.5 = (bf16[16,160,128]{2,1,0:T(8,128)(2,1)S(1)}, bf16[16,160,128]{2,1,0:T(8,128)(2,1)S(1)}, u32[]{:S(2)}, u32[]{:S(2)}) collective-permute-start(bf16[16,160,128]{2,1,0:T(8,128)(2,1)S(1)} %bitcast.14), channel_id=1, source_target_pairs={{0,72},{4,508},{8,64},{12,468},{16,88},{20,460},{24,80},{28,484},{... | collective-permute-start | bytes 1966088 | tf_op jit(solution)/shard_map/ppermute | solution.py:518
  47.8 1.9 %collective-permute-start = (bf16[16,160,128]{2,1,0:T(8,128)(2,1)S(1)}, bf16[16,160,128]{2,1,0:T(8,128)(2,1)}, u32[]{:S(2)}, u32[]{:S(2)}) collective-permute-start(bf16[16,160,128]{2,1,0:T(8,128)(2,1)S(1)} %bitcast.15), channel_id=1, source_target_pairs={{0,4},{4,0},{8,12},{12,8},{16,20},{20,16},{24,28},{28,24},{32,36},... | collective-permute-start | bytes 1966088 | tf_op jit(solution)/shard_map/ppermute | solution.py:521
  53.0 8.7 %collective-permute-done.3.p2.refs_2_ = bf16[16,160,128]{2,1,0:T(8,128)(2,1)S(1)} collective-permute-done((bf16[16,160,128]{2,1,0:T(8,128)(2,1)S(1)}, bf16[16,160,128]{2,1,0:T(8,128)(2,1)S(1)}, u32[]{:S(2)}, u32[]{:S(2)}) %collective-permute-start.3) | collective-permute-done | bytes 655392 | tf_op jit(solution)/shard_map/ppermute | solution.py:518
  63.6 2.4 %collective-permute-start.6 = (bf16[16,160,128]{2,1,0:T(8,128)(2,1)S(1)}, bf16[16,160,128]{2,1,0:T(8,128)(2,1)}, u32[]{:S(2)}, u32[]{:S(2)}) collective-permute-start(bf16[16,160,128]{2,1,0:T(8,128)(2,1)S(1)} %collective-permute-done.5.p3.refs_3_), channel_id=1, source_target_pairs={{0,4},{4,0},{8,12},{12,8},{16,20},{20,16},{24,28},{28,24},{32,36},... | collective-permute-start | bytes 1966088 | tf_op jit(solution)/shard_map/ppermute | solution.py:521
  66.1 3.4 %collective-permute-start.7 = (bf16[192,512]{1,0:T(8,128)(2,1)S(1)}, bf16[192,512]{1,0:T(8,128)(2,1)S(1)}, u32[]{:S(2)}, u32[]{:S(2)}) collective-permute-start(bf16[192,512]{1,0:T(8,128)(2,1)S(1)} %copy-done.2), channel_id=1, source_target_pairs={{0,1},{1,2},{2,3},{3,0},{4,5},{5,6},{6,7},{7,4},{8,9},{9,10},{10,1... | collective-permute-start | bytes 589832 | tf_op jit(solution)/shard_map/ppermute | solution.py:514
  69.5 6.5 %collective-permute-done.7.t1_ref = bf16[192,512]{1,0:T(8,128)(2,1)S(1)} collective-permute-done((bf16[192,512]{1,0:T(8,128)(2,1)S(1)}, bf16[192,512]{1,0:T(8,128)(2,1)S(1)}, u32[]{:S(2)}, u32[]{:S(2)}) %collective-permute-start.7) | collective-permute-done | bytes 196640 | tf_op jit(solution)/shard_map/ppermute | solution.py:514
  76.0 3.7 %collective-permute-start.8 = (bf16[192,512]{1,0:T(8,128)(2,1)S(1)}, bf16[192,512]{1,0:T(8,128)(2,1)S(1)}, u32[]{:S(2)}, u32[]{:S(2)}) collective-permute-start(bf16[192,512]{1,0:T(8,128)(2,1)S(1)} %copy-done.2), channel_id=1, source_target_pairs={{0,2},{1,3},{2,0},{3,1},{4,6},{5,7},{6,4},{7,5},{8,10},{9,11},{10,... | collective-permute-start | bytes 589832 | tf_op jit(solution)/shard_map/ppermute | solution.py:514
  79.7 5.6 %collective-permute-done.8.t2_ref = bf16[192,512]{1,0:T(8,128)(2,1)S(1)} collective-permute-done((bf16[192,512]{1,0:T(8,128)(2,1)S(1)}, bf16[192,512]{1,0:T(8,128)(2,1)S(1)}, u32[]{:S(2)}, u32[]{:S(2)}) %collective-permute-start.8) | collective-permute-done | bytes 196640 | tf_op jit(solution)/shard_map/ppermute | solution.py:514
  85.3 3.4 %collective-permute-start.9 = (bf16[192,512]{1,0:T(8,128)(2,1)S(1)}, bf16[192,512]{1,0:T(8,128)(2,1)S(1)}, u32[]{:S(2)}, u32[]{:S(2)}) collective-permute-start(bf16[192,512]{1,0:T(8,128)(2,1)S(1)} %copy-done.2), channel_id=1, source_target_pairs={{0,3},{1,0},{2,1},{3,2},{4,7},{5,4},{6,5},{7,6},{8,11},{9,8},{10,9... | collective-permute-start | bytes 589832 | tf_op jit(solution)/shard_map/ppermute | solution.py:514
  88.9 4.0 %collective-permute-done.9.t3_ref = bf16[192,512]{1,0:T(8,128)(2,1)S(1)} collective-permute-done((bf16[192,512]{1,0:T(8,128)(2,1)S(1)}, bf16[192,512]{1,0:T(8,128)(2,1)S(1)}, u32[]{:S(2)}, u32[]{:S(2)}) %collective-permute-start.9) | collective-permute-done | bytes 196640 | tf_op jit(solution)/shard_map/ppermute | solution.py:514
  98.9 7.9 %shard_map.201 = (f32[64,128]{1,0:T(8,128)S(1)}, f32[64,128]{1,0:T(8,128)S(1)}, f32[2,192,128]{2,1,0:T(8,128)S(1)}, f32[192,128]{1,0:T(8,128)S(1)}, bf16[192,128...) custom-call(s32[2]{0:T(128)S(1)} %pad_add_fusion.place_ref.core_ref, ...), custom_call_target="tpu_custom_call" | custom-call | tf_op jit(solution)/shard_map/pallas_call | solution.py:88
  106.9 2.1 %collective-permute-start.10 = (f32[64,128]{1,0:T(8,128)S(1)}, f32[64,128]{1,0:T(8,128)S(1)}, u32[]{:S(2)}, u32[]{:S(2)}) collective-permute-start(f32[64,128]{1,0:T(8,128)S(1)} %get-tuple-element.25), channel_id=1, source_target_pairs={{0,4},{4,0},{8,12},{12,8},{16,20},{20,16},{24,28},{28,24},{32,36},... | collective-permute-start | bytes 98312 | tf_op jit(solution)/shard_map/ppermute | solution.py:569
  110.8 12.1 %all_to_all.27.steps_ref = bf16[8,64,128]{2,1,0:T(8,128)(2,1)S(1)} all-to-all(bf16[8,64,128]{2,1,0:T(8,128)(2,1)S(1)} %shard_map.202), channel_id=1, replica_groups={{0,8,16,24,32,40,48,56},{4,12,20,28,36,44,52,60},{64,72,80,88,96,104,11..., dimensions={0} | all-to-all | bytes 262144 | tf_op jit(solution)/shard_map/all_to_all | solution.py:470
  124.2 11.4 %all_to_all.28.steps_ref = bf16[8,64,128]{2,1,0:T(8,128)(2,1)S(1)} all-to-all(bf16[8,64,128]{2,1,0:T(8,128)(2,1)S(1)} %get-tuple-element.26), channel_id=1, replica_groups={{0,64,128,192,256,320,384,448},{4,68,132,196,260,324,388,452},{8,72,136..., dimensions={0} | all-to-all | bytes 262144 | tf_op jit(solution)/shard_map/all_to_all | solution.py:470
  135.6 1.9 %shard_map.204 = (f32[64,128]{1,0:T(8,128)S(1)}, f32[64,128]{1,0:T(8,128)}) custom-call(s32[2]{0:T(128)S(1)} %pad_add_fusion.place_ref.core_ref, bf16[8,64,128]{2,1,0:T(8,128)(2,1)S(1)} %all_to_all.28.steps_ref, f32[64,128]{1,0:T(8,128)S(1)} %get-tuple-element.27.before_ref, f32[64,128]{1,0:T(8,128)S(1)} %get-tuple-element.24.mine_ref, ...), custom_call_target="tpu_custom_call" | custom-call | tf_op jit(solution)/shard_map/pallas_call | solution.py:88
  139.4 2.4 %collective-permute-start.12 = (bf16[32,128]{1,0:T(8,128)(2,1)S(1)}, bf16[32,128]{1,0:T(8,128)(2,1)S(1)}, u32[]{:S(2)}, u32[]{:S(2)}) collective-permute-start(bf16[32,128]{1,0:T(8,128)(2,1)S(1)} %get-tuple-element.32), channel_id=1, source_target_pairs={{0,4},{4,8},{8,12},{12,16},{16,20},{20,24},{24,28},{28,32},{32,36}... | collective-permute-start | bytes 24584 | tf_op jit(solution)/shard_map/ppermute | solution.py:570
  141.9 2.3 %shard_map.206.columns_ref = bf16[2048,256]{1,0:T(8,128)(2,1)S(1)} custom-call(s32[2]{0:T(128)S(1)} %pad_add_fusion.place_ref.core_ref, bf16[16,160,128]{2,1,0:T(8,128)(2,1)S(1)} %bitcast.17, bf16[16,160,128]{2,1,0:T(8,128)(2,1)S(1)} %collective-permute-done.1.p1.refs_1_, bf16[16,160,128]{2,1,0:T(8,128)(2,1)S(1)} %collective-permute-done.3.p2.refs_2_, ...), custom_call_target="tpu_custom_call" | custom-call | tf_op jit(solution)/shard_map/pallas_call | solution.py:88
  144.2 2.3 %collective-permute-done.12.rim_ref = bf16[32,128]{1,0:T(8,128)(2,1)S(1)} collective-permute-done((bf16[32,128]{1,0:T(8,128)(2,1)S(1)}, bf16[32,128]{1,0:T(8,128)(2,1)S(1)}, u32[]{:S(2)}, u32[]{:S(2)}) %collective-permute-start.12) | collective-permute-done | bytes 8224 | tf_op jit(solution)/shard_map/ppermute | solution.py:570
  147.8 10.5 %psum.7.sums_ref = f32[8,128]{1,0:T(8,128)S(1)} all-reduce(f32[8,128]{1,0:T(8,128)S(1)} %get-tuple-element.34), channel_id=1, replica_groups=mesh['sp'=128,'tp'=4] {'tp'}, use_global_device_ids=true, to_apply=%region_0.0 | all-reduce | flops 1024 | bytes 8192 | tf_op jit(solution)/shard_map/psum | solution.py:585
  159.9 11.9 %all_to_all.29 = bf16[4,192,512]{2,1,0:T(8,128)(2,1)S(1)} all-to-all(bf16[4,192,512]{2,1,0:T(8,128)(2,1)S(1)} %shard_map.207), channel_id=1, replica_groups=mesh['sp'=128,'tp'=4] {'tp'}, dimensions={0} | all-to-all | bytes 1572864 | tf_op jit(solution)/shard_map/all_to_all | solution.py:601
  (48 shorter events, 21.6 us)
Async XLA Ops:
  15.7 50.4 %copy-start.2 = (bf16[192,512]{1,0:T(8,128)(2,1)S(1)}, bf16[192,512]{1,0:T(8,128)(2,1)}, u32[]{:S(2)}) copy-start(bf16[192,512]{1,0:T(8,128)(2,1)} %t0_ref.1) | copy-start | bytes 589828
  15.7 77.2 %copy-start.3 = (f32[192,128]{1,0:T(8,128)S(1)}, f32[192,128]{1,0:T(8,128)}, u32[]{:S(2)}) copy-start(f32[192,128]{1,0:T(8,128)} %refs_8_.1) | copy-start | bytes 294916
  38.5 50.3 %copy-start.12 = (f32[2048]{0:T(1024)S(1)}, f32[2048]{0:T(1024)}, u32[]{:S(2)}) copy-start(f32[2048]{0:T(1024)} %param.22) | copy-start | bytes 24580
  38.5 12.6 %collective-permute-start.1 = (bf16[16,160,128]{2,1,0:T(8,128)(2,1)S(1)}, bf16[16,160,128]{2,1,0:T(8,128)(2,1)S(1)}, u32[]{:S(2)}, u32[]{:S(2)}) collective-permute-start(bf16[16,160,128]{2,1,0:T(8,128)(2,1)S(1)} %bitcast.12), channel_id=1, source_target_pairs={{0,8},{4,60},{8,0},{12,20},{16,24},{20,12},{24,16},{28,36},{32,40}... | collective-permute-start | bytes 1966088 | tf_op jit(solution)/shard_map/ppermute | solution.py:518
  42.2 19.5 %collective-permute-start.3 = (bf16[16,160,128]{2,1,0:T(8,128)(2,1)S(1)}, bf16[16,160,128]{2,1,0:T(8,128)(2,1)S(1)}, u32[]{:S(2)}, u32[]{:S(2)}) collective-permute-start(bf16[16,160,128]{2,1,0:T(8,128)(2,1)S(1)} %bitcast.13), channel_id=1, source_target_pairs={{0,64},{4,452},{8,72},{12,460},{16,80},{20,468},{24,88},{28,476},{... | collective-permute-start | bytes 1966088 | tf_op jit(solution)/shard_map/ppermute | solution.py:518
  44.3 19.3 %collective-permute-start.5 = (bf16[16,160,128]{2,1,0:T(8,128)(2,1)S(1)}, bf16[16,160,128]{2,1,0:T(8,128)(2,1)S(1)}, u32[]{:S(2)}, u32[]{:S(2)}) collective-permute-start(bf16[16,160,128]{2,1,0:T(8,128)(2,1)S(1)} %bitcast.14), channel_id=1, source_target_pairs={{0,72},{4,508},{8,64},{12,468},{16,88},{20,460},{24,80},{28,484},{... | collective-permute-start | bytes 1966088 | tf_op jit(solution)/shard_map/ppermute | solution.py:518
  47.8 51.1 %collective-permute-start = (bf16[16,160,128]{2,1,0:T(8,128)(2,1)S(1)}, bf16[16,160,128]{2,1,0:T(8,128)(2,1)}, u32[]{:S(2)}, u32[]{:S(2)}) collective-permute-start(bf16[16,160,128]{2,1,0:T(8,128)(2,1)S(1)} %bitcast.15), channel_id=1, source_target_pairs={{0,4},{4,0},{8,12},{12,8},{16,20},{20,16},{24,28},{28,24},{32,36},... | collective-permute-start | bytes 1966088 | tf_op jit(solution)/shard_map/ppermute | solution.py:521
  51.1 47.8 %collective-permute-start.2 = (bf16[16,160,128]{2,1,0:T(8,128)(2,1)S(1)}, bf16[16,160,128]{2,1,0:T(8,128)(2,1)}, u32[]{:S(2)}, u32[]{:S(2)}) collective-permute-start(bf16[16,160,128]{2,1,0:T(8,128)(2,1)S(1)} %collective-permute-done.1.p1.refs_1_), channel_id=1, source_target_pairs={{0,4},{4,0},{8,12},{12,8},{16,20},{20,16},{24,28},{28,24},{32,36},... | collective-permute-start | bytes 1966088 | tf_op jit(solution)/shard_map/ppermute | solution.py:521
  61.7 37.2 %collective-permute-start.4 = (bf16[16,160,128]{2,1,0:T(8,128)(2,1)S(1)}, bf16[16,160,128]{2,1,0:T(8,128)(2,1)}, u32[]{:S(2)}, u32[]{:S(2)}) collective-permute-start(bf16[16,160,128]{2,1,0:T(8,128)(2,1)S(1)} %collective-permute-done.3.p2.refs_2_), channel_id=1, source_target_pairs={{0,4},{4,0},{8,12},{12,8},{16,20},{20,16},{24,28},{28,24},{32,36},... | collective-permute-start | bytes 1966088 | tf_op jit(solution)/shard_map/ppermute | solution.py:521
  63.6 35.3 %copy-start = (bf16[16,160,128]{2,1,0:T(8,128)(2,1)}, bf16[16,160,128]{2,1,0:T(8,128)(2,1)S(1)}, u32[]{:S(2)}) copy-start(bf16[16,160,128]{2,1,0:T(8,128)(2,1)S(1)} %collective-permute-done.5.p3.refs_3_) | copy-start | bytes 1966084
  63.6 35.3 %collective-permute-start.6 = (bf16[16,160,128]{2,1,0:T(8,128)(2,1)S(1)}, bf16[16,160,128]{2,1,0:T(8,128)(2,1)}, u32[]{:S(2)}, u32[]{:S(2)}) collective-permute-start(bf16[16,160,128]{2,1,0:T(8,128)(2,1)S(1)} %collective-permute-done.5.p3.refs_3_), channel_id=1, source_target_pairs={{0,4},{4,0},{8,12},{12,8},{16,20},{20,16},{24,28},{28,24},{32,36},... | collective-permute-start | bytes 1966088 | tf_op jit(solution)/shard_map/ppermute | solution.py:521
  66.1 9.9 %collective-permute-start.7 = (bf16[192,512]{1,0:T(8,128)(2,1)S(1)}, bf16[192,512]{1,0:T(8,128)(2,1)S(1)}, u32[]{:S(2)}, u32[]{:S(2)}) collective-permute-start(bf16[192,512]{1,0:T(8,128)(2,1)S(1)} %copy-done.2), channel_id=1, source_target_pairs={{0,1},{1,2},{2,3},{3,0},{4,5},{5,6},{6,7},{7,4},{8,9},{9,10},{10,1... | collective-permute-start | bytes 589832 | tf_op jit(solution)/shard_map/ppermute | solution.py:514
  76.0 9.3 %collective-permute-start.8 = (bf16[192,512]{1,0:T(8,128)(2,1)S(1)}, bf16[192,512]{1,0:T(8,128)(2,1)S(1)}, u32[]{:S(2)}, u32[]{:S(2)}) collective-permute-start(bf16[192,512]{1,0:T(8,128)(2,1)S(1)} %copy-done.2), channel_id=1, source_target_pairs={{0,2},{1,3},{2,0},{3,1},{4,6},{5,7},{6,4},{7,5},{8,10},{9,11},{10,... | collective-permute-start | bytes 589832 | tf_op jit(solution)/shard_map/ppermute | solution.py:514
  85.3 7.6 %collective-permute-start.9 = (bf16[192,512]{1,0:T(8,128)(2,1)S(1)}, bf16[192,512]{1,0:T(8,128)(2,1)S(1)}, u32[]{:S(2)}, u32[]{:S(2)}) collective-permute-start(bf16[192,512]{1,0:T(8,128)(2,1)S(1)} %copy-done.2), channel_id=1, source_target_pairs={{0,3},{1,0},{2,1},{3,2},{4,7},{5,4},{6,5},{7,6},{8,11},{9,8},{10,9... | collective-permute-start | bytes 589832 | tf_op jit(solution)/shard_map/ppermute | solution.py:514
  88.8 4.1 %copy-start.4 = (f32[31,128]{1,0:T(8,128)S(1)}, f32[31,128]{1,0:T(8,128)}, u32[]{:S(2)}) copy-start(f32[31,128]{1,0:T(8,128)} %refs_7_.3) | copy-start | bytes 47620
  92.9 0.7 copy-start.5
  92.9 0.7 copy-start.6
  92.9 0.7 copy-start.7
  93.6 0.7 copy-start.8
  94.9 0.7 copy-start.10
  106.9 35.0 %copy-start.1 = (bf16[16,160,128]{2,1,0:T(8,128)(2,1)S(1)}, bf16[16,160,128]{2,1,0:T(8,128)(2,1)}, u32[]{:S(2)}) copy-start(bf16[16,160,128]{2,1,0:T(8,128)(2,1)} %copy-done) | copy-start | bytes 1966084
  106.9 3.2 %collective-permute-start.10 = (f32[64,128]{1,0:T(8,128)S(1)}, f32[64,128]{1,0:T(8,128)S(1)}, u32[]{:S(2)}, u32[]{:S(2)}) collective-permute-start(f32[64,128]{1,0:T(8,128)S(1)} %get-tuple-element.25), channel_id=1, source_target_pairs={{0,4},{4,0},{8,12},{12,8},{16,20},{20,16},{24,28},{28,24},{32,36},... | collective-permute-start | bytes 98312 | tf_op jit(solution)/shard_map/ppermute | solution.py:569
  137.5 20.8 %collective-permute-start.11 = (f32[64,128]{1,0:T(8,128)}, f32[64,128]{1,0:T(8,128)S(1)}, u32[]{:S(2)}, u32[]{:S(2)}) collective-permute-start(f32[64,128]{1,0:T(8,128)} %get-tuple-element.29), channel_id=1, source_target_pairs={{0,4},{4,0},{8,12},{12,8},{16,20},{20,16},{24,28},{28,24},{32,36},... | collective-permute-start | bytes 98312 | tf_op jit(solution)/shard_map/ppermute | solution.py:580
  139.4 7.1 %collective-permute-start.12 = (bf16[32,128]{1,0:T(8,128)(2,1)S(1)}, bf16[32,128]{1,0:T(8,128)(2,1)S(1)}, u32[]{:S(2)}, u32[]{:S(2)}) collective-permute-start(bf16[32,128]{1,0:T(8,128)(2,1)S(1)} %get-tuple-element.32), channel_id=1, source_target_pairs={{0,4},{4,8},{8,12},{12,16},{16,20},{20,24},{24,28},{28,32},{32,36}... | collective-permute-start | bytes 24584 | tf_op jit(solution)/shard_map/ppermute | solution.py:570
  (2 other events, 1.3 us)

commit v6 on v4

--- a/solution.py
+++ b/solution.py
@@ -26,12 +26,10 @@
 
 
 SETS = (((0, 2, 5, 7), (1, 3, 4, 6)), ((1, 3, 6, 0), (2, 4, 5, 7)))
-FAR = [
-    [place(z, y, c) for z in SETS[c][p] for y in SETS[c][q]]
-    for c in range(2)
-    for p in range(2)
-    for q in range(2)
-]
+FAR_Y = [[[place(z, y, c) for y in ys] for z in range(8) for ys in SETS[c]] for c in range(2)]
+FAR_Z = [[[place(z, y, c) for z in zs] for y in range(8) for zs in SETS[c]] for c in range(2)]
+FAR_FIRST = FAR_Y[0] + FAR_Z[1]
+FAR_SECOND = FAR_Z[0] + FAR_Y[1]
 
 
 def near(k, p, c):
@@ -99,14 +97,14 @@
     out = refs[-1]
     blocks = [ref[...] for ref in refs[:-1]]
     both = jnp.concatenate(blocks, axis=0)
-    for k in range(16):
+    for k in range(4):
         out[k] = both
 
 
 def pack(*mats):
     return pl.pallas_call(
         pack_kernel,
-        out_shape=jax.ShapeDtypeStruct((16, 16 * len(mats), 128), BF16),
+        out_shape=jax.ShapeDtypeStruct((4, 16 * len(mats), 128), BF16),
         name="pack",
     )(*mats)
 
@@ -114,18 +112,21 @@
 def fill_rows(core, source, height, store):
     for a in range(4):
         for b in range(16):
-            row0, row1 = (
-                height(SETS[c][a // 2][b // 4], SETS[c][a % 2][b % 4], c) for c in range(2)
-            )
+            i, j = b // 4, b % 4
+            row0 = height(SETS[0][a // 2][i], SETS[0][a % 2][j], 0)
+            row1 = height(SETS[1][a // 2][j], SETS[1][a % 2][i], 1)
             store(pl.multiple_of(jnp.where(core == 0, row0, row1), 16), source, a, b)
 
 
-def norm_kernel(place_ref, tokens_ref, gain_ref, *refs):
-    vectors, (taps_ref, extra_ref), (normed_ref, table_ref, extra_out_ref) = (
-        refs[:-5],
-        refs[-5:-3],
-        refs[-3:],
-    )
+def table_kernel(place_ref, *refs):
+    vectors, taps_ref, extra_ref, table_ref, extra_out_ref = refs[:-4], *refs[-4:]
+    for k, ref in enumerate(vectors):
+        table_ref[k : k + 1, :] = ref[...]
+    table_ref[8 : 8 + TAPS, :] = taps_ref[...]
+    extra_out_ref[...] = extra_ref[...]
+
+
+def norm_kernel(place_ref, tokens_ref, gain_ref, normed_ref):
     parts = [tokens_ref[j].astype(F32) for j in range(4)]
     total = sum(jnp.sum(part * part, axis=-1, keepdims=True) for part in parts)
     inverse_rms = lax.rsqrt(total * (1.0 / 2048.0) + 1e-06)
@@ -141,10 +142,6 @@
             z = j * 2 + k
             normed_ref[0, :, z * 128 : z * 128 + 128] = moved[:, :128]
             normed_ref[1, :, z * 128 : z * 128 + 128] = moved[:, 128:]
-    for k, ref in enumerate(vectors):
-        table_ref[k : k + 1, :] = ref[...]
-    table_ref[8 : 8 + TAPS, :] = taps_ref[...]
-    extra_out_ref[...] = extra_ref[...]
 
 
 def projected(core, source_ref, normed_ref, weights):
@@ -158,7 +155,8 @@
     return [jnp.dot(normed, weights[p], preferred_element_type=F32) for p in range(MATS // 2)]
 
 
-def half_kernel(place_ref, own_ref, normed_ref, out_ref, weights):
+def half_kernel(place_ref, own_ref, normed_ref, out_ref, rest_ref, weights):
+    rest_ref[...] = own_ref[:, :, MATS * 16 :, :]
     products = projected(place_ref[0] % 2, own_ref, normed_ref, weights)
     for p in range(MATS // 2):
         out_ref[p] = products[p]
@@ -177,9 +175,11 @@
     gate_ref,
     conv_ref,
     rim_ref,
+    rest_ref,
     weights,
 ):
     core = core_ref[0] % 2
+    rest_ref[...] = other_ref[:, :, MATS * 16 :, :]
     products = []
     for p, product in enumerate(projected(1 - core, other_ref, normed_ref, weights)):
         product = (product + half_ref[p]).astype(BF16).astype(F32)
@@ -353,17 +353,18 @@
     sums_ref[...] = jnp.where(at == 2, exact(ones, rest, NT), sums)
 
 
-def columns_kernel(core_ref, own_ref, other_ref, out_ref):
-    core = core_ref[0] % 2
-
+def fill_columns(core, own_ref, other_ref, columns):
     def store(row, source, a, b):
         for m in range(2):
-            at = (MATS + m) * 16
-            out_ref[pl.ds(row, 16), m * 128 : m * 128 + 128] = source[a, b, at : at + 16, :]
+            columns[pl.ds(row, 16), m * 128 : m * 128 + 128] = source[a, b, m * 16 : m * 16 + 16, :]
 
     height = lambda z, y, c: place(z, y, c) * 16
     fill_rows(core, own_ref, height, store)
     fill_rows(1 - core, other_ref, height, store)
+
+
+def product(features, columns):
+    return lax.dot_general(features, columns, NT, preferred_element_type=F32)
 
 
 def final_kernel(
@@ -374,9 +375,13 @@
     gate_ref,
     filtered_ref,
     sums_ref,
-    columns_ref,
+    own_ref,
+    other_ref,
     table_ref,
     out_ref,
+    features_ref,
+    kept_ref,
+    columns,
 ):
     core = core_ref[0] % 2
     mine, theirs = mine_ref[...], theirs_ref[...]
@@ -420,10 +425,22 @@
     )
     conv_out = (scaled * jax.nn.sigmoid(scaled)).astype(BF16)
     features = jnp.concatenate([scan_out, conv_out], axis=1)
+    features_ref[...] = features
+    fill_columns(core, own_ref, other_ref, columns)
     for j in range(4):
-        out_ref[j] = lax.dot_general(
-            features, columns_ref[j * 512 : j * 512 + 512, :], NT, preferred_element_type=F32
-        ).astype(BF16)
+        out_ref[j] = product(features, columns[j * 512 : j * 512 + 512, :]).astype(BF16)
+    kept_ref[...] = columns[pl.ds(pl.multiple_of(core_ref[1] * 512, 512), 512), :]
+
+
+def stay_kernel(place_ref, features_ref, columns_ref, out_ref):
+    out_ref[...] = product(features_ref[...], columns_ref[...])
+
+
+def add_kernel(place_ref, parts_ref, stay_ref, out_ref):
+    total = stay_ref[...]
+    for j in range(4):
+        total = total + jnp.where(place_ref[1] == j, 0.0, parts_ref[j].astype(F32))
+    out_ref[...] = total.astype(BF16)
 
 
 def to_each(x, groups):
@@ -453,7 +470,7 @@
     out_scan_weight,
     out_conv_weight,
 ):
-    index = lax.axis_index("sp").astype(jnp.int32)[None]
+    index = jnp.stack([lax.axis_index("sp"), lax.axis_index("tp")]).astype(jnp.int32)
     row = lambda v: v.reshape(1, -1)
 
     packed = pack(
@@ -468,17 +485,14 @@
         out_scan_weight.T,
         out_conv_weight.T,
     )
-    stage1 = to_each(packed, FAR)
-    wide = jnp.broadcast_to(stage1[None], (4, *stage1.shape))
-    stage2 = to_each(wide, NEAR)
-    whole = lax.all_gather(tokens, "tp")
-    normed, table, extra = on_core(
-        norm_kernel,
-        (vmem((2, LENGTH, 1024), BF16), vmem((40, 128), F32), vmem((LENGTH, 128), F32)),
+    line = to_each(packed, FAR_FIRST)
+    wide = jnp.broadcast_to(line[None], (4, *line.shape))
+    plane = to_each(wide, FAR_SECOND)
+    table, extra = on_core(
+        table_kernel,
+        (vmem((40, 128), F32), vmem((LENGTH, 128), F32)),
         index,
-        whole,
         given=(
-            norm_gain.reshape(4, 512),
             row(key_gain),
             row(removal_gain),
             row(removal_bias),
@@ -490,17 +504,23 @@
             decay_extra,
         ),
     )
+    wide = jnp.broadcast_to(plane[None], (4, *plane.shape))
+    stage2 = to_each(wide, NEAR).reshape(4, 16, *plane.shape[2:])
+    whole = lax.all_gather(tokens, "tp")
+    normed = on_core(
+        norm_kernel, vmem((2, LENGTH, 1024), BF16), index, whole, given=(norm_gain.reshape(4, 512),)
+    )
     swapped = lax.ppermute(stage2, "sp", SWAP)
-    half = on_core(
+    half, rest = on_core(
         half_kernel,
-        vmem((MATS // 2, LENGTH, 256), F32),
+        (vmem((MATS // 2, LENGTH, 256), F32), vmem((4, 16, 32, 128), BF16)),
         index,
         stage2,
         normed,
         scratch=[pltpu.VMEM(WEIGHTS, BF16)],
         limit=16,
     )
-    mine, theirs, reads, gate, conv_input, rim = on_core(
+    mine, theirs, reads, gate, conv_input, rim, other_rest = on_core(
         local_kernel,
         (
             vmem((HEAD, 128), F32),
@@ -509,6 +529,7 @@
             vmem((LENGTH, 128), F32),
             vmem((LENGTH, 128), BF16),
             vmem((32, 128), BF16),
+            vmem((4, 16, 32, 128), BF16),
         ),
         index,
         swapped,
@@ -537,11 +558,10 @@
         conv_kernel, (vmem((LENGTH, 128), F32), vmem((8, 128), F32)), index, conv_input, rim, table
     )
     sums = lax.psum(sums, "tp")
-    columns = on_core(columns_kernel, vmem((2048, 256), BF16), index, stage2, swapped)
-
-    terms = on_core(
+
+    terms, features, kept = on_core(
         final_kernel,
-        vmem((4, LENGTH, 512), BF16),
+        (vmem((4, LENGTH, 512), BF16), vmem((LENGTH, 256), BF16), vmem((512, 256), BF16)),
         index,
         reads,
         own_state,
@@ -549,11 +569,15 @@
         gate,
         filtered,
         sums,
-        columns,
+        rest,
+        other_rest,
         table,
+        scratch=[pltpu.VMEM((2048, 256), BF16)],
+        limit=12,
     )
     parts = lax.all_to_all(terms, "tp", 0, 0, tiled=True)
-    return jnp.sum(parts.astype(F32), axis=0).astype(BF16)
+    stay = on_core(stay_kernel, vmem((LENGTH, 512), F32), index, features, kept)
+    return on_core(add_kernel, jax.ShapeDtypeStruct((LENGTH, 512), BF16), index, parts, stay)
 
 
 def solution(mesh):

time: 151 us -> 157 us (1.040)
  the two profiles are of different devices: /device:TPU:2 before, /device:TPU:64 now
where the time goes in v6:
time: 157 us; the launch traced here: 156 us
  blocking collectives  107 us (68%)
  Pallas kernels  22.3 us (14%)
  waiting for transfers between devices  14.5 us (9%)
  starting transfers between devices  11.7 us (7%)
    all_to_all x5, blocking collectives, to_each(): return lax.all_to_all(x, 'sp', 0, 0, tiled=True, axis_index_groups=groups)  81.7 us
    pallas_call x11, Pallas kernels, on_core(): pl.pallas_call(kernel, in_specs=[pl.BlockSpec(memory_space=pltpu.SMEM)] +...  20.8 us
    all_gather x1, blocking collectives, layer(): whole = lax.all_gather(tokens, 'tp')  14.2 us
    psum x1, blocking collectives, layer(): sums = lax.psum(sums, 'tp')  10.7 us
    all_to_all x1, waiting for transfers between devices, layer(): parts = lax.all_to_all(terms, 'tp', 0, 0, tiled=True)  8.67 us
    ppermute x1, waiting for transfers between devices, layer(): rim = lax.ppermute(rim, 'sp', ONWARD)  4.67 us
    all_to_all x1, starting transfers between devices, layer(): parts = lax.all_to_all(terms, 'tp', 0, 0, tiled=True)  3.49 us
  transfers between devices with their start and end apart: 5, of which 3 were waited for; matrix products, arithmetic and copies ran while one was open for 0% of the time, Pallas kernels for 3%

profile of v6, /device:TPU:64, one launch (start us, length us, event | category | flops | bytes accessed | tf_op | source)
XLA Modules:
  0.0 156.2 jit_solution(14528915617526184251)
XLA Ops:
  0.0 1.5 pack.1
  1.5 14.1 %all_to_all.30 = bf16[4,160,128]{2,1,0:T(8,128)(2,1)S(1)} all-to-all(bf16[4,160,128]{2,1,0:T(8,128)(2,1)} %pack.1), channel_id=1, replica_groups={{0,16,40,56},{8,24,32,48},{64,80,104,120},{72,88,96,112},{128,144,168,1..., dimensions={0} | all-to-all | bytes 327680 | tf_op jit(solution)/shard_map/all_to_all | solution.py:447
  15.7 22.6 %all_to_all.31 = bf16[4,4,160,128]{3,2,1,0:T(8,128)(2,1)S(1)} all-to-all(bf16[4,4,160,128]{3,2,1,0:T(8,128)(2,1)S(1)} %broadcast_in_dim.4), channel_id=1, replica_groups={{0,128,320,448},{64,192,256,384},{8,136,328,456},{72,200,264,392},{16,1..., dimensions={0} | all-to-all | bytes 1310720 | tf_op jit(solution)/shard_map/all_to_all | solution.py:447
  38.9 21.6 %all_to_all.32 = bf16[4,4,4,160,128]{4,3,2,1,0:T(8,128)(2,1)S(1)} all-to-all(bf16[4,4,4,160,128]{4,3,2,1,0:T(8,128)(2,1)S(1)} %broadcast_in_dim.5), channel_id=1, replica_groups={{0,8,64,72},{16,24,80,88},{40,32,104,96},{56,48,120,112},{128,136,192,2..., dimensions={0} | all-to-all | bytes 5242880 | tf_op jit(solution)/shard_map/all_to_all | solution.py:447
  60.6 1.9 %collective-permute-start = (bf16[4,16,160,128]{3,2,1,0:T(8,128)(2,1)S(1)}, bf16[4,16,160,128]{3,2,1,0:T(8,128)(2,1)}, u32[]{:S(2)}, u32[]{:S(2)}) collective-permute-start(bf16[4,16,160,128]{3,2,1,0:T(8,128)(2,1)S(1)} %bitcast.13), channel_id=1, source_target_pairs={{0,4},{4,0},{8,12},{12,8},{16,20},{20,16},{24,28},{28,24},{32,36},... | collective-permute-start | bytes 7864328 | tf_op jit(solution)/shard_map/ppermute | solution.py:513
  62.6 14.2 %all-gather = bf16[768,512]{1,0:T(8,128)(2,1)S(1)} all-gather(bf16[192,512]{1,0:T(8,128)(2,1)S(1)} %copy-done.9), channel_id=2, replica_groups=mesh['sp'=128,'tp'=4] {'tp'}, dimensions={0}, use_global_device_ids=true | all-gather | bytes 983040 | tf_op jit(solution)/shard_map/all_gather | solution.py:509
  76.8 1.1 shard_map.199.normed_ref
  78.6 1.6 %shard_map.200 = (f32[4,192,256]{2,1,0:T(8,128)S(1)}, bf16[4,16,32,128]{3,2,1,0:T(8,128)(2,1)S(1)}) custom-call(s32[2]{0:T(128)S(1)} %pad_add_fusion.place_ref.core_ref, bf16[4,16,160,128]{3,2,1,0:T(8,128)(2,1)S(1)} %bitcast.14, bf16[2,192,1024]{2,1,0:T(8,128)(2,1)S(1)} %shard_map.199.normed_ref), custom_call_target="tpu_custom_call" | custom-call | tf_op jit(solution)/shard_map/pallas_call | solution.py:86
  80.2 8.1 %shard_map.202 = (f32[64,128]{1,0:T(8,128)S(1)}, f32[64,128]{1,0:T(8,128)S(1)}, f32[2,192,128]{2,1,0:T(8,128)S(1)}, f32[192,128]{1,0:T(8,128)S(1)}, bf16[192,128...) custom-call(s32[2]{0:T(128)S(1)} %pad_add_fusion.place_ref.core_ref, ...), custom_call_target="tpu_custom_call" | custom-call | tf_op jit(solution)/shard_map/pallas_call | solution.py:86
  88.3 1.9 %collective-permute-start.1 = (f32[64,128]{1,0:T(8,128)S(1)}, f32[64,128]{1,0:T(8,128)S(1)}, u32[]{:S(2)}, u32[]{:S(2)}) collective-permute-start(f32[64,128]{1,0:T(8,128)S(1)} %get-tuple-element.30), channel_id=1, source_target_pairs={{0,4},{4,0},{8,12},{12,8},{16,20},{20,16},{24,28},{28,24},{32,36},... | collective-permute-start | bytes 98312 | tf_op jit(solution)/shard_map/ppermute | solution.py:544
  90.2 1.2 collective-permute-done.1.theirs_ref
  92.1 12.1 %all_to_all.33.steps_ref = bf16[8,64,128]{2,1,0:T(8,128)(2,1)S(1)} all-to-all(bf16[8,64,128]{2,1,0:T(8,128)(2,1)S(1)} %shard_map.203), channel_id=1, replica_groups={{0,8,16,24,32,40,48,56},{4,12,20,28,36,44,52,60},{64,72,80,88,96,104,11..., dimensions={0} | all-to-all | bytes 262144 | tf_op jit(solution)/shard_map/all_to_all | solution.py:447
  104.1 1.3 shard_map.204
  105.5 11.4 %all_to_all.34.steps_ref = bf16[8,64,128]{2,1,0:T(8,128)(2,1)S(1)} all-to-all(bf16[8,64,128]{2,1,0:T(8,128)(2,1)S(1)} %get-tuple-element.31), channel_id=1, replica_groups={{0,64,128,192,256,320,384,448},{4,68,132,196,260,324,388,452},{8,72,136..., dimensions={0} | all-to-all | bytes 262144 | tf_op jit(solution)/shard_map/all_to_all | solution.py:447
  116.9 1.3 shard_map.205
  118.2 1.9 %collective-permute-start.2 = (f32[64,128]{1,0:T(8,128)S(1)}, f32[64,128]{1,0:T(8,128)S(1)}, u32[]{:S(2)}, u32[]{:S(2)}) collective-permute-start(f32[64,128]{1,0:T(8,128)S(1)} %get-tuple-element.34), channel_id=1, source_target_pairs={{0,4},{4,0},{8,12},{12,8},{16,20},{20,16},{24,28},{28,24},{32,36},... | collective-permute-start | bytes 98312 | tf_op jit(solution)/shard_map/ppermute | solution.py:555
  120.1 2.4 %collective-permute-start.3 = (bf16[32,128]{1,0:T(8,128)(2,1)S(1)}, bf16[32,128]{1,0:T(8,128)(2,1)S(1)}, u32[]{:S(2)}, u32[]{:S(2)}) collective-permute-start(bf16[32,128]{1,0:T(8,128)(2,1)S(1)} %get-tuple-element.37), channel_id=1, source_target_pairs={{0,4},{4,8},{8,12},{12,16},{16,20},{20,24},{24,28},{28,32},{32,36}... | collective-permute-start | bytes 24584 | tf_op jit(solution)/shard_map/ppermute | solution.py:545
  122.5 4.7 %collective-permute-done.3.rim_ref = bf16[32,128]{1,0:T(8,128)(2,1)S(1)} collective-permute-done((bf16[32,128]{1,0:T(8,128)(2,1)S(1)}, bf16[32,128]{1,0:T(8,128)(2,1)S(1)}, u32[]{:S(2)}, u32[]{:S(2)}) %collective-permute-start.3) | collective-permute-done | bytes 8224 | tf_op jit(solution)/shard_map/ppermute | solution.py:545
  127.2 1.3 shard_map.206
  128.5 10.7 %psum.7.sums_ref = f32[8,128]{1,0:T(8,128)S(1)} all-reduce(f32[8,128]{1,0:T(8,128)S(1)} %get-tuple-element.39), channel_id=1, replica_groups=mesh['sp'=128,'tp'=4] {'tp'}, use_global_device_ids=true, to_apply=%region_0.0 | all-reduce | flops 1024 | bytes 8192 | tf_op jit(solution)/shard_map/psum | solution.py:560
  139.2 2.6 %shard_map.207 = (bf16[4,192,512]{2,1,0:T(8,128)(2,1)}, bf16[192,256]{1,0:T(8,128)(2,1)S(1)}, bf16[512,256]{1,0:T(8,128)(2,1)S(1)}) custom-call(s32[2]{0:T(128)S(1)} %pad_add_fusion.place_ref.core_ref, f32[2,192,128]{2,1,0:T(8,128)S(1)} %get-tuple-element.28.reads_ref, f32[64,128]{1,0:T(8,128)S(1)} %get-tuple-element.33.mine_ref, ...), custom_call_target="tpu_custom_call" | custom-call | tf_op jit(solution)/shard_map/pallas_call | solution.py:86
  141.8 3.5 %all-to-all-start.5 = ((bf16[4,192,512]{2,1,0:T(8,128)(2,1)}), bf16[4,192,512]{2,1,0:T(8,128)(2,1)S(1)}, u32[]{:S(2)}, u32[]{:S(2)}) async-start(bf16[4,192,512]{2,1,0:T(8,128)(2,1)} %get-tuple-element.42), calls=%async_computation.5 | async-start | bytes 1572864 | tf_op jit(solution)/shard_map/all_to_all | solution.py:578
  146.1 8.7 %all-to-all-done.5.parts_ref = bf16[4,192,512]{2,1,0:T(8,128)(2,1)S(1)} async-done(((bf16[4,192,512]{2,1,0:T(8,128)(2,1)}), bf16[4,192,512]{2,1,0:T(8,128)(2,1)S(1)}, u32[]{:S(2)}, u32[]{:S(2)}) %all-to-all-start.5) | async-done | bytes 786464 | tf_op jit(solution)/shard_map/all_to_all | solution.py:578
  154.8 1.4 shard_map.209
  (31 shorter events, 2.8 us)
Async XLA Ops:
  38.8 23.7 %copy-start.10 = (f32[2048]{0:T(1024)S(1)}, f32[2048]{0:T(1024)}, u32[]{:S(2)}) copy-start(f32[2048]{0:T(1024)} %param.22) | copy-start | bytes 24580
  38.8 23.8 %copy-start.9 = (bf16[192,512]{1,0:T(8,128)(2,1)S(1)}, bf16[192,512]{1,0:T(8,128)(2,1)}, u32[]{:S(2)}) copy-start(bf16[192,512]{1,0:T(8,128)(2,1)} %param.21) | copy-start | bytes 589828
  38.8 39.1 %copy-start = (f32[192,128]{1,0:T(8,128)S(1)}, f32[192,128]{1,0:T(8,128)}, u32[]{:S(2)}) copy-start(f32[192,128]{1,0:T(8,128)} %refs_8_.1) | copy-start | bytes 294916
  38.9 39.1 %copy-start.1 = (f32[31,128]{1,0:T(8,128)S(1)}, f32[31,128]{1,0:T(8,128)}, u32[]{:S(2)}) copy-start(f32[31,128]{1,0:T(8,128)} %refs_7_.3) | copy-start | bytes 47620
  38.9 39.1 %copy-start.2 = (f32[128]{0:T(128)S(1)}, f32[128]{0:T(128)}, u32[]{:S(2)}) copy-start(f32[128]{0:T(128)} %param.29) | copy-start | bytes 1540
  38.9 39.1 %copy-start.3 = (f32[128]{0:T(128)S(1)}, f32[128]{0:T(128)}, u32[]{:S(2)}) copy-start(f32[128]{0:T(128)} %param.30) | copy-start | bytes 1540
  38.9 39.1 %copy-start.4 = (f32[128]{0:T(128)S(1)}, f32[128]{0:T(128)}, u32[]{:S(2)}) copy-start(f32[128]{0:T(128)} %param.31) | copy-start | bytes 1540
  38.9 39.1 %copy-start.5 = (f32[128]{0:T(128)S(1)}, f32[128]{0:T(128)}, u32[]{:S(2)}) copy-start(f32[128]{0:T(128)} %param.32) | copy-start | bytes 1540
  38.9 39.1 %copy-start.6 = (f32[128]{0:T(128)S(1)}, f32[128]{0:T(128)}, u32[]{:S(2)}) copy-start(f32[128]{0:T(128)} %param.34) | copy-start | bytes 1540
  38.9 39.1 %copy-start.7 = (f32[128]{0:T(128)S(1)}, f32[128]{0:T(128)}, u32[]{:S(2)}) copy-start(f32[128]{0:T(128)} %param.38) | copy-start | bytes 1540
  38.9 39.1 %copy-start.8 = (f32[128]{0:T(128)S(1)}, f32[128]{0:T(128)}, u32[]{:S(2)}) copy-start(f32[128]{0:T(128)} %param.39) | copy-start | bytes 1540
  60.6 19.6 %collective-permute-start = (bf16[4,16,160,128]{3,2,1,0:T(8,128)(2,1)S(1)}, bf16[4,16,160,128]{3,2,1,0:T(8,128)(2,1)}, u32[]{:S(2)}, u32[]{:S(2)}) collective-permute-start(bf16[4,16,160,128]{3,2,1,0:T(8,128)(2,1)S(1)} %bitcast.13), channel_id=1, source_target_pairs={{0,4},{4,0},{8,12},{12,8},{16,20},{20,16},{24,28},{28,24},{32,36},... | collective-permute-start | bytes 7864328 | tf_op jit(solution)/shard_map/ppermute | solution.py:513
  88.3 3.1 %collective-permute-start.1 = (f32[64,128]{1,0:T(8,128)S(1)}, f32[64,128]{1,0:T(8,128)S(1)}, u32[]{:S(2)}, u32[]{:S(2)}) collective-permute-start(f32[64,128]{1,0:T(8,128)S(1)} %get-tuple-element.30), channel_id=1, source_target_pairs={{0,4},{4,0},{8,12},{12,8},{16,20},{20,16},{24,28},{28,24},{32,36},... | collective-permute-start | bytes 98312 | tf_op jit(solution)/shard_map/ppermute | solution.py:544
  118.2 21.0 %collective-permute-start.2 = (f32[64,128]{1,0:T(8,128)S(1)}, f32[64,128]{1,0:T(8,128)S(1)}, u32[]{:S(2)}, u32[]{:S(2)}) collective-permute-start(f32[64,128]{1,0:T(8,128)S(1)} %get-tuple-element.34), channel_id=1, source_target_pairs={{0,4},{4,0},{8,12},{12,8},{16,20},{20,16},{24,28},{28,24},{32,36},... | collective-permute-start | bytes 98312 | tf_op jit(solution)/shard_map/ppermute | solution.py:555
  120.1 7.1 %collective-permute-start.3 = (bf16[32,128]{1,0:T(8,128)(2,1)S(1)}, bf16[32,128]{1,0:T(8,128)(2,1)S(1)}, u32[]{:S(2)}, u32[]{:S(2)}) collective-permute-start(bf16[32,128]{1,0:T(8,128)(2,1)S(1)} %get-tuple-element.37), channel_id=1, source_target_pairs={{0,4},{4,8},{8,12},{12,16},{16,20},{20,24},{24,28},{28,32},{32,36}... | collective-permute-start | bytes 24584 | tf_op jit(solution)/shard_map/ppermute | solution.py:545
  141.8 13.0 %all-to-all-start.5 = ((bf16[4,192,512]{2,1,0:T(8,128)(2,1)}), bf16[4,192,512]{2,1,0:T(8,128)(2,1)S(1)}, u32[]{:S(2)}, u32[]{:S(2)}) async-start(bf16[4,192,512]{2,1,0:T(8,128)(2,1)} %get-tuple-element.42), calls=%async_computation.5 | async-start | bytes 1572864 | tf_op jit(solution)/shard_map/all_to_all | solution.py:578

commit v7 on v5

--- a/solution.py
+++ b/solution.py
@@ -26,10 +26,12 @@
 
 
 SETS = (((0, 2, 5, 7), (1, 3, 4, 6)), ((1, 3, 6, 0), (2, 4, 5, 7)))
-FAR_Y = [[[place(z, y, c) for y in ys] for z in range(8) for ys in SETS[c]] for c in range(2)]
-FAR_Z = [[[place(z, y, c) for z in zs] for y in range(8) for zs in SETS[c]] for c in range(2)]
-FAR_FIRST = FAR_Y[0] + FAR_Z[1]
-FAR_SECOND = FAR_Z[0] + FAR_Y[1]
+FAR = [
+    [place(z, y, c) for z in SETS[c][p] for y in SETS[c][q]]
+    for c in range(2)
+    for p in range(2)
+    for q in range(2)
+]
 
 
 def partner(v, c):
@@ -99,14 +101,14 @@
     out = refs[-1]
     blocks = [ref[...] for ref in refs[:-1]]
     both = jnp.concatenate(blocks, axis=0)
-    for k in range(4):
+    for k in range(16):
         out[k] = both
 
 
 def pack(*mats):
     return pl.pallas_call(
         pack_kernel,
-        out_shape=jax.ShapeDtypeStruct((4, 16 * len(mats), 128), BF16),
+        out_shape=jax.ShapeDtypeStruct((16, 16 * len(mats), 128), BF16),
         name="pack",
     )(*mats)
 
@@ -148,37 +150,34 @@
     zs, ys = axis(index // 16), axis((index // 2) % 8)
     for piece, (flip_z, flip_y) in zip(pieces, FLIPS):
         for b in range(16):
-            i, j = b // 4, b % 4
-            z = jnp.where(second, zs[flip_z][j], zs[flip_z][i])
-            y = jnp.where(second, ys[flip_y][i], ys[flip_y][j])
-            store(pl.multiple_of(height(z, y, core), 16), piece, b)
-
-
-def norm_kernel(place_ref, t0_ref, t1_ref, t2_ref, t3_ref, gain_ref, *refs):
-    vectors, (taps_ref, extra_ref), (normed_ref, table_ref, extra_out_ref) = (
-        refs[:-5],
-        refs[-5:-3],
-        refs[-3:],
-    )
-    parts = [ref[...].astype(F32) for ref in (t0_ref, t1_ref, t2_ref, t3_ref)]
+            row = height(zs[flip_z][b // 4], ys[flip_y][b % 4], core)
+            store(pl.multiple_of(row, 16), piece, b)
+
+
+def table_kernel(place_ref, *refs):
+    vectors, taps_ref, extra_ref, table_ref, extra_out_ref = refs[:-4], *refs[-4:]
+    for k, ref in enumerate(vectors):
+        table_ref[k : k + 1, :] = ref[...]
+    table_ref[8 : 8 + TAPS, :] = taps_ref[...]
+    extra_out_ref[...] = extra_ref[...]
+
+
+def norm_kernel(place_ref, tokens_ref, gain_ref, normed_ref):
+    parts = [tokens_ref[j].astype(F32) for j in range(4)]
     total = sum(jnp.sum(part * part, axis=-1, keepdims=True) for part in parts)
     inverse_rms = lax.rsqrt(total * (1.0 / 2048.0) + 1e-06)
     goal = iota((256, 256), 1)
     source = ((goal % 128) // 16) * 32 + (goal // 128) * 16 + goal % 16
     moves = jnp.where(iota((256, 256), 0) == source, 1.0, 0.0).astype(BF16)
-    for k, part in enumerate(parts):
-        j = (place_ref[1] + 4 - k) % 4
-        normed = (part * inverse_rms * gain_ref[pl.ds(j, 1), :]).astype(BF16)
+    for j, part in enumerate(parts):
+        normed = (part * inverse_rms * gain_ref[j : j + 1, :]).astype(BF16)
         for h in range(2):
             moved = jnp.dot(
                 normed[:, h * 256 : h * 256 + 256], moves, preferred_element_type=F32
             ).astype(BF16)
-            normed_ref[0, j * 2 + h] = moved[:, :128]
-            normed_ref[1, j * 2 + h] = moved[:, 128:]
-    for k, ref in enumerate(vectors):
-        table_ref[k : k + 1, :] = ref[...]
-    table_ref[8 : 8 + TAPS, :] = taps_ref[...]
-    extra_out_ref[...] = extra_ref[...]
+            z = j * 2 + h
+            normed_ref[0, :, z * 128 : z * 128 + 128] = moved[:, :128]
+            normed_ref[1, :, z * 128 : z * 128 + 128] = moved[:, 128:]
 
 
 def projected(index, core, pieces, normed_ref, weights):
@@ -188,7 +187,7 @@
             weights[m // 2, pl.ds(row, 16), lanes] = piece[b, m * 16 : m * 16 + 16, :]
 
     fill_rows(index, core, pieces, lambda z, y, c: (z * 8 + y) * 16, store)
-    normed = jnp.concatenate([normed_ref[core, z] for z in range(8)], axis=1)
+    normed = normed_ref[core % 2]
     return [jnp.dot(normed, weights[p], preferred_element_type=F32) for p in range(MATS // 2)]
 
 
@@ -493,7 +492,7 @@
     out_scan_weight,
     out_conv_weight,
 ):
-    index = jnp.stack([lax.axis_index("sp"), lax.axis_index("tp")]).astype(jnp.int32)
+    index = lax.axis_index("sp").astype(jnp.int32)[None]
     row = lambda v: v.reshape(1, -1)
 
     packed = pack(
@@ -508,24 +507,13 @@
         out_scan_weight.T,
         out_conv_weight.T,
     )
-    line = to_each(packed, FAR_FIRST)
-    around = [tokens]
-    for k in range(1, 4):
-        around.append(lax.ppermute(tokens, "tp", [(x, (x + k) % 4) for x in range(4)]))
-    plane = to_each(jnp.broadcast_to(line[None], (4, *line.shape)), FAR_SECOND)
-    pieces = [plane.reshape(16, *plane.shape[2:])]
-    for along_z, along_y in FLIPS[1:]:
-        pieces.append(lax.ppermute(pieces[0], "sp", neighbours(along_z, along_y)))
-    swapped = []
-    for piece in pieces:
-        swapped.append(lax.ppermute(piece, "sp", SWAP))
-    normed, table, extra = on_core(
-        norm_kernel,
-        (vmem((2, 8, LENGTH, 128), BF16), vmem((40, 128), F32), vmem((LENGTH, 128), F32)),
+    plane = to_each(packed, FAR)
+    whole = lax.all_gather(tokens, "tp")
+    table, extra = on_core(
+        table_kernel,
+        (vmem((40, 128), F32), vmem((LENGTH, 128), F32)),
         index,
-        *around,
         given=(
-            norm_gain.reshape(4, 512),
             row(key_gain),
             row(removal_gain),
             row(removal_bias),
@@ -537,6 +525,15 @@
             decay_extra,
         ),
     )
+    normed = on_core(
+        norm_kernel, vmem((2, LENGTH, 1024), BF16), index, whole, given=(norm_gain.reshape(4, 512),)
+    )
+    pieces = [plane]
+    for along_z, along_y in FLIPS[1:]:
+        pieces.append(lax.ppermute(pieces[0], "sp", neighbours(along_z, along_y)))
+    swapped = []
+    for piece in pieces:
+        swapped.append(lax.ppermute(piece, "sp", SWAP))
     half = on_core(
         half_kernel,
         vmem((MATS // 2, LENGTH, 256), F32),

time: 174 us -> 152 us (0.87)
  waiting for transfers between devices: 29.7 us -> 12.6 us
  blocking collectives: 82.7 us -> 96.4 us
  starting transfers between devices: 34.4 us -> 23.7 us
  Pallas kernels: 21.3 us -> 16.7 us
  local copies, waits for them, and re-layouts: 3.41 us -> 0.7 us
    ppermute x3 -> x0, waiting for transfers between devices: 16.1 us -> none  [layer(): lax.ppermute(tokens, 'tp', [(x, (x + k) % 4) for x in range(4)])]
    all_gather x0 -> x1, blocking collectives: none -> 13.8 us  [layer(): whole = lax.all_gather(tokens, 'tp')]
    ppermute x3 -> x0, starting transfers between devices: 10.6 us -> none  [layer(): lax.ppermute(tokens, 'tp', [(x, (x + k) % 4) for x in range(4)])]
    pallas_call x9 -> x10, Pallas kernels: 19.8 us -> 14.9 us  [on_core(): pl.pallas_call(kernel, in_specs=[pl.BlockSpec(memory_space=pltpu.SMEM)] +...]
    unnamed x26, local copies, waits for them, and re-layouts: 3.32 us -> 0.69 us
    all_to_all x4 -> x3, blocking collectives: 60.3 us -> 60 us  [to_each(): return lax.all_to_all(x, 'sp', 0, 0, tiled=True, axis_index_groups=groups)]
  transfers between devices with their start and end apart: 13 -> 10, of which waited for: 7 -> 4; matrix products, arithmetic and copies ran while one was open for 0% -> 0% of each run, Pallas kernels for 4% -> 3%
where the time goes in v7:
time: 152 us; the launch traced here: 151 us
  blocking collectives  96.4 us (63%)
  starting transfers between devices  23.7 us (16%)
  Pallas kernels  16.7 us (11%)
  waiting for transfers between devices  12.6 us (8%)
    all_to_all x3, blocking collectives, to_each(): return lax.all_to_all(x, 'sp', 0, 0, tiled=True, axis_index_groups=groups)  60 us
    pallas_call x10, Pallas kernels, on_core(): pl.pallas_call(kernel, in_specs=[pl.BlockSpec(memory_space=pltpu.SMEM)] +...  14.9 us
    all_gather x1, blocking collectives, layer(): whole = lax.all_gather(tokens, 'tp')  13.8 us
    all_to_all x1, blocking collectives, layer(): parts = lax.all_to_all(terms, 'tp', 0, 0, tiled=True)  11.9 us
    psum x1, blocking collectives, layer(): sums = lax.psum(sums, 'tp')  10.8 us
    ppermute x3, starting transfers between devices, layer(): pieces.append(lax.ppermute(pieces[0], 'sp', neighbours(along_z, along_y)))  9.2 us
    ppermute x3, waiting for transfers between devices, layer(): pieces.append(lax.ppermute(pieces[0], 'sp', neighbours(along_z, along_y)))  8.67 us
    ppermute x4, starting transfers between devices, layer(): swapped.append(lax.ppermute(piece, 'sp', SWAP))  8.15 us
  transfers between devices with their start and end apart: 10, of which 4 were waited for; matrix products, arithmetic and copies ran while one was open for 0% of the time, Pallas kernels for 3%

profile of v7, /device:TPU:64, one launch (start us, length us, event | category | flops | bytes accessed | tf_op | source)
XLA Modules:
  0.0 151.2 jit_solution(14154741949588302992)
XLA Ops:
  0.0 1.8 %pack.1 = bf16[16,160,128]{2,1,0:T(8,128)(2,1)} custom-call(bf16[16,128]{1,0:T(8,128)(2,1)} %refs_0_.1, bf16[16,128]{1,0:T(8,128)(2,1)} %refs_1_.1, bf16[16,128]{1,0:T(8,128)(2,1)} %refs_2_.1, bf16[16,128]{1,0:T(8,128)(2,1)} %refs_3_.1, bf16[16,128]{1,0:T(8,128)(2,1)} %refs_4_.1, bf16[16,128]{1,0:T(8,128)(2,1)} %refs_5_.1, bf16[16,128]{1,0:T(8,128)(2,1)} %refs_6_.1, ...), custom_call_target="tpu_custom_call" | custom-call | tf_op jit(solution)/shard_map/pack/pallas_call | solution.py:109
  1.8 35.5 %all_to_all.20.p0.refs_0_ = bf16[16,160,128]{2,1,0:T(8,128)(2,1)S(1)} all-to-all(bf16[16,160,128]{2,1,0:T(8,128)(2,1)} %pack.1), channel_id=1, replica_groups={{0,16,40,56,128,144,168,184,320,336,360,376,448,464,488,504},{8,24,32,4..., dimensions={0} | all-to-all | bytes 1310720 | tf_op jit(solution)/shard_map/all_to_all | solution.py:469
  37.3 2.2 %collective-permute-start.1 = (bf16[16,160,128]{2,1,0:T(8,128)(2,1)S(1)}, bf16[16,160,128]{2,1,0:T(8,128)(2,1)S(1)}, u32[]{:S(2)}, u32[]{:S(2)}) collective-permute-start(bf16[16,160,128]{2,1,0:T(8,128)(2,1)S(1)} %all_to_all.20.p0.refs_0_), channel_id=1, source_target_pairs={{0,8},{4,60},{8,0},{12,20},{16,24},{20,12},{24,16},{28,36},{32,40}... | collective-permute-start | bytes 1966088 | tf_op jit(solution)/shard_map/ppermute | solution.py:533
  39.5 2.7 %collective-permute-start.3 = (bf16[16,160,128]{2,1,0:T(8,128)(2,1)S(1)}, bf16[16,160,128]{2,1,0:T(8,128)(2,1)S(1)}, u32[]{:S(2)}, u32[]{:S(2)}) collective-permute-start(bf16[16,160,128]{2,1,0:T(8,128)(2,1)S(1)} %all_to_all.20.p0.refs_0_), channel_id=1, source_target_pairs={{0,64},{4,452},{8,72},{12,460},{16,80},{20,468},{24,88},{28,476},{... | collective-permute-start | bytes 1966088 | tf_op jit(solution)/shard_map/ppermute | solution.py:533
  42.2 4.3 %collective-permute-start.5 = (bf16[16,160,128]{2,1,0:T(8,128)(2,1)S(1)}, bf16[16,160,128]{2,1,0:T(8,128)(2,1)S(1)}, u32[]{:S(2)}, u32[]{:S(2)}) collective-permute-start(bf16[16,160,128]{2,1,0:T(8,128)(2,1)S(1)} %all_to_all.20.p0.refs_0_), channel_id=1, source_target_pairs={{0,72},{4,508},{8,64},{12,468},{16,88},{20,460},{24,80},{28,484},{... | collective-permute-start | bytes 1966088 | tf_op jit(solution)/shard_map/ppermute | solution.py:533
  46.5 1.9 %collective-permute-start = (bf16[16,160,128]{2,1,0:T(8,128)(2,1)S(1)}, bf16[16,160,128]{2,1,0:T(8,128)(2,1)}, u32[]{:S(2)}, u32[]{:S(2)}) collective-permute-start(bf16[16,160,128]{2,1,0:T(8,128)(2,1)S(1)} %all_to_all.20.p0.refs_0_), channel_id=1, source_target_pairs={{0,4},{4,0},{8,12},{12,8},{16,20},{20,16},{24,28},{28,24},{32,36},... | collective-permute-start | bytes 1966088 | tf_op jit(solution)/shard_map/ppermute | solution.py:536
  48.4 1.3 collective-permute-done.1.p1.refs_1_
  49.7 1.9 %collective-permute-start.2 = (bf16[16,160,128]{2,1,0:T(8,128)(2,1)S(1)}, bf16[16,160,128]{2,1,0:T(8,128)(2,1)}, u32[]{:S(2)}, u32[]{:S(2)}) collective-permute-start(bf16[16,160,128]{2,1,0:T(8,128)(2,1)S(1)} %collective-permute-done.1.p1.refs_1_), channel_id=1, source_target_pairs={{0,4},{4,0},{8,12},{12,8},{16,20},{20,16},{24,28},{28,24},{32,36},... | collective-permute-start | bytes 1966088 | tf_op jit(solution)/shard_map/ppermute | solution.py:536
  51.6 7.4 %collective-permute-done.3.p2.refs_2_ = bf16[16,160,128]{2,1,0:T(8,128)(2,1)S(1)} collective-permute-done((bf16[16,160,128]{2,1,0:T(8,128)(2,1)S(1)}, bf16[16,160,128]{2,1,0:T(8,128)(2,1)S(1)}, u32[]{:S(2)}, u32[]{:S(2)}) %collective-permute-start.3) | collective-permute-done | bytes 655392 | tf_op jit(solution)/shard_map/ppermute | solution.py:533
  59.0 1.9 %collective-permute-start.4 = (bf16[16,160,128]{2,1,0:T(8,128)(2,1)S(1)}, bf16[16,160,128]{2,1,0:T(8,128)(2,1)}, u32[]{:S(2)}, u32[]{:S(2)}) collective-permute-start(bf16[16,160,128]{2,1,0:T(8,128)(2,1)S(1)} %collective-permute-done.3.p2.refs_2_), channel_id=1, source_target_pairs={{0,4},{4,0},{8,12},{12,8},{16,20},{20,16},{24,28},{28,24},{32,36},... | collective-permute-start | bytes 1966088 | tf_op jit(solution)/shard_map/ppermute | solution.py:536
  60.9 2.4 %collective-permute-start.6 = (bf16[16,160,128]{2,1,0:T(8,128)(2,1)S(1)}, bf16[16,160,128]{2,1,0:T(8,128)(2,1)}, u32[]{:S(2)}, u32[]{:S(2)}) collective-permute-start(bf16[16,160,128]{2,1,0:T(8,128)(2,1)S(1)} %collective-permute-done.5.p3.refs_3_), channel_id=1, source_target_pairs={{0,4},{4,0},{8,12},{12,8},{16,20},{20,16},{24,28},{28,24},{32,36},... | collective-permute-start | bytes 1966088 | tf_op jit(solution)/shard_map/ppermute | solution.py:536
  63.4 13.8 %all-gather = bf16[768,512]{1,0:T(8,128)(2,1)S(1)} all-gather(bf16[192,512]{1,0:T(8,128)(2,1)S(1)} %copy-done.11), channel_id=2, replica_groups=mesh['sp'=128,'tp'=4] {'tp'}, dimensions={0}, use_global_device_ids=true | all-gather | bytes 983040 | tf_op jit(solution)/shard_map/all_gather | solution.py:511
  79.6 7.9 %shard_map.202 = (f32[64,128]{1,0:T(8,128)S(1)}, f32[64,128]{1,0:T(8,128)S(1)}, f32[2,192,128]{2,1,0:T(8,128)S(1)}, f32[192,128]{1,0:T(8,128)S(1)}, bf16[192,128...) custom-call(s32[1]{0:T(128)} %bitcast.place_ref.core_ref, bf16[16,160,128]{2,1,0:T(8,128)(2,1)} %collective-permute-done.p0.refs_4_, ...), custom_call_target="tpu_custom_call" | custom-call | tf_op jit(solution)/shard_map/pallas_call | solution.py:90
  87.5 2.1 %collective-permute-start.7 = (f32[64,128]{1,0:T(8,128)S(1)}, f32[64,128]{1,0:T(8,128)S(1)}, u32[]{:S(2)}, u32[]{:S(2)}) collective-permute-start(f32[64,128]{1,0:T(8,128)S(1)} %get-tuple-element.23), channel_id=1, source_target_pairs={{0,4},{4,0},{8,12},{12,8},{16,20},{20,16},{24,28},{28,24},{32,36},... | collective-permute-start | bytes 98312 | tf_op jit(solution)/shard_map/ppermute | solution.py:566
  89.5 1.2 collective-permute-done.7.theirs_ref
  90.8 12.6 %all_to_all.21.steps_ref = bf16[8,64,128]{2,1,0:T(8,128)(2,1)S(1)} all-to-all(bf16[8,64,128]{2,1,0:T(8,128)(2,1)S(1)} %shard_map.203), channel_id=1, replica_groups={{0,8,16,24,32,40,48,56},{4,12,20,28,36,44,52,60},{64,72,80,88,96,104,11..., dimensions={0} | all-to-all | bytes 262144 | tf_op jit(solution)/shard_map/all_to_all | solution.py:469
  104.3 11.9 %all_to_all.22.steps_ref = bf16[8,64,128]{2,1,0:T(8,128)(2,1)S(1)} all-to-all(bf16[8,64,128]{2,1,0:T(8,128)(2,1)S(1)} %get-tuple-element.24), channel_id=1, replica_groups={{0,64,128,192,256,320,384,448},{4,68,132,196,260,324,388,452},{8,72,136..., dimensions={0} | all-to-all | bytes 262144 | tf_op jit(solution)/shard_map/all_to_all | solution.py:469
  116.9 1.9 %collective-permute-start.8 = (f32[64,128]{1,0:T(8,128)S(1)}, f32[64,128]{1,0:T(8,128)S(1)}, u32[]{:S(2)}, u32[]{:S(2)}) collective-permute-start(f32[64,128]{1,0:T(8,128)S(1)} %get-tuple-element.27), channel_id=1, source_target_pairs={{0,4},{4,0},{8,12},{12,8},{16,20},{20,16},{24,28},{28,24},{32,36},... | collective-permute-start | bytes 98312 | tf_op jit(solution)/shard_map/ppermute | solution.py:577
  118.9 2.4 %collective-permute-start.9 = (bf16[32,128]{1,0:T(8,128)(2,1)S(1)}, bf16[32,128]{1,0:T(8,128)(2,1)S(1)}, u32[]{:S(2)}, u32[]{:S(2)}) collective-permute-start(bf16[32,128]{1,0:T(8,128)(2,1)S(1)} %get-tuple-element.30), channel_id=1, source_target_pairs={{0,4},{4,8},{8,12},{12,16},{16,20},{20,24},{24,28},{28,32},{32,36}... | collective-permute-start | bytes 24584 | tf_op jit(solution)/shard_map/ppermute | solution.py:567
  121.3 1.9 %shard_map.207.columns_ref = bf16[2048,256]{1,0:T(8,128)(2,1)S(1)} custom-call(s32[1]{0:T(128)} %bitcast.place_ref.core_ref, bf16[16,160,128]{2,1,0:T(8,128)(2,1)S(1)} %all_to_all.20.p0.refs_0_, bf16[16,160,128]{2,1,0:T(8,128)(2,1)S(1)} %collective-permute-done.1.p1.refs_1_, bf16[16,160,128]{2,1,0:T(8,128)(2,1)S(1)} %collective-permute-done.3.p2.refs_2_, ...), custom_call_target="tpu_custom_call" | custom-call | tf_op jit(solution)/shard_map/pallas_call | solution.py:90
  123.2 2.8 %collective-permute-done.9.rim_ref = bf16[32,128]{1,0:T(8,128)(2,1)S(1)} collective-permute-done((bf16[32,128]{1,0:T(8,128)(2,1)S(1)}, bf16[32,128]{1,0:T(8,128)(2,1)S(1)}, u32[]{:S(2)}, u32[]{:S(2)}) %collective-permute-start.9) | collective-permute-done | bytes 8224 | tf_op jit(solution)/shard_map/ppermute | solution.py:567
  126.7 10.8 %psum.7.sums_ref = f32[8,128]{1,0:T(8,128)S(1)} all-reduce(f32[8,128]{1,0:T(8,128)S(1)} %get-tuple-element.32), channel_id=1, replica_groups=mesh['sp'=128,'tp'=4] {'tp'}, use_global_device_ids=true, to_apply=%region_0.0 | all-reduce | flops 1024 | bytes 8192 | tf_op jit(solution)/shard_map/psum | solution.py:582
  137.4 1.1 shard_map.208
  138.5 11.9 %all_to_all.23 = bf16[4,192,512]{2,1,0:T(8,128)(2,1)S(1)} all-to-all(bf16[4,192,512]{2,1,0:T(8,128)(2,1)S(1)} %shard_map.208), channel_id=1, replica_groups=mesh['sp'=128,'tp'=4] {'tp'}, dimensions={0} | all-to-all | bytes 1572864 | tf_op jit(solution)/shard_map/all_to_all | solution.py:598
  (41 shorter events, 5.6 us)
Async XLA Ops:
  1.8 61.6 %copy-start.12 = (f32[2048]{0:T(1024)S(1)}, f32[2048]{0:T(1024)}, u32[]{:S(2)}) copy-start(f32[2048]{0:T(1024)} %param.22) | copy-start | bytes 24580
  1.8 61.6 %copy-start.11 = (bf16[192,512]{1,0:T(8,128)(2,1)S(1)}, bf16[192,512]{1,0:T(8,128)(2,1)}, u32[]{:S(2)}) copy-start(bf16[192,512]{1,0:T(8,128)(2,1)} %param.21) | copy-start | bytes 589828
  37.3 12.5 %collective-permute-start.1 = (bf16[16,160,128]{2,1,0:T(8,128)(2,1)S(1)}, bf16[16,160,128]{2,1,0:T(8,128)(2,1)S(1)}, u32[]{:S(2)}, u32[]{:S(2)}) collective-permute-start(bf16[16,160,128]{2,1,0:T(8,128)(2,1)S(1)} %all_to_all.20.p0.refs_0_), channel_id=1, source_target_pairs={{0,8},{4,60},{8,0},{12,20},{16,24},{20,12},{24,16},{28,36},{32,40}... | collective-permute-start | bytes 1966088 | tf_op jit(solution)/shard_map/ppermute | solution.py:533
  39.5 19.5 %collective-permute-start.3 = (bf16[16,160,128]{2,1,0:T(8,128)(2,1)S(1)}, bf16[16,160,128]{2,1,0:T(8,128)(2,1)S(1)}, u32[]{:S(2)}, u32[]{:S(2)}) collective-permute-start(bf16[16,160,128]{2,1,0:T(8,128)(2,1)S(1)} %all_to_all.20.p0.refs_0_), channel_id=1, source_target_pairs={{0,64},{4,452},{8,72},{12,460},{16,80},{20,468},{24,88},{28,476},{... | collective-permute-start | bytes 1966088 | tf_op jit(solution)/shard_map/ppermute | solution.py:533
  42.2 18.7 %collective-permute-start.5 = (bf16[16,160,128]{2,1,0:T(8,128)(2,1)S(1)}, bf16[16,160,128]{2,1,0:T(8,128)(2,1)S(1)}, u32[]{:S(2)}, u32[]{:S(2)}) collective-permute-start(bf16[16,160,128]{2,1,0:T(8,128)(2,1)S(1)} %all_to_all.20.p0.refs_0_), channel_id=1, source_target_pairs={{0,72},{4,508},{8,64},{12,468},{16,88},{20,460},{24,80},{28,484},{... | collective-permute-start | bytes 1966088 | tf_op jit(solution)/shard_map/ppermute | solution.py:533
  46.5 33.0 %collective-permute-start = (bf16[16,160,128]{2,1,0:T(8,128)(2,1)S(1)}, bf16[16,160,128]{2,1,0:T(8,128)(2,1)}, u32[]{:S(2)}, u32[]{:S(2)}) collective-permute-start(bf16[16,160,128]{2,1,0:T(8,128)(2,1)S(1)} %all_to_all.20.p0.refs_0_), channel_id=1, source_target_pairs={{0,4},{4,0},{8,12},{12,8},{16,20},{20,16},{24,28},{28,24},{32,36},... | collective-permute-start | bytes 1966088 | tf_op jit(solution)/shard_map/ppermute | solution.py:536
  49.7 29.8 %collective-permute-start.2 = (bf16[16,160,128]{2,1,0:T(8,128)(2,1)S(1)}, bf16[16,160,128]{2,1,0:T(8,128)(2,1)}, u32[]{:S(2)}, u32[]{:S(2)}) collective-permute-start(bf16[16,160,128]{2,1,0:T(8,128)(2,1)S(1)} %collective-permute-done.1.p1.refs_1_), channel_id=1, source_target_pairs={{0,4},{4,0},{8,12},{12,8},{16,20},{20,16},{24,28},{28,24},{32,36},... | collective-permute-start | bytes 1966088 | tf_op jit(solution)/shard_map/ppermute | solution.py:536
  59.0 20.5 %collective-permute-start.4 = (bf16[16,160,128]{2,1,0:T(8,128)(2,1)S(1)}, bf16[16,160,128]{2,1,0:T(8,128)(2,1)}, u32[]{:S(2)}, u32[]{:S(2)}) collective-permute-start(bf16[16,160,128]{2,1,0:T(8,128)(2,1)S(1)} %collective-permute-done.3.p2.refs_2_), channel_id=1, source_target_pairs={{0,4},{4,0},{8,12},{12,8},{16,20},{20,16},{24,28},{28,24},{32,36},... | collective-permute-start | bytes 1966088 | tf_op jit(solution)/shard_map/ppermute | solution.py:536
  60.9 17.5 %copy-start = (bf16[16,160,128]{2,1,0:T(8,128)(2,1)}, bf16[16,160,128]{2,1,0:T(8,128)(2,1)S(1)}, u32[]{:S(2)}) copy-start(bf16[16,160,128]{2,1,0:T(8,128)(2,1)S(1)} %collective-permute-done.5.p3.refs_3_) | copy-start | bytes 1966084
  60.9 18.6 %collective-permute-start.6 = (bf16[16,160,128]{2,1,0:T(8,128)(2,1)S(1)}, bf16[16,160,128]{2,1,0:T(8,128)(2,1)}, u32[]{:S(2)}, u32[]{:S(2)}) collective-permute-start(bf16[16,160,128]{2,1,0:T(8,128)(2,1)S(1)} %collective-permute-done.5.p3.refs_3_), channel_id=1, source_target_pairs={{0,4},{4,0},{8,12},{12,8},{16,20},{20,16},{24,28},{28,24},{32,36},... | collective-permute-start | bytes 1966088 | tf_op jit(solution)/shard_map/ppermute | solution.py:536
  77.2 0.9 copy-start.2
  77.2 0.9 copy-start.3
  77.2 0.9 copy-start.7
  77.2 0.9 copy-start.8
  77.2 0.9 copy-start.9
  77.2 0.9 copy-start.10
  77.8 0.7 copy-start.4
  77.8 0.7 copy-start.5
  77.8 0.7 copy-start.6
  87.5 33.8 %copy-start.1 = (bf16[16,160,128]{2,1,0:T(8,128)(2,1)S(1)}, bf16[16,160,128]{2,1,0:T(8,128)(2,1)}, u32[]{:S(2)}) copy-start(bf16[16,160,128]{2,1,0:T(8,128)(2,1)} %copy-done) | copy-start | bytes 1966084
  87.5 3.2 %collective-permute-start.7 = (f32[64,128]{1,0:T(8,128)S(1)}, f32[64,128]{1,0:T(8,128)S(1)}, u32[]{:S(2)}, u32[]{:S(2)}) collective-permute-start(f32[64,128]{1,0:T(8,128)S(1)} %get-tuple-element.23), channel_id=1, source_target_pairs={{0,4},{4,0},{8,12},{12,8},{16,20},{20,16},{24,28},{28,24},{32,36},... | collective-permute-start | bytes 98312 | tf_op jit(solution)/shard_map/ppermute | solution.py:566
  116.9 20.5 %collective-permute-start.8 = (f32[64,128]{1,0:T(8,128)S(1)}, f32[64,128]{1,0:T(8,128)S(1)}, u32[]{:S(2)}, u32[]{:S(2)}) collective-permute-start(f32[64,128]{1,0:T(8,128)S(1)} %get-tuple-element.27), channel_id=1, source_target_pairs={{0,4},{4,0},{8,12},{12,8},{16,20},{20,16},{24,28},{28,24},{32,36},... | collective-permute-start | bytes 98312 | tf_op jit(solution)/shard_map/ppermute | solution.py:577
  118.9 7.1 %collective-permute-start.9 = (bf16[32,128]{1,0:T(8,128)(2,1)S(1)}, bf16[32,128]{1,0:T(8,128)(2,1)S(1)}, u32[]{:S(2)}, u32[]{:S(2)}) collective-permute-start(bf16[32,128]{1,0:T(8,128)(2,1)S(1)} %get-tuple-element.30), channel_id=1, source_target_pairs={{0,4},{4,8},{8,12},{12,16},{16,20},{20,24},{24,28},{28,32},{32,36}... | collective-permute-start | bytes 24584 | tf_op jit(solution)/shard_map/ppermute | solution.py:567

commit v8 on v7

--- a/solution.py
+++ b/solution.py
@@ -210,10 +210,12 @@
     extra_ref,
     mine_ref,
     theirs_ref,
-    reads_ref,
     gate_ref,
     conv_ref,
     rim_ref,
+    tables_ref,
+    solved_ref,
+    steps_ref,
     weights,
 ):
     core = core_ref[0] % 2
@@ -246,9 +248,6 @@
     same = (row // BLOCK) == (column // BLOCK)
     strict = same & (row > column)
     inclusive = same & (row >= column)
-    wide_row, wide_column = iota((LENGTH, 2 * LENGTH), 0), iota((LENGTH, 2 * LENGTH), 1)
-    wide_column = jnp.where(wide_column >= LENGTH, wide_column - LENGTH, wide_column)
-    inclusive_twice = ((wide_row // BLOCK) == (wide_column // BLOCK)) & (wide_row >= wide_column)
     falling = -sums_of(jnp.where(inclusive, 1.0, 0.0).astype(BF16), rate)
     before = falling + rate
     by_block = falling.reshape(BLOCKS, BLOCK, 128)
@@ -259,30 +258,28 @@
     beta = unit * removal
     rising = jnp.exp(middle - falling)
     alpha_mid = -unit * jnp.exp(before - middle)
-    recept_mid = recept * jnp.exp(falling - middle)
+    tables_ref[0] = recept * jnp.exp(falling - middle)
     right = jnp.concatenate([beta * rising, written * rising], axis=0)
     start_alpha = -unit * jnp.exp(before)
-    start_recept = recept * jnp.exp(falling)
+    tables_ref[1] = recept * jnp.exp(falling)
     closing = jnp.exp(ending - falling)
     end_beta = beta * closing
     end_keys = written * closing
     kept = jnp.exp(by_block[:, BLOCK - 1, :])
     turned_values = pltpu.roll(values, HEAD, 1)
+    tables_ref[2] = right[:LENGTH]
+    tables_ref[3] = right[LENGTH:]
+    tables_ref[4] = turned_values
 
     square_row, square_lane = iota((128, 128), 0), iota((128, 128), 1)
     diagonal = square_row == square_lane
     own = [first, jnp.logical_not(first)]
     own_row = [square_row < HEAD, square_row >= HEAD]
-    power, solved, query, value_rows = [], [], [], []
-    recept_pairs = []
+    power, solved, value_rows = [], [], []
     for h in range(2):
-        left = jnp.concatenate(
-            [jnp.where(own[h], alpha_mid, 0.0), jnp.where(own[h], recept_mid, 0.0)], axis=0
-        )
-        pairs = dot3(left, right, NT)
-        power.append(jnp.where(strict, pairs[:LENGTH, :LENGTH], 0.0))
-        alpha_keys = jnp.where(strict, pairs[:LENGTH, LENGTH:], 0.0)
-        recept_pairs.append(jnp.where(inclusive_twice, pairs[LENGTH:], 0.0))
+        pairs = dot3(jnp.where(own[h], alpha_mid, 0.0), right, NT)
+        power.append(jnp.where(strict, pairs[:, :LENGTH], 0.0))
+        alpha_keys = jnp.where(strict, pairs[:, LENGTH:], 0.0)
         value_rows.append(jnp.where(own[h], 0.0, turned_values))
         solved.append(jnp.where(own[h], start_alpha, dot3(alpha_keys, value_rows[h])))
     for step in range(5):
@@ -290,8 +287,7 @@
         if step < 4:
             power = [dot3(power[h], power[h]) for h in range(2)]
     for h in range(2):
-        known = jnp.concatenate([solved[h], value_rows[h]], axis=0)
-        query.append(jnp.where(own[h], start_recept, 0.0) + dot3(recept_pairs[h], known))
+        solved_ref[h] = solved[h]
     steps = [[], []]
     whole = jnp.where(diagonal, 1.0, 0.0)
     for b in range(BLOCKS):
@@ -310,14 +306,29 @@
     mine_ref[...] = jnp.where(core == 0, finals[0], finals[1])
     theirs_ref[...] = jnp.where(core == 0, finals[1], finals[0])
     for h in range(2):
-        prefixes = [
-            None,
-            steps[h][0],
-            one[h],
-            dot3(steps[h][2], one[h]),
-            four[h],
-            dot3(steps[h][4], four[h]),
-        ]
+        for k, step in enumerate((steps[h][0], one[h], steps[h][2], four[h], steps[h][4])):
+            steps_ref[h, k] = step
+
+
+def reads_kernel(place_ref, tables_ref, solved_ref, steps_ref, reads_ref):
+    recept_mid, start_recept, turned_values = tables_ref[0], tables_ref[1], tables_ref[4]
+    right = jnp.concatenate([tables_ref[2], tables_ref[3]], axis=0)
+    first = iota((LENGTH, 128), 1) < HEAD
+    wide_row, wide_column = iota((LENGTH, 2 * LENGTH), 0), iota((LENGTH, 2 * LENGTH), 1)
+    wide_column = jnp.where(wide_column >= LENGTH, wide_column - LENGTH, wide_column)
+    inclusive_twice = ((wide_row // BLOCK) == (wide_column // BLOCK)) & (wide_row >= wide_column)
+    own = [first, jnp.logical_not(first)]
+    query = []
+    for h in range(2):
+        pairs = dot3(jnp.where(own[h], recept_mid, 0.0), right, NT)
+        pairs = jnp.where(inclusive_twice, pairs, 0.0)
+        known = jnp.concatenate(
+            [solved_ref[h], jnp.where(own[h], 0.0, turned_values)], axis=0
+        )
+        query.append(jnp.where(own[h], start_recept, 0.0) + dot3(pairs, known))
+    for h in range(2):
+        zero, one, two, four, five = (steps_ref[h, k] for k in range(5))
+        prefixes = (None, zero, one, dot3(two, one), four, dot3(five, four))
         reads_ref[h, 0:BLOCK, :] = query[h][0:BLOCK]
         for b in range(1, BLOCKS):
             rows = slice(b * BLOCK, b * BLOCK + BLOCK)
@@ -412,7 +423,10 @@
     theirs_ref,
     gate_ref,
     filtered_ref,
-    sums_ref,
+    sums0_ref,
+    sums1_ref,
+    sums2_ref,
+    sums3_ref,
     columns_ref,
     table_ref,
     out_ref,
@@ -446,8 +460,10 @@
     spread = head_mean(centered * centered)
     scan_out = (centered * lax.rsqrt(spread + 0.00064) * gate_ref[...]).astype(BF16)
 
+    sums = (sums0_ref[...] + sums1_ref[...]) + (sums2_ref[...] + sums3_ref[...])
+
     def spread_out(k):
-        return exact(sums_ref[...], jnp.where(iota((8, 128), 0) == k, 1.0 / 512.0, 0.0), TN)
+        return exact(sums, jnp.where(iota((8, 128), 0) == k, 1.0 / 512.0, 0.0), TN)
 
     rest = spread_out(2)
     center = jnp.concatenate([spread_out(0), rest[:64]], axis=0)
@@ -543,15 +559,17 @@
         scratch=[pltpu.VMEM(WEIGHTS, BF16)],
         limit=16,
     )
-    mine, theirs, reads, gate, conv_input, rim = on_core(
+    mine, theirs, gate, conv_input, rim, tables, solved, steps = on_core(
         local_kernel,
         (
             vmem((HEAD, 128), F32),
             vmem((HEAD, 128), F32),
-            vmem((2, LENGTH, 128), F32),
             vmem((LENGTH, 128), F32),
             vmem((LENGTH, 128), BF16),
             vmem((32, 128), BF16),
+            vmem((5, LENGTH, 128), F32),
+            vmem((2, LENGTH, 128), F32),
+            vmem((2, 5, 128, 128), F32),
         ),
         index,
         *swapped,
@@ -579,7 +597,12 @@
     filtered, sums = on_core(
         conv_kernel, (vmem((LENGTH, 128), F32), vmem((8, 128), F32)), index, conv_input, rim, table
     )
-    sums = lax.psum(sums, "tp")
+    shares = [sums]
+    for k in range(1, 4):
+        shares.append(lax.ppermute(sums, "tp", [(x, (x + k) % 4) for x in range(4)]))
+    reads = on_core(
+        reads_kernel, vmem((2, LENGTH, 128), F32), index, tables, solved, steps, limit=12
+    )
     columns = on_core(columns_kernel, vmem((2048, 256), BF16), index, *pieces, *swapped)
 
     terms = on_core(
@@ -591,7 +614,7 @@
         other_state,
         gate,
         filtered,
-        sums,
+        *shares,
         columns,
         table,
     )

time: 152 us -> 154 us (1.013)
  starting transfers between devices: 23.7 us -> 33.2 us
  blocking collectives: 96.4 us -> 86.9 us
  waiting for transfers between devices: 12.6 us -> 14.9 us
    psum x1 -> x0, blocking collectives: 10.8 us -> none  [layer(): sums = lax.psum(sums, 'tp')]
    ppermute x0 -> x3, starting transfers between devices: none -> 9.62 us  [layer(): lax.ppermute(sums, 'tp', [(x, (x + k) % 4) for x in range(4)])]
    ppermute x1, waiting for transfers between devices: 2.77 us -> 4.67 us  [layer(): rim = lax.ppermute(rim, 'sp', ONWARD)]
    ppermute x0 -> x3, waiting for transfers between devices: none -> 1.72 us  [layer(): lax.ppermute(sums, 'tp', [(x, (x + k) % 4) for x in range(4)])]
    pallas_call x10 -> x11, Pallas kernels: 14.9 us -> 14.6 us  [on_core(): pl.pallas_call(kernel, in_specs=[pl.BlockSpec(memory_space=pltpu.SMEM)] +...]
  transfers between devices with their start and end apart: 10 -> 13, of which waited for: 4 -> 5; matrix products, arithmetic and copies ran while one was open for 0% -> 0% of each run, Pallas kernels for 3% -> 4%
where the time goes in v8:
time: 154 us; the launch traced here: 153 us
  blocking collectives  86.9 us (56%)
  starting transfers between devices  33.2 us (22%)
  Pallas kernels  16.4 us (11%)
  waiting for transfers between devices  14.9 us (10%)
    all_to_all x3, blocking collectives, to_each(): return lax.all_to_all(x, 'sp', 0, 0, tiled=True, axis_index_groups=groups)  61.1 us
    pallas_call x11, Pallas kernels, on_core(): pl.pallas_call(kernel, in_specs=[pl.BlockSpec(memory_space=pltpu.SMEM)] +...  14.6 us
    all_gather x1, blocking collectives, layer(): whole = lax.all_gather(tokens, 'tp')  13.8 us
    all_to_all x1, blocking collectives, layer(): parts = lax.all_to_all(terms, 'tp', 0, 0, tiled=True)  12.1 us
    ppermute x3, starting transfers between devices, layer(): lax.ppermute(sums, 'tp', [(x, (x + k) % 4) for x in range(4)])  9.62 us
    ppermute x3, starting transfers between devices, layer(): pieces.append(lax.ppermute(pieces[0], 'sp', neighbours(along_z, along_y)))  9.2 us
    ppermute x4, starting transfers between devices, layer(): swapped.append(lax.ppermute(piece, 'sp', SWAP))  8.15 us
    ppermute x3, waiting for transfers between devices, layer(): pieces.append(lax.ppermute(pieces[0], 'sp', neighbours(along_z, along_y)))  7.32 us
  transfers between devices with their start and end apart: 13, of which 5 were waited for; matrix products, arithmetic and copies ran while one was open for 0% of the time, Pallas kernels for 4%

profile of v8, /device:TPU:64, one launch (start us, length us, event | category | flops | bytes accessed | tf_op | source)
XLA Modules:
  0.0 153.2 jit_solution(11215903032391391898)
XLA Ops:
  0.0 1.8 %pack.1 = bf16[16,160,128]{2,1,0:T(8,128)(2,1)} custom-call(bf16[16,128]{1,0:T(8,128)(2,1)} %refs_0_.1, bf16[16,128]{1,0:T(8,128)(2,1)} %refs_1_.1, bf16[16,128]{1,0:T(8,128)(2,1)} %refs_2_.1, bf16[16,128]{1,0:T(8,128)(2,1)} %refs_3_.1, bf16[16,128]{1,0:T(8,128)(2,1)} %refs_4_.1, bf16[16,128]{1,0:T(8,128)(2,1)} %refs_5_.1, bf16[16,128]{1,0:T(8,128)(2,1)} %refs_6_.1, ...), custom_call_target="tpu_custom_call" | custom-call | tf_op jit(solution)/shard_map/pack/pallas_call | solution.py:109
  1.8 35.5 %all_to_all.20.p0.refs_0_ = bf16[16,160,128]{2,1,0:T(8,128)(2,1)S(1)} all-to-all(bf16[16,160,128]{2,1,0:T(8,128)(2,1)} %pack.1), channel_id=1, replica_groups={{0,16,40,56,128,144,168,184,320,336,360,376,448,464,488,504},{8,24,32,4..., dimensions={0} | all-to-all | bytes 1310720 | tf_op jit(solution)/shard_map/all_to_all | solution.py:485
  37.2 2.4 %collective-permute-start.5 = (bf16[16,160,128]{2,1,0:T(8,128)(2,1)S(1)}, bf16[16,160,128]{2,1,0:T(8,128)(2,1)S(1)}, u32[]{:S(2)}, u32[]{:S(2)}) collective-permute-start(bf16[16,160,128]{2,1,0:T(8,128)(2,1)S(1)} %all_to_all.20.p0.refs_0_), channel_id=1, source_target_pairs={{0,72},{4,508},{8,64},{12,468},{16,88},{20,460},{24,80},{28,484},{... | collective-permute-start | bytes 1966088 | tf_op jit(solution)/shard_map/ppermute | solution.py:549
  39.7 3.2 %collective-permute-start.3 = (bf16[16,160,128]{2,1,0:T(8,128)(2,1)S(1)}, bf16[16,160,128]{2,1,0:T(8,128)(2,1)S(1)}, u32[]{:S(2)}, u32[]{:S(2)}) collective-permute-start(bf16[16,160,128]{2,1,0:T(8,128)(2,1)S(1)} %all_to_all.20.p0.refs_0_), channel_id=1, source_target_pairs={{0,64},{4,452},{8,72},{12,460},{16,80},{20,468},{24,88},{28,476},{... | collective-permute-start | bytes 1966088 | tf_op jit(solution)/shard_map/ppermute | solution.py:549
  42.9 3.6 %collective-permute-start.1 = (bf16[16,160,128]{2,1,0:T(8,128)(2,1)S(1)}, bf16[16,160,128]{2,1,0:T(8,128)(2,1)S(1)}, u32[]{:S(2)}, u32[]{:S(2)}) collective-permute-start(bf16[16,160,128]{2,1,0:T(8,128)(2,1)S(1)} %all_to_all.20.p0.refs_0_), channel_id=1, source_target_pairs={{0,8},{4,60},{8,0},{12,20},{16,24},{20,12},{24,16},{28,36},{32,40}... | collective-permute-start | bytes 1966088 | tf_op jit(solution)/shard_map/ppermute | solution.py:549
  46.5 1.9 %collective-permute-start = (bf16[16,160,128]{2,1,0:T(8,128)(2,1)S(1)}, bf16[16,160,128]{2,1,0:T(8,128)(2,1)S(1)}, u32[]{:S(2)}, u32[]{:S(2)}) collective-permute-start(bf16[16,160,128]{2,1,0:T(8,128)(2,1)S(1)} %all_to_all.20.p0.refs_0_), channel_id=1, source_target_pairs={{0,4},{4,0},{8,12},{12,8},{16,20},{20,16},{24,28},{28,24},{32,36},... | collective-permute-start | bytes 1966088 | tf_op jit(solution)/shard_map/ppermute | solution.py:552
  48.4 2.3 %collective-permute-done.5.p3.refs_3_ = bf16[16,160,128]{2,1,0:T(8,128)(2,1)S(1)} collective-permute-done((bf16[16,160,128]{2,1,0:T(8,128)(2,1)S(1)}, bf16[16,160,128]{2,1,0:T(8,128)(2,1)S(1)}, u32[]{:S(2)}, u32[]{:S(2)}) %collective-permute-start.5) | collective-permute-done | bytes 655392 | tf_op jit(solution)/shard_map/ppermute | solution.py:549
  50.7 1.9 %collective-permute-start.6 = (bf16[16,160,128]{2,1,0:T(8,128)(2,1)S(1)}, bf16[16,160,128]{2,1,0:T(8,128)(2,1)}, u32[]{:S(2)}, u32[]{:S(2)}) collective-permute-start(bf16[16,160,128]{2,1,0:T(8,128)(2,1)S(1)} %collective-permute-done.5.p3.refs_3_), channel_id=1, source_target_pairs={{0,4},{4,0},{8,12},{12,8},{16,20},{20,16},{24,28},{28,24},{32,36},... | collective-permute-start | bytes 1966088 | tf_op jit(solution)/shard_map/ppermute | solution.py:552
  52.6 5.0 %collective-permute-done.3.p2.refs_2_ = bf16[16,160,128]{2,1,0:T(8,128)(2,1)S(1)} collective-permute-done((bf16[16,160,128]{2,1,0:T(8,128)(2,1)S(1)}, bf16[16,160,128]{2,1,0:T(8,128)(2,1)S(1)}, u32[]{:S(2)}, u32[]{:S(2)}) %collective-permute-start.3) | collective-permute-done | bytes 655392 | tf_op jit(solution)/shard_map/ppermute | solution.py:549
  57.6 1.9 %collective-permute-start.4 = (bf16[16,160,128]{2,1,0:T(8,128)(2,1)S(1)}, bf16[16,160,128]{2,1,0:T(8,128)(2,1)}, u32[]{:S(2)}, u32[]{:S(2)}) collective-permute-start(bf16[16,160,128]{2,1,0:T(8,128)(2,1)S(1)} %collective-permute-done.3.p2.refs_2_), channel_id=1, source_target_pairs={{0,4},{4,0},{8,12},{12,8},{16,20},{20,16},{24,28},{28,24},{32,36},... | collective-permute-start | bytes 1966088 | tf_op jit(solution)/shard_map/ppermute | solution.py:552
  59.6 2.4 %collective-permute-start.2 = (bf16[16,160,128]{2,1,0:T(8,128)(2,1)S(1)}, bf16[16,160,128]{2,1,0:T(8,128)(2,1)}, u32[]{:S(2)}, u32[]{:S(2)}) collective-permute-start(bf16[16,160,128]{2,1,0:T(8,128)(2,1)S(1)} %collective-permute-done.1.p1.refs_1_), channel_id=1, source_target_pairs={{0,4},{4,0},{8,12},{12,8},{16,20},{20,16},{24,28},{28,24},{32,36},... | collective-permute-start | bytes 1966088 | tf_op jit(solution)/shard_map/ppermute | solution.py:552
  62.0 13.8 %all-gather = bf16[768,512]{1,0:T(8,128)(2,1)S(1)} all-gather(bf16[192,512]{1,0:T(8,128)(2,1)S(1)} %copy-done.9), channel_id=2, replica_groups=mesh['sp'=128,'tp'=4] {'tp'}, dimensions={0}, use_global_device_ids=true | all-gather | bytes 983040 | tf_op jit(solution)/shard_map/all_gather | solution.py:527
  78.1 6.5 %shard_map.202 = (f32[64,128]{1,0:T(8,128)S(1)}, f32[64,128]{1,0:T(8,128)S(1)}, f32[192,128]{1,0:T(8,128)S(1)}, bf16[192,128]{1,0:T(8,128)(2,1)S(1)}, bf16[32,12...) custom-call(s32[1]{0:T(128)} %bitcast.place_ref.core_ref, ...), custom_call_target="tpu_custom_call" | custom-call | tf_op jit(solution)/shard_map/pallas_call | solution.py:90
  84.7 1.9 %collective-permute-start.7 = (f32[64,128]{1,0:T(8,128)S(1)}, f32[64,128]{1,0:T(8,128)S(1)}, u32[]{:S(2)}, u32[]{:S(2)}) collective-permute-start(f32[64,128]{1,0:T(8,128)S(1)} %get-tuple-element.27), channel_id=1, source_target_pairs={{0,4},{4,0},{8,12},{12,8},{16,20},{20,16},{24,28},{28,24},{32,36},... | collective-permute-start | bytes 98312 | tf_op jit(solution)/shard_map/ppermute | solution.py:584
  87.9 12.1 %all_to_all.21.steps_ref = bf16[8,64,128]{2,1,0:T(8,128)(2,1)S(1)} all-to-all(bf16[8,64,128]{2,1,0:T(8,128)(2,1)S(1)} %shard_map.204), channel_id=1, replica_groups={{0,8,16,24,32,40,48,56},{4,12,20,28,36,44,52,60},{64,72,80,88,96,104,11..., dimensions={0} | all-to-all | bytes 262144 | tf_op jit(solution)/shard_map/all_to_all | solution.py:485
  100.8 13.5 %all_to_all.22.steps_ref = bf16[8,64,128]{2,1,0:T(8,128)(2,1)S(1)} all-to-all(bf16[8,64,128]{2,1,0:T(8,128)(2,1)S(1)} %get-tuple-element.28), channel_id=1, replica_groups={{0,64,128,192,256,320,384,448},{4,68,132,196,260,324,388,452},{8,72,136..., dimensions={0} | all-to-all | bytes 262144 | tf_op jit(solution)/shard_map/all_to_all | solution.py:485
  115.1 1.9 %collective-permute-start.8 = (f32[64,128]{1,0:T(8,128)S(1)}, f32[64,128]{1,0:T(8,128)S(1)}, u32[]{:S(2)}, u32[]{:S(2)}) collective-permute-start(f32[64,128]{1,0:T(8,128)S(1)} %get-tuple-element.31), channel_id=1, source_target_pairs={{0,4},{4,0},{8,12},{12,8},{16,20},{20,16},{24,28},{28,24},{32,36},... | collective-permute-start | bytes 98312 | tf_op jit(solution)/shard_map/ppermute | solution.py:595
  117.0 2.4 %collective-permute-start.9 = (bf16[32,128]{1,0:T(8,128)(2,1)S(1)}, bf16[32,128]{1,0:T(8,128)(2,1)S(1)}, u32[]{:S(2)}, u32[]{:S(2)}) collective-permute-start(bf16[32,128]{1,0:T(8,128)(2,1)S(1)} %get-tuple-element.34), channel_id=1, source_target_pairs={{0,4},{4,8},{8,12},{12,16},{16,20},{20,24},{24,28},{28,32},{32,36}... | collective-permute-start | bytes 24584 | tf_op jit(solution)/shard_map/ppermute | solution.py:585
  119.4 4.7 %collective-permute-done.9.rim_ref = bf16[32,128]{1,0:T(8,128)(2,1)S(1)} collective-permute-done((bf16[32,128]{1,0:T(8,128)(2,1)S(1)}, bf16[32,128]{1,0:T(8,128)(2,1)S(1)}, u32[]{:S(2)}, u32[]{:S(2)}) %collective-permute-start.9) | collective-permute-done | bytes 8224 | tf_op jit(solution)/shard_map/ppermute | solution.py:585
  124.8 4.9 %collective-permute-start.12 = (f32[8,128]{1,0:T(8,128)S(1)}, f32[8,128]{1,0:T(8,128)S(1)}, u32[]{:S(2)}, u32[]{:S(2)}) collective-permute-start(f32[8,128]{1,0:T(8,128)S(1)} %get-tuple-element.36.sums0_ref), channel_id=1, source_target_pairs={{0,3},{1,0},{2,1},{3,2},{4,7},{5,4},{6,5},{7,6},{8,11},{9,8},{10,9... | collective-permute-start | bytes 12296 | tf_op jit(solution)/shard_map/ppermute | solution.py:602
  129.8 2.8 %collective-permute-start.11 = (f32[8,128]{1,0:T(8,128)S(1)}, f32[8,128]{1,0:T(8,128)S(1)}, u32[]{:S(2)}, u32[]{:S(2)}) collective-permute-start(f32[8,128]{1,0:T(8,128)S(1)} %get-tuple-element.36.sums0_ref), channel_id=1, source_target_pairs={{0,2},{1,3},{2,0},{3,1},{4,6},{5,7},{6,4},{7,5},{8,10},{9,11},{10,... | collective-permute-start | bytes 12296 | tf_op jit(solution)/shard_map/ppermute | solution.py:602
  132.6 1.9 %collective-permute-start.10 = (f32[8,128]{1,0:T(8,128)S(1)}, f32[8,128]{1,0:T(8,128)S(1)}, u32[]{:S(2)}, u32[]{:S(2)}) collective-permute-start(f32[8,128]{1,0:T(8,128)S(1)} %get-tuple-element.36.sums0_ref), channel_id=1, source_target_pairs={{0,1},{1,2},{2,3},{3,0},{4,5},{5,6},{6,7},{7,4},{8,9},{9,10},{10,1... | collective-permute-start | bytes 12296 | tf_op jit(solution)/shard_map/ppermute | solution.py:602
  137.6 1.7 %collective-permute-done.10.sums1_ref = f32[8,128]{1,0:T(8,128)S(1)} collective-permute-done((f32[8,128]{1,0:T(8,128)S(1)}, f32[8,128]{1,0:T(8,128)S(1)}, u32[]{:S(2)}, u32[]{:S(2)}) %collective-permute-start.10) | collective-permute-done | bytes 4128 | tf_op jit(solution)/shard_map/ppermute | solution.py:602
  140.3 12.1 %all_to_all.23 = bf16[4,192,512]{2,1,0:T(8,128)(2,1)S(1)} all-to-all(bf16[4,192,512]{2,1,0:T(8,128)(2,1)S(1)} %shard_map.209), channel_id=1, replica_groups=mesh['sp'=128,'tp'=4] {'tp'}, dimensions={0} | all-to-all | bytes 1572864 | tf_op jit(solution)/shard_map/all_to_all | solution.py:621
  (43 shorter events, 10.8 us)
Async XLA Ops:
  1.8 60.2 %copy-start.10 = (f32[2048]{0:T(1024)S(1)}, f32[2048]{0:T(1024)}, u32[]{:S(2)}) copy-start(f32[2048]{0:T(1024)} %param.22) | copy-start | bytes 24580
  1.8 60.2 %copy-start.9 = (bf16[192,512]{1,0:T(8,128)(2,1)S(1)}, bf16[192,512]{1,0:T(8,128)(2,1)}, u32[]{:S(2)}) copy-start(bf16[192,512]{1,0:T(8,128)(2,1)} %param.21) | copy-start | bytes 589828
  37.2 13.5 %collective-permute-start.5 = (bf16[16,160,128]{2,1,0:T(8,128)(2,1)S(1)}, bf16[16,160,128]{2,1,0:T(8,128)(2,1)S(1)}, u32[]{:S(2)}, u32[]{:S(2)}) collective-permute-start(bf16[16,160,128]{2,1,0:T(8,128)(2,1)S(1)} %all_to_all.20.p0.refs_0_), channel_id=1, source_target_pairs={{0,72},{4,508},{8,64},{12,468},{16,88},{20,460},{24,80},{28,484},{... | collective-permute-start | bytes 1966088 | tf_op jit(solution)/shard_map/ppermute | solution.py:549
  39.7 18.0 %collective-permute-start.3 = (bf16[16,160,128]{2,1,0:T(8,128)(2,1)S(1)}, bf16[16,160,128]{2,1,0:T(8,128)(2,1)S(1)}, u32[]{:S(2)}, u32[]{:S(2)}) collective-permute-start(bf16[16,160,128]{2,1,0:T(8,128)(2,1)S(1)} %all_to_all.20.p0.refs_0_), channel_id=1, source_target_pairs={{0,64},{4,452},{8,72},{12,460},{16,80},{20,468},{24,88},{28,476},{... | collective-permute-start | bytes 1966088 | tf_op jit(solution)/shard_map/ppermute | solution.py:549
  42.9 16.7 %collective-permute-start.1 = (bf16[16,160,128]{2,1,0:T(8,128)(2,1)S(1)}, bf16[16,160,128]{2,1,0:T(8,128)(2,1)S(1)}, u32[]{:S(2)}, u32[]{:S(2)}) collective-permute-start(bf16[16,160,128]{2,1,0:T(8,128)(2,1)S(1)} %all_to_all.20.p0.refs_0_), channel_id=1, source_target_pairs={{0,8},{4,60},{8,0},{12,20},{16,24},{20,12},{24,16},{28,36},{32,40}... | collective-permute-start | bytes 1966088 | tf_op jit(solution)/shard_map/ppermute | solution.py:549
  46.5 31.6 %collective-permute-start = (bf16[16,160,128]{2,1,0:T(8,128)(2,1)S(1)}, bf16[16,160,128]{2,1,0:T(8,128)(2,1)S(1)}, u32[]{:S(2)}, u32[]{:S(2)}) collective-permute-start(bf16[16,160,128]{2,1,0:T(8,128)(2,1)S(1)} %all_to_all.20.p0.refs_0_), channel_id=1, source_target_pairs={{0,4},{4,0},{8,12},{12,8},{16,20},{20,16},{24,28},{28,24},{32,36},... | collective-permute-start | bytes 1966088 | tf_op jit(solution)/shard_map/ppermute | solution.py:552
  50.7 27.4 %collective-permute-start.6 = (bf16[16,160,128]{2,1,0:T(8,128)(2,1)S(1)}, bf16[16,160,128]{2,1,0:T(8,128)(2,1)}, u32[]{:S(2)}, u32[]{:S(2)}) collective-permute-start(bf16[16,160,128]{2,1,0:T(8,128)(2,1)S(1)} %collective-permute-done.5.p3.refs_3_), channel_id=1, source_target_pairs={{0,4},{4,0},{8,12},{12,8},{16,20},{20,16},{24,28},{28,24},{32,36},... | collective-permute-start | bytes 1966088 | tf_op jit(solution)/shard_map/ppermute | solution.py:552
  57.6 20.5 %collective-permute-start.4 = (bf16[16,160,128]{2,1,0:T(8,128)(2,1)S(1)}, bf16[16,160,128]{2,1,0:T(8,128)(2,1)}, u32[]{:S(2)}, u32[]{:S(2)}) collective-permute-start(bf16[16,160,128]{2,1,0:T(8,128)(2,1)S(1)} %collective-permute-done.3.p2.refs_2_), channel_id=1, source_target_pairs={{0,4},{4,0},{8,12},{12,8},{16,20},{20,16},{24,28},{28,24},{32,36},... | collective-permute-start | bytes 1966088 | tf_op jit(solution)/shard_map/ppermute | solution.py:552
  59.6 18.6 %collective-permute-start.2 = (bf16[16,160,128]{2,1,0:T(8,128)(2,1)S(1)}, bf16[16,160,128]{2,1,0:T(8,128)(2,1)}, u32[]{:S(2)}, u32[]{:S(2)}) collective-permute-start(bf16[16,160,128]{2,1,0:T(8,128)(2,1)S(1)} %collective-permute-done.1.p1.refs_1_), channel_id=1, source_target_pairs={{0,4},{4,0},{8,12},{12,8},{16,20},{20,16},{24,28},{28,24},{32,36},... | collective-permute-start | bytes 1966088 | tf_op jit(solution)/shard_map/ppermute | solution.py:552
  75.8 0.9 copy-start
  75.8 0.9 copy-start.1
  75.8 0.9 copy-start.5
  75.8 0.9 copy-start.6
  75.8 0.9 copy-start.7
  75.8 0.9 copy-start.8
  76.4 0.7 copy-start.2
  76.4 0.7 copy-start.3
  76.4 0.7 copy-start.4
  84.7 3.1 %collective-permute-start.7 = (f32[64,128]{1,0:T(8,128)S(1)}, f32[64,128]{1,0:T(8,128)S(1)}, u32[]{:S(2)}, u32[]{:S(2)}) collective-permute-start(f32[64,128]{1,0:T(8,128)S(1)} %get-tuple-element.27), channel_id=1, source_target_pairs={{0,4},{4,0},{8,12},{12,8},{16,20},{20,16},{24,28},{28,24},{32,36},... | collective-permute-start | bytes 98312 | tf_op jit(solution)/shard_map/ppermute | solution.py:584
  115.1 24.2 %collective-permute-start.8 = (f32[64,128]{1,0:T(8,128)S(1)}, f32[64,128]{1,0:T(8,128)S(1)}, u32[]{:S(2)}, u32[]{:S(2)}) collective-permute-start(f32[64,128]{1,0:T(8,128)S(1)} %get-tuple-element.31), channel_id=1, source_target_pairs={{0,4},{4,0},{8,12},{12,8},{16,20},{20,16},{24,28},{28,24},{32,36},... | collective-permute-start | bytes 98312 | tf_op jit(solution)/shard_map/ppermute | solution.py:595
  117.0 7.1 %collective-permute-start.9 = (bf16[32,128]{1,0:T(8,128)(2,1)S(1)}, bf16[32,128]{1,0:T(8,128)(2,1)S(1)}, u32[]{:S(2)}, u32[]{:S(2)}) collective-permute-start(bf16[32,128]{1,0:T(8,128)(2,1)S(1)} %get-tuple-element.34), channel_id=1, source_target_pairs={{0,4},{4,8},{8,12},{12,16},{16,20},{20,24},{24,28},{28,32},{32,36}... | collective-permute-start | bytes 24584 | tf_op jit(solution)/shard_map/ppermute | solution.py:585
  124.8 12.7 %collective-permute-start.12 = (f32[8,128]{1,0:T(8,128)S(1)}, f32[8,128]{1,0:T(8,128)S(1)}, u32[]{:S(2)}, u32[]{:S(2)}) collective-permute-start(f32[8,128]{1,0:T(8,128)S(1)} %get-tuple-element.36.sums0_ref), channel_id=1, source_target_pairs={{0,3},{1,0},{2,1},{3,2},{4,7},{5,4},{6,5},{7,6},{8,11},{9,8},{10,9... | collective-permute-start | bytes 12296 | tf_op jit(solution)/shard_map/ppermute | solution.py:602
  129.8 7.8 %collective-permute-start.11 = (f32[8,128]{1,0:T(8,128)S(1)}, f32[8,128]{1,0:T(8,128)S(1)}, u32[]{:S(2)}, u32[]{:S(2)}) collective-permute-start(f32[8,128]{1,0:T(8,128)S(1)} %get-tuple-element.36.sums0_ref), channel_id=1, source_target_pairs={{0,2},{1,3},{2,0},{3,1},{4,6},{5,7},{6,4},{7,5},{8,10},{9,11},{10,... | collective-permute-start | bytes 12296 | tf_op jit(solution)/shard_map/ppermute | solution.py:602
  132.6 6.7 %collective-permute-start.10 = (f32[8,128]{1,0:T(8,128)S(1)}, f32[8,128]{1,0:T(8,128)S(1)}, u32[]{:S(2)}, u32[]{:S(2)}) collective-permute-start(f32[8,128]{1,0:T(8,128)S(1)} %get-tuple-element.36.sums0_ref), channel_id=1, source_target_pairs={{0,1},{1,2},{2,3},{3,0},{4,5},{5,6},{6,7},{7,4},{8,9},{9,10},{10,1... | collective-permute-start | bytes 12296 | tf_op jit(solution)/shard_map/ppermute | solution.py:602

commit v9 on v8

--- a/solution.py
+++ b/solution.py
@@ -307,7 +307,7 @@
     theirs_ref[...] = jnp.where(core == 0, finals[1], finals[0])
     for h in range(2):
         for k, step in enumerate((steps[h][0], one[h], steps[h][2], four[h], steps[h][4])):
-            steps_ref[h, k] = step
+            steps_ref[h, k] = step[h * HEAD : h * HEAD + HEAD]
 
 
 def reads_kernel(place_ref, tables_ref, solved_ref, steps_ref, reads_ref):
@@ -326,8 +326,15 @@
             [solved_ref[h], jnp.where(own[h], 0.0, turned_values)], axis=0
         )
         query.append(jnp.where(own[h], start_recept, 0.0) + dot3(pairs, known))
+    lane, equal = iota((HEAD, 128), 1), iota((HEAD, 128), 0)
     for h in range(2):
-        zero, one, two, four, five = (steps_ref[h, k] for k in range(5))
+        rest = jnp.where(lane == equal + (HEAD if h == 0 else 0), 1.0, 0.0)
+        zero, one, two, four, five = (
+            jnp.concatenate(
+                [steps_ref[h, k], rest] if h == 0 else [rest, steps_ref[h, k]], axis=0
+            )
+            for k in range(5)
+        )
         prefixes = (None, zero, one, dot3(two, one), four, dot3(five, four))
         reads_ref[h, 0:BLOCK, :] = query[h][0:BLOCK]
         for b in range(1, BLOCKS):
@@ -423,10 +430,7 @@
     theirs_ref,
     gate_ref,
     filtered_ref,
-    sums0_ref,
-    sums1_ref,
-    sums2_ref,
-    sums3_ref,
+    shares_ref,
     columns_ref,
     table_ref,
     out_ref,
@@ -460,7 +464,7 @@
     spread = head_mean(centered * centered)
     scan_out = (centered * lax.rsqrt(spread + 0.00064) * gate_ref[...]).astype(BF16)
 
-    sums = (sums0_ref[...] + sums1_ref[...]) + (sums2_ref[...] + sums3_ref[...])
+    sums = (shares_ref[0] + shares_ref[1]) + (shares_ref[2] + shares_ref[3])
 
     def spread_out(k):
         return exact(sums, jnp.where(iota((8, 128), 0) == k, 1.0 / 512.0, 0.0), TN)
@@ -569,7 +573,7 @@
             vmem((32, 128), BF16),
             vmem((5, LENGTH, 128), F32),
             vmem((2, LENGTH, 128), F32),
-            vmem((2, 5, 128, 128), F32),
+            vmem((2, 5, HEAD, 128), F32),
         ),
         index,
         *swapped,
@@ -597,9 +601,7 @@
     filtered, sums = on_core(
         conv_kernel, (vmem((LENGTH, 128), F32), vmem((8, 128), F32)), index, conv_input, rim, table
     )
-    shares = [sums]
-    for k in range(1, 4):
-        shares.append(lax.ppermute(sums, "tp", [(x, (x + k) % 4) for x in range(4)]))
+    shares = lax.all_gather(sums, "tp")
     reads = on_core(
         reads_kernel, vmem((2, LENGTH, 128), F32), index, tables, solved, steps, limit=12
     )
@@ -614,7 +616,7 @@
         other_state,
         gate,
         filtered,
-        *shares,
+        shares,
         columns,
         table,
     )

time: 154 us -> 153 us (level)
  blocking collectives: 86.9 us -> 100 us
  starting transfers between devices: 33.2 us -> 23.6 us
  waiting for transfers between devices: 14.9 us -> 10.1 us
    all_gather x0 -> x1, blocking collectives: none -> 12 us  [layer(): shares = lax.all_gather(sums, 'tp')]
    ppermute x3 -> x0, starting transfers between devices: 9.62 us -> none  [layer(): lax.ppermute(sums, 'tp', [(x, (x + k) % 4) for x in range(4)])]
    ppermute x1, waiting for transfers between devices: 4.67 us -> 1.62 us  [layer(): rim = lax.ppermute(rim, 'sp', ONWARD)]
    ppermute x3 -> x0, waiting for transfers between devices: 1.72 us -> none  [layer(): lax.ppermute(sums, 'tp', [(x, (x + k) % 4) for x in range(4)])]
  transfers between devices with their start and end apart: 13 -> 10, of which waited for: 5 -> 4; matrix products, arithmetic and copies ran while one was open for 0% -> 0% of each run, Pallas kernels for 4% -> 4%
where the time goes in v9:
time: 153 us; the launch traced here: 152 us
  blocking collectives  100 us (65%)
  starting transfers between devices  23.6 us (15%)
  Pallas kernels  16.4 us (11%)
  waiting for transfers between devices  10.1 us (7%)
    all_to_all x3, blocking collectives, to_each(): return lax.all_to_all(x, 'sp', 0, 0, tiled=True, axis_index_groups=groups)  61.1 us
    pallas_call x11, Pallas kernels, on_core(): pl.pallas_call(kernel, in_specs=[pl.BlockSpec(memory_space=pltpu.SMEM)] +...  14.6 us
    all_gather x1, blocking collectives, layer(): whole = lax.all_gather(tokens, 'tp')  13.8 us
    all_to_all x1, blocking collectives, layer(): parts = lax.all_to_all(terms, 'tp', 0, 0, tiled=True)  13.6 us
    all_gather x1, blocking collectives, layer(): shares = lax.all_gather(sums, 'tp')  12 us
    ppermute x3, starting transfers between devices, layer(): pieces.append(lax.ppermute(pieces[0], 'sp', neighbours(along_z, along_y)))  9.2 us
    ppermute x4, starting transfers between devices, layer(): swapped.append(lax.ppermute(piece, 'sp', SWAP))  8.15 us
    ppermute x3, waiting for transfers between devices, layer(): pieces.append(lax.ppermute(pieces[0], 'sp', neighbours(along_z, along_y)))  7.32 us
  transfers between devices with their start and end apart: 10, of which 4 were waited for; matrix products, arithmetic and copies ran while one was open for 0% of the time, Pallas kernels for 4%

profile of v9, /device:TPU:64, one launch (start us, length us, event | category | flops | bytes accessed | tf_op | source)
XLA Modules:
  0.0 152.4 jit_solution(4976540571135443330)
XLA Ops:
  0.0 1.8 %pack.1 = bf16[16,160,128]{2,1,0:T(8,128)(2,1)} custom-call(bf16[16,128]{1,0:T(8,128)(2,1)} %refs_0_.1, bf16[16,128]{1,0:T(8,128)(2,1)} %refs_1_.1, bf16[16,128]{1,0:T(8,128)(2,1)} %refs_2_.1, bf16[16,128]{1,0:T(8,128)(2,1)} %refs_3_.1, bf16[16,128]{1,0:T(8,128)(2,1)} %refs_4_.1, bf16[16,128]{1,0:T(8,128)(2,1)} %refs_5_.1, bf16[16,128]{1,0:T(8,128)(2,1)} %refs_6_.1, ...), custom_call_target="tpu_custom_call" | custom-call | tf_op jit(solution)/shard_map/pack/pallas_call | solution.py:109
  1.8 35.5 %all_to_all.20.p0.refs_0_ = bf16[16,160,128]{2,1,0:T(8,128)(2,1)S(1)} all-to-all(bf16[16,160,128]{2,1,0:T(8,128)(2,1)} %pack.1), channel_id=1, replica_groups={{0,16,40,56,128,144,168,184,320,336,360,376,448,464,488,504},{8,24,32,4..., dimensions={0} | all-to-all | bytes 1310720 | tf_op jit(solution)/shard_map/all_to_all | solution.py:489
  37.3 2.4 %collective-permute-start.5 = (bf16[16,160,128]{2,1,0:T(8,128)(2,1)S(1)}, bf16[16,160,128]{2,1,0:T(8,128)(2,1)S(1)}, u32[]{:S(2)}, u32[]{:S(2)}) collective-permute-start(bf16[16,160,128]{2,1,0:T(8,128)(2,1)S(1)} %all_to_all.20.p0.refs_0_), channel_id=1, source_target_pairs={{0,72},{4,508},{8,64},{12,468},{16,88},{20,460},{24,80},{28,484},{... | collective-permute-start | bytes 1966088 | tf_op jit(solution)/shard_map/ppermute | solution.py:553
  39.7 3.2 %collective-permute-start.3 = (bf16[16,160,128]{2,1,0:T(8,128)(2,1)S(1)}, bf16[16,160,128]{2,1,0:T(8,128)(2,1)S(1)}, u32[]{:S(2)}, u32[]{:S(2)}) collective-permute-start(bf16[16,160,128]{2,1,0:T(8,128)(2,1)S(1)} %all_to_all.20.p0.refs_0_), channel_id=1, source_target_pairs={{0,64},{4,452},{8,72},{12,460},{16,80},{20,468},{24,88},{28,476},{... | collective-permute-start | bytes 1966088 | tf_op jit(solution)/shard_map/ppermute | solution.py:553
  42.9 3.6 %collective-permute-start.1 = (bf16[16,160,128]{2,1,0:T(8,128)(2,1)S(1)}, bf16[16,160,128]{2,1,0:T(8,128)(2,1)S(1)}, u32[]{:S(2)}, u32[]{:S(2)}) collective-permute-start(bf16[16,160,128]{2,1,0:T(8,128)(2,1)S(1)} %all_to_all.20.p0.refs_0_), channel_id=1, source_target_pairs={{0,8},{4,60},{8,0},{12,20},{16,24},{20,12},{24,16},{28,36},{32,40}... | collective-permute-start | bytes 1966088 | tf_op jit(solution)/shard_map/ppermute | solution.py:553
  46.5 1.9 %collective-permute-start = (bf16[16,160,128]{2,1,0:T(8,128)(2,1)S(1)}, bf16[16,160,128]{2,1,0:T(8,128)(2,1)S(1)}, u32[]{:S(2)}, u32[]{:S(2)}) collective-permute-start(bf16[16,160,128]{2,1,0:T(8,128)(2,1)S(1)} %all_to_all.20.p0.refs_0_), channel_id=1, source_target_pairs={{0,4},{4,0},{8,12},{12,8},{16,20},{20,16},{24,28},{28,24},{32,36},... | collective-permute-start | bytes 1966088 | tf_op jit(solution)/shard_map/ppermute | solution.py:556
  48.4 2.3 %collective-permute-done.5.p3.refs_3_ = bf16[16,160,128]{2,1,0:T(8,128)(2,1)S(1)} collective-permute-done((bf16[16,160,128]{2,1,0:T(8,128)(2,1)S(1)}, bf16[16,160,128]{2,1,0:T(8,128)(2,1)S(1)}, u32[]{:S(2)}, u32[]{:S(2)}) %collective-permute-start.5) | collective-permute-done | bytes 655392 | tf_op jit(solution)/shard_map/ppermute | solution.py:553
  50.7 1.9 %collective-permute-start.6 = (bf16[16,160,128]{2,1,0:T(8,128)(2,1)S(1)}, bf16[16,160,128]{2,1,0:T(8,128)(2,1)}, u32[]{:S(2)}, u32[]{:S(2)}) collective-permute-start(bf16[16,160,128]{2,1,0:T(8,128)(2,1)S(1)} %collective-permute-done.5.p3.refs_3_), channel_id=1, source_target_pairs={{0,4},{4,0},{8,12},{12,8},{16,20},{20,16},{24,28},{28,24},{32,36},... | collective-permute-start | bytes 1966088 | tf_op jit(solution)/shard_map/ppermute | solution.py:556
  52.6 5.0 %collective-permute-done.3.p2.refs_2_ = bf16[16,160,128]{2,1,0:T(8,128)(2,1)S(1)} collective-permute-done((bf16[16,160,128]{2,1,0:T(8,128)(2,1)S(1)}, bf16[16,160,128]{2,1,0:T(8,128)(2,1)S(1)}, u32[]{:S(2)}, u32[]{:S(2)}) %collective-permute-start.3) | collective-permute-done | bytes 655392 | tf_op jit(solution)/shard_map/ppermute | solution.py:553
  57.6 1.9 %collective-permute-start.4 = (bf16[16,160,128]{2,1,0:T(8,128)(2,1)S(1)}, bf16[16,160,128]{2,1,0:T(8,128)(2,1)}, u32[]{:S(2)}, u32[]{:S(2)}) collective-permute-start(bf16[16,160,128]{2,1,0:T(8,128)(2,1)S(1)} %collective-permute-done.3.p2.refs_2_), channel_id=1, source_target_pairs={{0,4},{4,0},{8,12},{12,8},{16,20},{20,16},{24,28},{28,24},{32,36},... | collective-permute-start | bytes 1966088 | tf_op jit(solution)/shard_map/ppermute | solution.py:556
  59.6 2.4 %collective-permute-start.2 = (bf16[16,160,128]{2,1,0:T(8,128)(2,1)S(1)}, bf16[16,160,128]{2,1,0:T(8,128)(2,1)}, u32[]{:S(2)}, u32[]{:S(2)}) collective-permute-start(bf16[16,160,128]{2,1,0:T(8,128)(2,1)S(1)} %collective-permute-done.1.p1.refs_1_), channel_id=1, source_target_pairs={{0,4},{4,0},{8,12},{12,8},{16,20},{20,16},{24,28},{28,24},{32,36},... | collective-permute-start | bytes 1966088 | tf_op jit(solution)/shard_map/ppermute | solution.py:556
  62.0 13.8 %all-gather = bf16[768,512]{1,0:T(8,128)(2,1)S(1)} all-gather(bf16[192,512]{1,0:T(8,128)(2,1)S(1)} %copy-done.9), channel_id=2, replica_groups=mesh['sp'=128,'tp'=4] {'tp'}, dimensions={0}, use_global_device_ids=true | all-gather | bytes 983040 | tf_op jit(solution)/shard_map/all_gather | solution.py:531
  78.2 6.5 %shard_map.202 = (f32[64,128]{1,0:T(8,128)S(1)}, f32[64,128]{1,0:T(8,128)S(1)}, f32[192,128]{1,0:T(8,128)S(1)}, bf16[192,128]{1,0:T(8,128)(2,1)S(1)}, bf16[32,12...) custom-call(s32[1]{0:T(128)} %bitcast.place_ref.core_ref, ...), custom_call_target="tpu_custom_call" | custom-call | tf_op jit(solution)/shard_map/pallas_call | solution.py:90
  84.7 1.9 %collective-permute-start.7 = (f32[64,128]{1,0:T(8,128)S(1)}, f32[64,128]{1,0:T(8,128)S(1)}, u32[]{:S(2)}, u32[]{:S(2)}) collective-permute-start(f32[64,128]{1,0:T(8,128)S(1)} %get-tuple-element.27), channel_id=1, source_target_pairs={{0,4},{4,0},{8,12},{12,8},{16,20},{20,16},{24,28},{28,24},{32,36},... | collective-permute-start | bytes 98312 | tf_op jit(solution)/shard_map/ppermute | solution.py:588
  86.6 1.2 collective-permute-done.7.theirs_ref
  87.9 12.1 %all_to_all.21.steps_ref = bf16[8,64,128]{2,1,0:T(8,128)(2,1)S(1)} all-to-all(bf16[8,64,128]{2,1,0:T(8,128)(2,1)S(1)} %shard_map.204), channel_id=1, replica_groups={{0,8,16,24,32,40,48,56},{4,12,20,28,36,44,52,60},{64,72,80,88,96,104,11..., dimensions={0} | all-to-all | bytes 262144 | tf_op jit(solution)/shard_map/all_to_all | solution.py:489
  100.8 13.5 %all_to_all.22.steps_ref = bf16[8,64,128]{2,1,0:T(8,128)(2,1)S(1)} all-to-all(bf16[8,64,128]{2,1,0:T(8,128)(2,1)S(1)} %get-tuple-element.28), channel_id=1, replica_groups={{0,64,128,192,256,320,384,448},{4,68,132,196,260,324,388,452},{8,72,136..., dimensions={0} | all-to-all | bytes 262144 | tf_op jit(solution)/shard_map/all_to_all | solution.py:489
  115.1 1.9 %collective-permute-start.8 = (f32[64,128]{1,0:T(8,128)S(1)}, f32[64,128]{1,0:T(8,128)S(1)}, u32[]{:S(2)}, u32[]{:S(2)}) collective-permute-start(f32[64,128]{1,0:T(8,128)S(1)} %get-tuple-element.31), channel_id=1, source_target_pairs={{0,4},{4,0},{8,12},{12,8},{16,20},{20,16},{24,28},{28,24},{32,36},... | collective-permute-start | bytes 98312 | tf_op jit(solution)/shard_map/ppermute | solution.py:599
  117.1 2.4 %collective-permute-start.9 = (bf16[32,128]{1,0:T(8,128)(2,1)S(1)}, bf16[32,128]{1,0:T(8,128)(2,1)S(1)}, u32[]{:S(2)}, u32[]{:S(2)}) collective-permute-start(bf16[32,128]{1,0:T(8,128)(2,1)S(1)} %get-tuple-element.34), channel_id=1, source_target_pairs={{0,4},{4,8},{8,12},{12,16},{16,20},{20,24},{24,28},{28,32},{32,36}... | collective-permute-start | bytes 24584 | tf_op jit(solution)/shard_map/ppermute | solution.py:589
  119.5 1.3 shard_map.203.reads_ref
  120.8 1.7 %shard_map.208.columns_ref = bf16[2048,256]{1,0:T(8,128)(2,1)S(1)} custom-call(s32[1]{0:T(128)} %bitcast.place_ref.core_ref, bf16[16,160,128]{2,1,0:T(8,128)(2,1)S(1)} %all_to_all.20.p0.refs_0_, bf16[16,160,128]{2,1,0:T(8,128)(2,1)S(1)} %collective-permute-done.1.p1.refs_1_, bf16[16,160,128]{2,1,0:T(8,128)(2,1)S(1)} %collective-permute-done.3.p2.refs_2_, ...), custom_call_target="tpu_custom_call" | custom-call | tf_op jit(solution)/shard_map/pallas_call | solution.py:90
  122.5 1.6 %collective-permute-done.9.rim_ref = bf16[32,128]{1,0:T(8,128)(2,1)S(1)} collective-permute-done((bf16[32,128]{1,0:T(8,128)(2,1)S(1)}, bf16[32,128]{1,0:T(8,128)(2,1)S(1)}, u32[]{:S(2)}, u32[]{:S(2)}) %collective-permute-start.9) | collective-permute-done | bytes 8224 | tf_op jit(solution)/shard_map/ppermute | solution.py:589
  124.9 12.0 %all-gather.1 = f32[32,128]{1,0:T(8,128)S(1)} all-gather(f32[8,128]{1,0:T(8,128)S(1)} %get-tuple-element.36), channel_id=3, replica_groups=mesh['sp'=128,'tp'=4] {'tp'}, dimensions={0}, use_global_device_ids=true | all-gather | bytes 20480 | tf_op jit(solution)/shard_map/all_gather | solution.py:604
  138.0 13.6 %all_to_all.23 = bf16[4,192,512]{2,1,0:T(8,128)(2,1)S(1)} all-to-all(bf16[4,192,512]{2,1,0:T(8,128)(2,1)S(1)} %shard_map.209), channel_id=1, replica_groups=mesh['sp'=128,'tp'=4] {'tp'}, dimensions={0} | all-to-all | bytes 1572864 | tf_op jit(solution)/shard_map/all_to_all | solution.py:623
  (38 shorter events, 6.6 us)
Async XLA Ops:
  1.8 60.2 %copy-start.10 = (f32[2048]{0:T(1024)S(1)}, f32[2048]{0:T(1024)}, u32[]{:S(2)}) copy-start(f32[2048]{0:T(1024)} %param.22) | copy-start | bytes 24580
  1.8 60.2 %copy-start.9 = (bf16[192,512]{1,0:T(8,128)(2,1)S(1)}, bf16[192,512]{1,0:T(8,128)(2,1)}, u32[]{:S(2)}) copy-start(bf16[192,512]{1,0:T(8,128)(2,1)} %param.21) | copy-start | bytes 589828
  37.3 13.5 %collective-permute-start.5 = (bf16[16,160,128]{2,1,0:T(8,128)(2,1)S(1)}, bf16[16,160,128]{2,1,0:T(8,128)(2,1)S(1)}, u32[]{:S(2)}, u32[]{:S(2)}) collective-permute-start(bf16[16,160,128]{2,1,0:T(8,128)(2,1)S(1)} %all_to_all.20.p0.refs_0_), channel_id=1, source_target_pairs={{0,72},{4,508},{8,64},{12,468},{16,88},{20,460},{24,80},{28,484},{... | collective-permute-start | bytes 1966088 | tf_op jit(solution)/shard_map/ppermute | solution.py:553
  39.7 18.0 %collective-permute-start.3 = (bf16[16,160,128]{2,1,0:T(8,128)(2,1)S(1)}, bf16[16,160,128]{2,1,0:T(8,128)(2,1)S(1)}, u32[]{:S(2)}, u32[]{:S(2)}) collective-permute-start(bf16[16,160,128]{2,1,0:T(8,128)(2,1)S(1)} %all_to_all.20.p0.refs_0_), channel_id=1, source_target_pairs={{0,64},{4,452},{8,72},{12,460},{16,80},{20,468},{24,88},{28,476},{... | collective-permute-start | bytes 1966088 | tf_op jit(solution)/shard_map/ppermute | solution.py:553
  42.9 16.7 %collective-permute-start.1 = (bf16[16,160,128]{2,1,0:T(8,128)(2,1)S(1)}, bf16[16,160,128]{2,1,0:T(8,128)(2,1)S(1)}, u32[]{:S(2)}, u32[]{:S(2)}) collective-permute-start(bf16[16,160,128]{2,1,0:T(8,128)(2,1)S(1)} %all_to_all.20.p0.refs_0_), channel_id=1, source_target_pairs={{0,8},{4,60},{8,0},{12,20},{16,24},{20,12},{24,16},{28,36},{32,40}... | collective-permute-start | bytes 1966088 | tf_op jit(solution)/shard_map/ppermute | solution.py:553
  46.5 31.6 %collective-permute-start = (bf16[16,160,128]{2,1,0:T(8,128)(2,1)S(1)}, bf16[16,160,128]{2,1,0:T(8,128)(2,1)S(1)}, u32[]{:S(2)}, u32[]{:S(2)}) collective-permute-start(bf16[16,160,128]{2,1,0:T(8,128)(2,1)S(1)} %all_to_all.20.p0.refs_0_), channel_id=1, source_target_pairs={{0,4},{4,0},{8,12},{12,8},{16,20},{20,16},{24,28},{28,24},{32,36},... | collective-permute-start | bytes 1966088 | tf_op jit(solution)/shard_map/ppermute | solution.py:556
  50.7 27.4 %collective-permute-start.6 = (bf16[16,160,128]{2,1,0:T(8,128)(2,1)S(1)}, bf16[16,160,128]{2,1,0:T(8,128)(2,1)}, u32[]{:S(2)}, u32[]{:S(2)}) collective-permute-start(bf16[16,160,128]{2,1,0:T(8,128)(2,1)S(1)} %collective-permute-done.5.p3.refs_3_), channel_id=1, source_target_pairs={{0,4},{4,0},{8,12},{12,8},{16,20},{20,16},{24,28},{28,24},{32,36},... | collective-permute-start | bytes 1966088 | tf_op jit(solution)/shard_map/ppermute | solution.py:556
  57.6 20.5 %collective-permute-start.4 = (bf16[16,160,128]{2,1,0:T(8,128)(2,1)S(1)}, bf16[16,160,128]{2,1,0:T(8,128)(2,1)}, u32[]{:S(2)}, u32[]{:S(2)}) collective-permute-start(bf16[16,160,128]{2,1,0:T(8,128)(2,1)S(1)} %collective-permute-done.3.p2.refs_2_), channel_id=1, source_target_pairs={{0,4},{4,0},{8,12},{12,8},{16,20},{20,16},{24,28},{28,24},{32,36},... | collective-permute-start | bytes 1966088 | tf_op jit(solution)/shard_map/ppermute | solution.py:556
  59.6 18.6 %collective-permute-start.2 = (bf16[16,160,128]{2,1,0:T(8,128)(2,1)S(1)}, bf16[16,160,128]{2,1,0:T(8,128)(2,1)}, u32[]{:S(2)}, u32[]{:S(2)}) collective-permute-start(bf16[16,160,128]{2,1,0:T(8,128)(2,1)S(1)} %collective-permute-done.1.p1.refs_1_), channel_id=1, source_target_pairs={{0,4},{4,0},{8,12},{12,8},{16,20},{20,16},{24,28},{28,24},{32,36},... | collective-permute-start | bytes 1966088 | tf_op jit(solution)/shard_map/ppermute | solution.py:556
  75.8 0.9 copy-start
  75.8 0.9 copy-start.1
  75.8 0.9 copy-start.5
  75.8 0.9 copy-start.6
  75.8 0.9 copy-start.7
  75.8 0.9 copy-start.8
  76.4 0.7 copy-start.2
  76.4 0.7 copy-start.3
  76.4 0.7 copy-start.4
  84.7 3.1 %collective-permute-start.7 = (f32[64,128]{1,0:T(8,128)S(1)}, f32[64,128]{1,0:T(8,128)S(1)}, u32[]{:S(2)}, u32[]{:S(2)}) collective-permute-start(f32[64,128]{1,0:T(8,128)S(1)} %get-tuple-element.27), channel_id=1, source_target_pairs={{0,4},{4,0},{8,12},{12,8},{16,20},{20,16},{24,28},{28,24},{32,36},... | collective-permute-start | bytes 98312 | tf_op jit(solution)/shard_map/ppermute | solution.py:588
  115.1 21.8 %collective-permute-start.8 = (f32[64,128]{1,0:T(8,128)S(1)}, f32[64,128]{1,0:T(8,128)S(1)}, u32[]{:S(2)}, u32[]{:S(2)}) collective-permute-start(f32[64,128]{1,0:T(8,128)S(1)} %get-tuple-element.31), channel_id=1, source_target_pairs={{0,4},{4,0},{8,12},{12,8},{16,20},{20,16},{24,28},{28,24},{32,36},... | collective-permute-start | bytes 98312 | tf_op jit(solution)/shard_map/ppermute | solution.py:599
  117.1 7.1 %collective-permute-start.9 = (bf16[32,128]{1,0:T(8,128)(2,1)S(1)}, bf16[32,128]{1,0:T(8,128)(2,1)S(1)}, u32[]{:S(2)}, u32[]{:S(2)}) collective-permute-start(bf16[32,128]{1,0:T(8,128)(2,1)S(1)} %get-tuple-element.34), channel_id=1, source_target_pairs={{0,4},{4,8},{8,12},{12,16},{16,20},{20,24},{24,28},{28,32},{32,36}... | collective-permute-start | bytes 24584 | tf_op jit(solution)/shard_map/ppermute | solution.py:589

commit v10 on v9

--- a/solution.py
+++ b/solution.py
@@ -430,7 +430,7 @@
     theirs_ref,
     gate_ref,
     filtered_ref,
-    shares_ref,
+    sums_ref,
     columns_ref,
     table_ref,
     out_ref,
@@ -464,7 +464,7 @@
     spread = head_mean(centered * centered)
     scan_out = (centered * lax.rsqrt(spread + 0.00064) * gate_ref[...]).astype(BF16)
 
-    sums = (shares_ref[0] + shares_ref[1]) + (shares_ref[2] + shares_ref[3])
+    sums = sums_ref[...]
 
     def spread_out(k):
         return exact(sums, jnp.where(iota((8, 128), 0) == k, 1.0 / 512.0, 0.0), TN)
@@ -601,7 +601,7 @@
     filtered, sums = on_core(
         conv_kernel, (vmem((LENGTH, 128), F32), vmem((8, 128), F32)), index, conv_input, rim, table
     )
-    shares = lax.all_gather(sums, "tp")
+    sums = lax.psum(sums, "tp")
     reads = on_core(
         reads_kernel, vmem((2, LENGTH, 128), F32), index, tables, solved, steps, limit=12
     )
@@ -616,7 +616,7 @@
         other_state,
         gate,
         filtered,
-        shares,
+        sums,
         columns,
         table,
     )

time: 153 us -> 151 us (0.987)
  the two profiles are of different devices: /device:TPU:64 before, /device:TPU:2 now
where the time goes in v10:
time: 151 us
  blocking collectives  99.8 us (66%)
  starting transfers between devices  23.7 us (16%)
  Pallas kernels  16.8 us (11%)
  waiting for transfers between devices  8.51 us (6%)
    all_to_all x3, blocking collectives, to_each(): return lax.all_to_all(x, 'sp', 0, 0, tiled=True, axis_index_groups=groups)  62.8 us
    pallas_call x11, Pallas kernels, on_core(): pl.pallas_call(kernel, in_specs=[pl.BlockSpec(memory_space=pltpu.SMEM)] +...  15 us
    all_to_all x1, blocking collectives, layer(): parts = lax.all_to_all(terms, 'tp', 0, 0, tiled=True)  14.9 us
    all_gather x1, blocking collectives, layer(): whole = lax.all_gather(tokens, 'tp')  14.1 us
    ppermute x3, starting transfers between devices, layer(): pieces.append(lax.ppermute(pieces[0], 'sp', neighbours(along_z, along_y)))  9.2 us
    ppermute x4, starting transfers between devices, layer(): swapped.append(lax.ppermute(piece, 'sp', SWAP))  8.15 us
    psum x1, blocking collectives, layer(): sums = lax.psum(sums, 'tp')  7.94 us
    ppermute x3, waiting for transfers between devices, layer(): pieces.append(lax.ppermute(pieces[0], 'sp', neighbours(along_z, along_y)))  7.32 us
  transfers between devices with their start and end apart: 10, of which 3 were waited for; matrix products, arithmetic and copies ran while one was open for 0% of the time, Pallas kernels for 4%

profile of v10, /device:TPU:2, one launch (start us, length us, event | category | flops | bytes accessed | tf_op | source)
XLA Modules:
  0.0 150.6 jit_solution(2429601611834737704)
XLA Ops:
  0.0 1.8 %pack.1 = bf16[16,160,128]{2,1,0:T(8,128)(2,1)} custom-call(bf16[16,128]{1,0:T(8,128)(2,1)} %refs_0_.1, bf16[16,128]{1,0:T(8,128)(2,1)} %refs_1_.1, bf16[16,128]{1,0:T(8,128)(2,1)} %refs_2_.1, bf16[16,128]{1,0:T(8,128)(2,1)} %refs_3_.1, bf16[16,128]{1,0:T(8,128)(2,1)} %refs_4_.1, bf16[16,128]{1,0:T(8,128)(2,1)} %refs_5_.1, bf16[16,128]{1,0:T(8,128)(2,1)} %refs_6_.1, ...), custom_call_target="tpu_custom_call" | custom-call | tf_op jit(solution)/shard_map/pack/pallas_call | solution.py:109
  1.8 36.9 %all_to_all.20.p0.refs_0_ = bf16[16,160,128]{2,1,0:T(8,128)(2,1)S(1)} all-to-all(bf16[16,160,128]{2,1,0:T(8,128)(2,1)} %pack.1), channel_id=1, replica_groups={{0,16,40,56,128,144,168,184,320,336,360,376,448,464,488,504},{8,24,32,4..., dimensions={0} | all-to-all | bytes 1310720 | tf_op jit(solution)/shard_map/all_to_all | solution.py:489
  38.7 2.6 %collective-permute-start.5 = (bf16[16,160,128]{2,1,0:T(8,128)(2,1)S(1)}, bf16[16,160,128]{2,1,0:T(8,128)(2,1)S(1)}, u32[]{:S(2)}, u32[]{:S(2)}) collective-permute-start(bf16[16,160,128]{2,1,0:T(8,128)(2,1)S(1)} %all_to_all.20.p0.refs_0_), channel_id=1, source_target_pairs={{0,72},{4,508},{8,64},{12,468},{16,88},{20,460},{24,80},{28,484},{... | collective-permute-start | bytes 1966088 | tf_op jit(solution)/shard_map/ppermute | solution.py:553
  41.3 2.7 %collective-permute-start.3 = (bf16[16,160,128]{2,1,0:T(8,128)(2,1)S(1)}, bf16[16,160,128]{2,1,0:T(8,128)(2,1)S(1)}, u32[]{:S(2)}, u32[]{:S(2)}) collective-permute-start(bf16[16,160,128]{2,1,0:T(8,128)(2,1)S(1)} %all_to_all.20.p0.refs_0_), channel_id=1, source_target_pairs={{0,64},{4,452},{8,72},{12,460},{16,80},{20,468},{24,88},{28,476},{... | collective-permute-start | bytes 1966088 | tf_op jit(solution)/shard_map/ppermute | solution.py:553
  44.0 3.9 %collective-permute-start.1 = (bf16[16,160,128]{2,1,0:T(8,128)(2,1)S(1)}, bf16[16,160,128]{2,1,0:T(8,128)(2,1)S(1)}, u32[]{:S(2)}, u32[]{:S(2)}) collective-permute-start(bf16[16,160,128]{2,1,0:T(8,128)(2,1)S(1)} %all_to_all.20.p0.refs_0_), channel_id=1, source_target_pairs={{0,8},{4,60},{8,0},{12,20},{16,24},{20,12},{24,16},{28,36},{32,40}... | collective-permute-start | bytes 1966088 | tf_op jit(solution)/shard_map/ppermute | solution.py:553
  47.9 1.9 %collective-permute-start = (bf16[16,160,128]{2,1,0:T(8,128)(2,1)S(1)}, bf16[16,160,128]{2,1,0:T(8,128)(2,1)}, u32[]{:S(2)}, u32[]{:S(2)}) collective-permute-start(bf16[16,160,128]{2,1,0:T(8,128)(2,1)S(1)} %all_to_all.20.p0.refs_0_), channel_id=1, source_target_pairs={{0,4},{4,0},{8,12},{12,8},{16,20},{20,16},{24,28},{28,24},{32,36},... | collective-permute-start | bytes 1966088 | tf_op jit(solution)/shard_map/ppermute | solution.py:556
  49.9 2.3 %collective-permute-done.5.p3.refs_3_ = bf16[16,160,128]{2,1,0:T(8,128)(2,1)S(1)} collective-permute-done((bf16[16,160,128]{2,1,0:T(8,128)(2,1)S(1)}, bf16[16,160,128]{2,1,0:T(8,128)(2,1)S(1)}, u32[]{:S(2)}, u32[]{:S(2)}) %collective-permute-start.5) | collective-permute-done | bytes 655392 | tf_op jit(solution)/shard_map/ppermute | solution.py:553
  52.2 1.9 %collective-permute-start.6 = (bf16[16,160,128]{2,1,0:T(8,128)(2,1)S(1)}, bf16[16,160,128]{2,1,0:T(8,128)(2,1)}, u32[]{:S(2)}, u32[]{:S(2)}) collective-permute-start(bf16[16,160,128]{2,1,0:T(8,128)(2,1)S(1)} %collective-permute-done.5.p3.refs_3_), channel_id=1, source_target_pairs={{0,4},{4,0},{8,12},{12,8},{16,20},{20,16},{24,28},{28,24},{32,36},... | collective-permute-start | bytes 1966088 | tf_op jit(solution)/shard_map/ppermute | solution.py:556
  54.1 5.0 %collective-permute-done.3.p2.refs_2_ = bf16[16,160,128]{2,1,0:T(8,128)(2,1)S(1)} collective-permute-done((bf16[16,160,128]{2,1,0:T(8,128)(2,1)S(1)}, bf16[16,160,128]{2,1,0:T(8,128)(2,1)S(1)}, u32[]{:S(2)}, u32[]{:S(2)}) %collective-permute-start.3) | collective-permute-done | bytes 655392 | tf_op jit(solution)/shard_map/ppermute | solution.py:553
  59.1 1.9 %collective-permute-start.4 = (bf16[16,160,128]{2,1,0:T(8,128)(2,1)S(1)}, bf16[16,160,128]{2,1,0:T(8,128)(2,1)}, u32[]{:S(2)}, u32[]{:S(2)}) collective-permute-start(bf16[16,160,128]{2,1,0:T(8,128)(2,1)S(1)} %collective-permute-done.3.p2.refs_2_), channel_id=1, source_target_pairs={{0,4},{4,0},{8,12},{12,8},{16,20},{20,16},{24,28},{28,24},{32,36},... | collective-permute-start | bytes 1966088 | tf_op jit(solution)/shard_map/ppermute | solution.py:556
  61.0 2.4 %collective-permute-start.2 = (bf16[16,160,128]{2,1,0:T(8,128)(2,1)S(1)}, bf16[16,160,128]{2,1,0:T(8,128)(2,1)}, u32[]{:S(2)}, u32[]{:S(2)}) collective-permute-start(bf16[16,160,128]{2,1,0:T(8,128)(2,1)S(1)} %collective-permute-done.1.p1.refs_1_), channel_id=1, source_target_pairs={{0,4},{4,0},{8,12},{12,8},{16,20},{20,16},{24,28},{28,24},{32,36},... | collective-permute-start | bytes 1966088 | tf_op jit(solution)/shard_map/ppermute | solution.py:556
  63.5 14.1 %all-gather = bf16[768,512]{1,0:T(8,128)(2,1)S(1)} all-gather(bf16[192,512]{1,0:T(8,128)(2,1)S(1)} %copy-done.11), channel_id=2, replica_groups=mesh['sp'=128,'tp'=4] {'tp'}, dimensions={0}, use_global_device_ids=true | all-gather | bytes 983040 | tf_op jit(solution)/shard_map/all_gather | solution.py:531
  80.0 6.7 %shard_map.202 = (f32[64,128]{1,0:T(8,128)S(1)}, f32[64,128]{1,0:T(8,128)S(1)}, f32[192,128]{1,0:T(8,128)S(1)}, bf16[192,128]{1,0:T(8,128)(2,1)S(1)}, bf16[32,12...) custom-call(s32[1]{0:T(128)} %bitcast.place_ref.core_ref, ...), custom_call_target="tpu_custom_call" | custom-call | tf_op jit(solution)/shard_map/pallas_call | solution.py:90
  86.7 1.9 %collective-permute-start.7 = (f32[64,128]{1,0:T(8,128)S(1)}, f32[64,128]{1,0:T(8,128)S(1)}, u32[]{:S(2)}, u32[]{:S(2)}) collective-permute-start(f32[64,128]{1,0:T(8,128)S(1)} %get-tuple-element.27), channel_id=1, source_target_pairs={{0,4},{4,0},{8,12},{12,8},{16,20},{20,16},{24,28},{28,24},{32,36},... | collective-permute-start | bytes 98312 | tf_op jit(solution)/shard_map/ppermute | solution.py:588
  88.6 1.2 collective-permute-done.7.theirs_ref
  90.0 12.7 %all_to_all.21.steps_ref = bf16[8,64,128]{2,1,0:T(8,128)(2,1)S(1)} all-to-all(bf16[8,64,128]{2,1,0:T(8,128)(2,1)S(1)} %shard_map.204), channel_id=1, replica_groups={{0,8,16,24,32,40,48,56},{4,12,20,28,36,44,52,60},{64,72,80,88,96,104,11..., dimensions={0} | all-to-all | bytes 262144 | tf_op jit(solution)/shard_map/all_to_all | solution.py:489
  103.5 13.2 %all_to_all.22.steps_ref = bf16[8,64,128]{2,1,0:T(8,128)(2,1)S(1)} all-to-all(bf16[8,64,128]{2,1,0:T(8,128)(2,1)S(1)} %get-tuple-element.28), channel_id=1, replica_groups={{0,64,128,192,256,320,384,448},{4,68,132,196,260,324,388,452},{8,72,136..., dimensions={0} | all-to-all | bytes 262144 | tf_op jit(solution)/shard_map/all_to_all | solution.py:489
  117.5 2.1 %collective-permute-start.8 = (f32[64,128]{1,0:T(8,128)S(1)}, f32[64,128]{1,0:T(8,128)S(1)}, u32[]{:S(2)}, u32[]{:S(2)}) collective-permute-start(f32[64,128]{1,0:T(8,128)S(1)} %get-tuple-element.31), channel_id=1, source_target_pairs={{0,4},{4,0},{8,12},{12,8},{16,20},{20,16},{24,28},{28,24},{32,36},... | collective-permute-start | bytes 98312 | tf_op jit(solution)/shard_map/ppermute | solution.py:599
  119.5 2.4 %collective-permute-start.9 = (bf16[32,128]{1,0:T(8,128)(2,1)S(1)}, bf16[32,128]{1,0:T(8,128)(2,1)S(1)}, u32[]{:S(2)}, u32[]{:S(2)}) collective-permute-start(bf16[32,128]{1,0:T(8,128)(2,1)S(1)} %get-tuple-element.34), channel_id=1, source_target_pairs={{0,4},{4,8},{8,12},{12,16},{16,20},{20,24},{24,28},{28,32},{32,36}... | collective-permute-start | bytes 24584 | tf_op jit(solution)/shard_map/ppermute | solution.py:589
  121.9 1.3 shard_map.203.reads_ref
  123.3 1.9 %shard_map.208.columns_ref = bf16[2048,256]{1,0:T(8,128)(2,1)S(1)} custom-call(s32[1]{0:T(128)} %bitcast.place_ref.core_ref, bf16[16,160,128]{2,1,0:T(8,128)(2,1)S(1)} %all_to_all.20.p0.refs_0_, bf16[16,160,128]{2,1,0:T(8,128)(2,1)S(1)} %copy-done.1, bf16[16,160,128]{2,1,0:T(8,128)(2,1)S(1)} %collective-permute-done.3.p2.refs_2_, ...), custom_call_target="tpu_custom_call" | custom-call | tf_op jit(solution)/shard_map/pallas_call | solution.py:90
  125.9 7.9 %psum.7.sums_ref = f32[8,128]{1,0:T(8,128)S(1)} all-reduce(f32[8,128]{1,0:T(8,128)S(1)} %get-tuple-element.36), channel_id=1, replica_groups=mesh['sp'=128,'tp'=4] {'tp'}, use_global_device_ids=true, to_apply=%region_0.0 | all-reduce | flops 1024 | bytes 8192 | tf_op jit(solution)/shard_map/psum | solution.py:604
  133.9 1.0 shard_map.209
  134.9 14.9 %all_to_all.23 = bf16[4,192,512]{2,1,0:T(8,128)(2,1)S(1)} all-to-all(bf16[4,192,512]{2,1,0:T(8,128)(2,1)S(1)} %shard_map.209), channel_id=1, replica_groups=mesh['sp'=128,'tp'=4] {'tp'}, dimensions={0} | all-to-all | bytes 1572864 | tf_op jit(solution)/shard_map/all_to_all | solution.py:623
  (42 shorter events, 5.6 us)
Async XLA Ops:
  1.8 61.7 %copy-start.12 = (f32[2048]{0:T(1024)S(1)}, f32[2048]{0:T(1024)}, u32[]{:S(2)}) copy-start(f32[2048]{0:T(1024)} %param.22) | copy-start | bytes 24580
  1.8 61.7 %copy-start.11 = (bf16[192,512]{1,0:T(8,128)(2,1)S(1)}, bf16[192,512]{1,0:T(8,128)(2,1)}, u32[]{:S(2)}) copy-start(bf16[192,512]{1,0:T(8,128)(2,1)} %param.21) | copy-start | bytes 589828
  38.7 13.5 %collective-permute-start.5 = (bf16[16,160,128]{2,1,0:T(8,128)(2,1)S(1)}, bf16[16,160,128]{2,1,0:T(8,128)(2,1)S(1)}, u32[]{:S(2)}, u32[]{:S(2)}) collective-permute-start(bf16[16,160,128]{2,1,0:T(8,128)(2,1)S(1)} %all_to_all.20.p0.refs_0_), channel_id=1, source_target_pairs={{0,72},{4,508},{8,64},{12,468},{16,88},{20,460},{24,80},{28,484},{... | collective-permute-start | bytes 1966088 | tf_op jit(solution)/shard_map/ppermute | solution.py:553
  41.3 17.8 %collective-permute-start.3 = (bf16[16,160,128]{2,1,0:T(8,128)(2,1)S(1)}, bf16[16,160,128]{2,1,0:T(8,128)(2,1)S(1)}, u32[]{:S(2)}, u32[]{:S(2)}) collective-permute-start(bf16[16,160,128]{2,1,0:T(8,128)(2,1)S(1)} %all_to_all.20.p0.refs_0_), channel_id=1, source_target_pairs={{0,64},{4,452},{8,72},{12,460},{16,80},{20,468},{24,88},{28,476},{... | collective-permute-start | bytes 1966088 | tf_op jit(solution)/shard_map/ppermute | solution.py:553
  44.0 17.0 %collective-permute-start.1 = (bf16[16,160,128]{2,1,0:T(8,128)(2,1)S(1)}, bf16[16,160,128]{2,1,0:T(8,128)(2,1)S(1)}, u32[]{:S(2)}, u32[]{:S(2)}) collective-permute-start(bf16[16,160,128]{2,1,0:T(8,128)(2,1)S(1)} %all_to_all.20.p0.refs_0_), channel_id=1, source_target_pairs={{0,8},{4,60},{8,0},{12,20},{16,24},{20,12},{24,16},{28,36},{32,40}... | collective-permute-start | bytes 1966088 | tf_op jit(solution)/shard_map/ppermute | solution.py:553
  47.9 32.0 %collective-permute-start = (bf16[16,160,128]{2,1,0:T(8,128)(2,1)S(1)}, bf16[16,160,128]{2,1,0:T(8,128)(2,1)}, u32[]{:S(2)}, u32[]{:S(2)}) collective-permute-start(bf16[16,160,128]{2,1,0:T(8,128)(2,1)S(1)} %all_to_all.20.p0.refs_0_), channel_id=1, source_target_pairs={{0,4},{4,0},{8,12},{12,8},{16,20},{20,16},{24,28},{28,24},{32,36},... | collective-permute-start | bytes 1966088 | tf_op jit(solution)/shard_map/ppermute | solution.py:556
  52.2 27.8 %collective-permute-start.6 = (bf16[16,160,128]{2,1,0:T(8,128)(2,1)S(1)}, bf16[16,160,128]{2,1,0:T(8,128)(2,1)}, u32[]{:S(2)}, u32[]{:S(2)}) collective-permute-start(bf16[16,160,128]{2,1,0:T(8,128)(2,1)S(1)} %collective-permute-done.5.p3.refs_3_), channel_id=1, source_target_pairs={{0,4},{4,0},{8,12},{12,8},{16,20},{20,16},{24,28},{28,24},{32,36},... | collective-permute-start | bytes 1966088 | tf_op jit(solution)/shard_map/ppermute | solution.py:556
  59.1 20.9 %collective-permute-start.4 = (bf16[16,160,128]{2,1,0:T(8,128)(2,1)S(1)}, bf16[16,160,128]{2,1,0:T(8,128)(2,1)}, u32[]{:S(2)}, u32[]{:S(2)}) collective-permute-start(bf16[16,160,128]{2,1,0:T(8,128)(2,1)S(1)} %collective-permute-done.3.p2.refs_2_), channel_id=1, source_target_pairs={{0,4},{4,0},{8,12},{12,8},{16,20},{20,16},{24,28},{28,24},{32,36},... | collective-permute-start | bytes 1966088 | tf_op jit(solution)/shard_map/ppermute | solution.py:556
  61.0 17.9 %copy-start = (bf16[16,160,128]{2,1,0:T(8,128)(2,1)}, bf16[16,160,128]{2,1,0:T(8,128)(2,1)S(1)}, u32[]{:S(2)}) copy-start(bf16[16,160,128]{2,1,0:T(8,128)(2,1)S(1)} %collective-permute-done.1.p1.refs_1_) | copy-start | bytes 1966084
  61.0 18.9 %collective-permute-start.2 = (bf16[16,160,128]{2,1,0:T(8,128)(2,1)S(1)}, bf16[16,160,128]{2,1,0:T(8,128)(2,1)}, u32[]{:S(2)}, u32[]{:S(2)}) collective-permute-start(bf16[16,160,128]{2,1,0:T(8,128)(2,1)S(1)} %collective-permute-done.1.p1.refs_1_), channel_id=1, source_target_pairs={{0,4},{4,0},{8,12},{12,8},{16,20},{20,16},{24,28},{28,24},{32,36},... | collective-permute-start | bytes 1966088 | tf_op jit(solution)/shard_map/ppermute | solution.py:556
  77.6 0.9 copy-start.2
  77.6 0.9 copy-start.3
  77.6 0.9 copy-start.7
  77.6 0.9 copy-start.8
  77.6 0.9 copy-start.9
  77.6 0.9 copy-start.10
  78.2 0.7 copy-start.4
  78.2 0.7 copy-start.5
  78.3 0.7 copy-start.6
  86.7 3.1 %collective-permute-start.7 = (f32[64,128]{1,0:T(8,128)S(1)}, f32[64,128]{1,0:T(8,128)S(1)}, u32[]{:S(2)}, u32[]{:S(2)}) collective-permute-start(f32[64,128]{1,0:T(8,128)S(1)} %get-tuple-element.27), channel_id=1, source_target_pairs={{0,4},{4,0},{8,12},{12,8},{16,20},{20,16},{24,28},{28,24},{32,36},... | collective-permute-start | bytes 98312 | tf_op jit(solution)/shard_map/ppermute | solution.py:588
  117.5 5.8 %copy-start.1 = (bf16[16,160,128]{2,1,0:T(8,128)(2,1)S(1)}, bf16[16,160,128]{2,1,0:T(8,128)(2,1)}, u32[]{:S(2)}) copy-start(bf16[16,160,128]{2,1,0:T(8,128)(2,1)} %copy-done) | copy-start | bytes 1966084
  117.5 16.4 %collective-permute-start.8 = (f32[64,128]{1,0:T(8,128)S(1)}, f32[64,128]{1,0:T(8,128)S(1)}, u32[]{:S(2)}, u32[]{:S(2)}) collective-permute-start(f32[64,128]{1,0:T(8,128)S(1)} %get-tuple-element.31), channel_id=1, source_target_pairs={{0,4},{4,0},{8,12},{12,8},{16,20},{20,16},{24,28},{28,24},{32,36},... | collective-permute-start | bytes 98312 | tf_op jit(solution)/shard_map/ppermute | solution.py:599
  119.5 5.7 %collective-permute-start.9 = (bf16[32,128]{1,0:T(8,128)(2,1)S(1)}, bf16[32,128]{1,0:T(8,128)(2,1)S(1)}, u32[]{:S(2)}, u32[]{:S(2)}) collective-permute-start(bf16[32,128]{1,0:T(8,128)(2,1)S(1)} %get-tuple-element.34), channel_id=1, source_target_pairs={{0,4},{4,8},{8,12},{12,16},{16,20},{20,24},{24,28},{28,32},{32,36}... | collective-permute-start | bytes 24584 | tf_op jit(solution)/shard_map/ppermute | solution.py:589
